TPU v7x, 32 devices: a whole 2x2x4 slice. The times are simulated.
32 devices in a mesh: kv: 16 (over z, y, x), tp: 2 (over core).
Axes of the slice: x: 2, y: 2, z: 4, core: 2. Of those that a mesh axis runs over, the one named last changes fastest.
Arguments:
- tokens: bfloat16 [256, 2048], P('kv', 'tp'), may hold values from -20 to 20
- norm_gain: float32 [2048], replicated, may hold values from 0.1 to 1.9
- w_query: bfloat16 [2048, 1024], P(None, 'tp'), may hold values from -0.125 to 0.125
- w_key: bfloat16 [2048, 1024], P(None, 'tp'), may hold values from -0.125 to 0.125
- w_value: bfloat16 [2048, 1024], P(None, 'tp'), may hold values from -0.125 to 0.125
- w_outgate: bfloat16 [2048, 1024], P(None, 'tp'), may hold values from -0.125 to 0.125
- w_input_gate: bfloat16 [2048, 8], replicated, may hold values from -0.125 to 0.125
- w_forget_gate: bfloat16 [2048, 8], replicated, may hold values from -0.125 to 0.125
- memory: float32 [256, 8, 128, 128], P('kv', 'tp'), may hold values from -6 to 6
- normalizer: float32 [256, 8, 128], P('kv', 'tp'), may hold values from -6 to 6
- memory_max: float32 [256, 8], P('kv', 'tp'), may hold values from -2 to 300
- w_output: bfloat16 [1024, 2048], P(None, 'tp'), may hold values from -0.1875 to 0.1875
- ffn_gain: float32 [2048], P('tp'), may hold values from 0.1 to 1.9
- w_gate: bfloat16 [2048, 5632], P('tp', 'kv'), may hold values from -0.125 to 0.125
- w_up: bfloat16 [2048, 5632], P('tp', 'kv'), may hold values from -0.125 to 0.125
- w_down: bfloat16 [5632, 2048], P('kv', 'tp'), may hold values from -0.078125 to 0.078125
Outputs:
- result: bfloat16 [256, 2048], P('kv', 'tp')
- new_memory: float32 [256, 8, 128, 128], P('kv', 'tp')
- new_normalizer: float32 [256, 8, 128], P('kv', 'tp')
- new_max: float32 [256, 8], P('kv', 'tp')
All inputs are finite; a program needn't handle non-finite values.
Results may differ from a plain program's by a relative error of at most 0.013.
Values may be sent and summed in bfloat16 or wider, within the bound.
No kernel may reach another device: no remote copies, remote signals or barrier semaphores. Data moves between devices by JAX's collectives and lax.ppermute only.
A program may use at most 64 MiB of HBM per device.

v0:
```python
import jax
import jax.numpy as jnp
from jax import lax
from jax.sharding import PartitionSpec as P

D = 2048


def activate(gate_sum, up_sum, square_sum):
    ffn_scale = lax.rsqrt(square_sum / D + 1e-06)[:, None]
    return (jax.nn.silu(ffn_scale * gate_sum) * (ffn_scale * up_sum)).astype(jnp.bfloat16)


def per_device(
    tokens,
    norm_gain,
    w_query,
    w_key,
    w_value,
    w_outgate,
    w_input_gate,
    w_forget_gate,
    memory,
    normalizer,
    memory_max,
    w_output,
    ffn_gain,
    w_gate,
    w_up,
    w_down,
):
    local_rows = tokens.shape[0]
    head_count = memory.shape[1]
    head_dim = memory.shape[2]
    full_rows = lax.all_gather(tokens, "tp", axis=1, tiled=True)
    rows_f = full_rows.astype(jnp.float32)
    row_scale = lax.rsqrt(jnp.mean(rows_f * rows_f, axis=-1, keepdims=True) + 1e-06)
    normed = (rows_f * row_scale * norm_gain).astype(jnp.bfloat16)

    def project(weight):
        return jnp.dot(normed, weight, preferred_element_type=jnp.float32).reshape(
            local_rows, head_count, head_dim
        )

    queries = project(w_query) * head_dim ** (-0.5)
    key_vec = project(w_key)
    values = project(w_value)
    outgate = project(w_outgate)
    first_head = lax.axis_index("tp") * head_count
    igate = lax.dynamic_slice_in_dim(
        jnp.dot(normed, w_input_gate, preferred_element_type=jnp.float32), first_head, head_count, 1
    )
    forget_pre = lax.dynamic_slice_in_dim(
        jnp.dot(normed, w_forget_gate, preferred_element_type=jnp.float32),
        first_head,
        head_count,
        1,
    )
    lforget = jax.nn.log_sigmoid(forget_pre)
    new_max = jnp.maximum(lforget + memory_max, igate)
    keep_weight = jnp.exp(lforget + memory_max - new_max)
    admit_weight = jnp.exp(igate - new_max)
    new_memory = keep_weight[..., None, None] * memory + admit_weight[..., None, None] * (
        key_vec[..., :, None] * values[..., None, :]
    )
    new_normalizer = keep_weight[..., None] * normalizer + admit_weight[..., None] * key_vec
    numerator = jnp.einsum("bhd,bhdv->bhv", queries, new_memory, precision=lax.Precision.HIGHEST)
    denominator = jnp.sum(queries * new_normalizer, axis=-1)
    cell_out = numerator / jnp.maximum(jnp.abs(denominator), jnp.exp(-new_max))[..., None]
    head_mean = jnp.mean(cell_out, axis=-1, keepdims=True)
    centered = cell_out - head_mean
    head_var = jnp.mean(centered * centered, axis=-1, keepdims=True)
    mixed = (
        (jax.nn.sigmoid(outgate) * centered * lax.rsqrt(head_var + 1e-05))
        .reshape(local_rows, head_count * head_dim)
        .astype(jnp.bfloat16)
    )
    branch_out = jnp.dot(
        lax.all_gather(mixed, "tp", axis=1, tiled=True),
        w_output,
        preferred_element_type=jnp.float32,
    )
    resid = (tokens.astype(jnp.float32) + branch_out).astype(jnp.bfloat16)
    every_row = lax.all_gather(resid, "kv", axis=0, tiled=True)
    every_f = every_row.astype(jnp.float32)
    square_part = jnp.sum(every_f * every_f, axis=-1)
    ffn_in = (every_f * ffn_gain).astype(jnp.bfloat16)
    gate_part = jnp.dot(ffn_in, w_gate, preferred_element_type=jnp.float32)
    up_part = jnp.dot(ffn_in, w_up, preferred_element_type=jnp.float32)
    gate_full, up_full, square_full = (
        lax.psum(gate_part.astype(jnp.bfloat16), "tp").astype(jnp.float32),
        lax.psum(up_part.astype(jnp.bfloat16), "tp").astype(jnp.float32),
        lax.psum(square_part.astype(jnp.bfloat16), "tp").astype(jnp.float32),
    )
    hidden = activate(gate_full, up_full, square_full)
    down_out = lax.psum_scatter(
        jnp.dot(hidden, w_down, preferred_element_type=jnp.float32),
        "kv",
        scatter_dimension=0,
        tiled=True,
    )
    result = (resid.astype(jnp.float32) + down_out).astype(jnp.bfloat16)
    return (result, new_memory, new_normalizer, new_max)


def solution(mesh):
    placed = (
        P("kv", "tp"),
        P(),
        P(None, "tp"),
        P(None, "tp"),
        P(None, "tp"),
        P(None, "tp"),
        P(),
        P(),
        P("kv", "tp", None, None),
        P("kv", "tp", None),
        P("kv", "tp"),
        P(None, "tp"),
        P("tp"),
        P("tp", "kv"),
        P("tp", "kv"),
        P("kv", "tp"),
    )
    return jax.shard_map(
        per_device,
        mesh=mesh,
        in_specs=placed,
        out_specs=(P("kv", "tp"), P("kv", "tp", None, None), P("kv", "tp", None), P("kv", "tp")),
        check_vma=False,
    )
```

profile of v0, /device:TPU:0, one launch (start us, length us, event | category | flops | bytes accessed | tf_op | source)
XLA Modules:
  0.0 181.3 jit_solution(10911743880774895137)
XLA Ops:
  7.2 0.0 all-reduce.3.cloned.1.call-start
  7.3 2.3 %all_gather.9 = bf16[16,2048]{1,0:T(8,128)(2,1)S(1)} all-gather(bf16[16,1024]{1,0:T(8,128)(2,1)} %param.16), channel_id=1, replica_groups=mesh['kv'=16,'tp'=2] {'tp'}, dimensions={1}, use_global_device_ids=true | all-gather | bytes 98304 | tf_op jit(solution)/shard_map/all_gather | solution.py:35
  9.6 0.1 fusion.11
  9.8 2.0 %convolution_multiply_fusion = f32[16,512]{1,0:T(8,128)S(1)} fusion(bf16[2048,512]{1,0:T(8,128)(2,1)} %param.18, bf16[16,2048]{1,0:T(8,128)(2,1)S(1)} %all_gather.9, f32[2048]{0:T(1024)} %param.17, f32[16]{0:T(128)S(1)} %add_rsqrt_fusion.2), kind=kOutput, calls=%fused_computation.7 | convolution fusion | flops 33693696 | bytes 2203712 | tf_op jit(solution)/shard_map/dot_general | solution.py:41
  11.9 0.2 fusion.21
  12.1 0.2 fusion.23
  12.3 0.1 copy.25
  12.4 0.1 copy.26
  12.5 2.0 %fusion.19 = f32[16,512]{1,0:T(8,128)S(1)} fusion(bf16[2048,512]{1,0:T(8,128)(2,1)} %param.19, bf16[16,2048]{1,0:T(8,128)(2,1)S(1)} %all_gather.9, f32[2048]{0:T(1024)S(1)} %copy-done.3, f32[16]{0:T(128)S(1)} %add_rsqrt_fusion.2), kind=kOutput, calls=%fused_computation.43 | convolution fusion | flops 33685504 | bytes 2203712 | tf_op jit(solution)/shard_map/dot_general | solution.py:41
  14.6 0.7 multiply_reduce_fusion.1
  15.3 0.1 copy.29
  15.4 0.1 copy.30
  15.5 2.2 %fusion.17 = f32[16,512]{1,0:T(8,128)S(1)} fusion(bf16[2048,512]{1,0:T(8,128)(2,1)} %param.20, bf16[16,2048]{1,0:T(8,128)(2,1)S(1)} %all_gather.9, f32[2048]{0:T(1024)S(1)} %copy-done.3, f32[16]{0:T(128)S(1)} %add_rsqrt_fusion.2), kind=kOutput, calls=%fused_computation.42 | convolution fusion | flops 33685504 | bytes 2203712 | tf_op jit(solution)/shard_map/dot_general | solution.py:41
  17.6 0.1 copy-done.2
  17.7 0.4 fusion.3
  18.2 3.7 %multiply_add_fusion = f32[16,4,128,128]{3,2,1,0:T(8,128)S(1)} fusion(f32[16,4,128,128]{3,2,1,0:T(8,128)} %param.24, f32[16,4,128]{2,1,0:T(4,128)S(1)} %mul.143, f32[16,4,128]{2,1,0:T(4,128)S(1)} %mul.141, f32[16,4]{1,0:T(8,128)S(1)} %copy.26, f32[16,4]{1,0:T(8,128)S(1)} %copy.25), kind=kLoop, calls=%fused_computation | loop fusion | flops 4194304 | bytes 8454656 | tf_op jit(solution)/shard_map/add | solution.py:63
  21.9 3.7 %fusion.28 = f32[16,4,1,128]{3,2,1,0:T(1,128)S(1)} fusion(f32[16,4,128,1]{2,3,1,0:T(1,128)S(1)} %bitcast.20, f32[16,4,128,128]{3,2,1,0:T(8,128)S(1)} %multiply_add_fusion), kind=kOutput, calls=%fused_computation.47 | convolution fusion | flops 12582912 | bytes 4259840 | tf_op jit(solution)/shard_map/bhd,bhdv->bhv/dot_general | solution.py:67
  25.6 0.2 fusion.27
  25.8 0.2 multiply_reduce_fusion
  26.0 0.1 multiply_convert_fusion.2
  26.1 1.8 %all_gather.10 = bf16[16,1024]{1,0:T(8,128)(2,1)S(1)} all-gather(bf16[16,512]{1,0:T(8,128)(2,1)S(1)} %bitcast.22), channel_id=1, replica_groups=mesh['kv'=16,'tp'=2] {'tp'}, dimensions={1}, use_global_device_ids=true | all-gather | bytes 49152 | tf_op jit(solution)/shard_map/all_gather | solution.py:79
  27.9 0.4 fusion
  28.3 45.4 %all_gather.11 = bf16[256,1024]{1,0:T(8,128)(2,1)S(1)} all-gather(bf16[16,1024]{1,0:T(8,128)(2,1)S(1)} %fusion), channel_id=1, replica_groups=mesh['kv'=16,'tp'=2] {'kv'}, dimensions={0}, use_global_device_ids=true | all-gather | bytes 557056 | tf_op jit(solution)/shard_map/all_gather | solution.py:84
  73.7 1.1 convolution_convert_fusion
  74.8 1.1 convolution_convert_fusion.1
  75.9 0.0 reduce-scatter.2.cloned.1.call-start
  75.9 0.2 fusion.4
  76.1 2.5 %psum.21 = bf16[256]{0:T(256)(128)(2,1)S(1)} all-reduce(bf16[256]{0:T(256)(128)(2,1)S(1)} %fusion.4), channel_id=1, replica_groups=mesh['kv'=16,'tp'=2] {'tp'}, use_global_device_ids=true, to_apply=%region_5.6 | all-reduce | flops 256 | bytes 1024 | tf_op jit(solution)/shard_map/psum | solution.py:93
  78.6 11.7 %all-reduce.3.cloned.1.call-done = (bf16[256,352]{0,1:T(8,128)(2,1)}, bf16[256,352]{0,1:T(8,128)(2,1)}) async-done(((bf16[256,352]{0,1:T(8,128)(2,1)}, bf16[256,352]{0,1:T(8,128)(2,1)}), (bf16[256,352]{0,1:T(8,128)(2,1)}, bf16[256,352]{0,1:T(8,128)(2,1)})) %all-reduce.3.cloned.1.call-update) | async-done | bytes 360464 | tf_op jit(solution)/shard_map/psum | solution.py:92
  90.3 2.5 %fusion.8 = f32[256,1024]{1,0:T(8,128)} fusion(bf16[352,1024]{1,0:T(8,128)(2,1)S(1)} %copy-done.10, bf16[256,352]{0,1:T(8,128)(2,1)} %get-tuple-element.4, bf16[256,352]{0,1:T(8,128)(2,1)} %get-tuple-element.5, f32[256]{0:T(256)S(1)} %add_rsqrt_fusion.1), kind=kOutput, calls=%fused_computation.15 | convolution fusion | flops 185450496 | bytes 2130944 | tf_op jit(solution)/shard_map/dot_general | solution.py:97
  92.9 80.1 %reduce-scatter.2.cloned.1.call-done = f32[16,1024]{1,0:T(8,128)} async-done(((f32[256,1024]{1,0:T(8,128)}), f32[16,1024]{1,0:T(8,128)}) %reduce-scatter.2.cloned.1.call-update) | async-done | bytes 65552 | tf_op jit(solution)/shard_map/reduce_scatter | solution.py:96
  173.0 1.5 add_convert_fusion
  (42 shorter events, 0.3 us)
Async XLA Ops:
  7.2 20.7 %copy-start = (bf16[1024,1024]{1,0:T(8,128)(2,1)S(1)}, bf16[1024,1024]{1,0:T(8,128)(2,1)}, u32[]{:S(2)}) copy-start(bf16[1024,1024]{1,0:T(8,128)(2,1)} %param.27) | copy-start | bytes 6291460
  7.2 4.7 %copy-start.3 = (f32[2048]{0:T(1024)S(1)}, f32[2048]{0:T(1024)}, u32[]{:S(2)}) copy-start(f32[2048]{0:T(1024)} %param.17) | copy-start | bytes 24580
  7.2 4.7 %copy-start.11 = (bf16[2048,8]{0,1:T(8,128)(2,1)S(1)}, bf16[2048,8]{0,1:T(8,128)(2,1)}, u32[]{:S(2)}) copy-start(bf16[2048,8]{0,1:T(8,128)(2,1)} %param.22) | copy-start | bytes 98308
  7.2 4.9 %copy-start.12 = (bf16[2048,8]{0,1:T(8,128)(2,1)S(1)}, bf16[2048,8]{0,1:T(8,128)(2,1)}, u32[]{:S(2)}) copy-start(bf16[2048,8]{0,1:T(8,128)(2,1)} %param.23) | copy-start | bytes 98308
  7.2 5.1 %copy-start.7 = (f32[16,4]{0,1:T(4,128)S(1)}, f32[16,4]{0,1:T(4,128)}, u32[]{:S(2)}) copy-start(f32[16,4]{0,1:T(4,128)} %param.26) | copy-start | bytes 772
  7.2 83.1 %all-reduce.3.cloned.1.call-start = ((), (), s32[]{:S(2)}) async-start(), calls=%async_computation.2 | async-start | bytes 720896 | tf_op jit(solution)/shard_map/psum | solution.py:92
  9.8 4.8 %copy-start.5 = (f32[16,4,128]{2,1,0:T(4,128)S(1)}, f32[16,4,128]{2,1,0:T(4,128)}, u32[]{:S(2)}) copy-start(f32[16,4,128]{2,1,0:T(4,128)} %param.25) | copy-start | bytes 98308
  12.3 5.3 %copy-start.6 = (f32[16,4]{0,1:T(4,128)}, f32[16,4]{0,1:T(4,128)S(1)}, u32[]{:S(2)}) copy-start(f32[16,4]{0,1:T(4,128)S(1)} %get-tuple-element.11) | copy-start | bytes 772
  15.4 2.2 %copy-start.2 = (bf16[2048,512]{1,0:T(8,128)(2,1)S(1)}, bf16[2048,512]{1,0:T(8,128)(2,1)}, u32[]{:S(2)}) copy-start(bf16[2048,512]{1,0:T(8,128)(2,1)} %param.21) | copy-start | bytes 6291460
  21.9 3.7 %copy-start.1 = (f32[16,4,128,128]{3,2,1,0:T(8,128)}, f32[16,4,128,128]{3,2,1,0:T(8,128)S(1)}, u32[]{:S(2)}) copy-start(f32[16,4,128,128]{3,2,1,0:T(8,128)S(1)} %multiply_add_fusion) | copy-start | bytes 12582916
  21.9 6.0 %copy-start.4 = (bf16[16,1024]{1,0:T(8,128)(2,1)S(1)}, bf16[16,1024]{1,0:T(8,128)(2,1)}, u32[]{:S(2)}) copy-start(bf16[16,1024]{1,0:T(8,128)(2,1)} %param.16) | copy-start | bytes 98308
  25.6 48.1 %copy-start.8 = (bf16[1024,352]{0,1:T(8,128)(2,1)S(1)}, bf16[1024,352]{0,1:T(8,128)(2,1)}, u32[]{:S(2)}) copy-start(bf16[1024,352]{0,1:T(8,128)(2,1)} %param.30) | copy-start | bytes 2162692
  25.6 48.1 %copy-start.13 = (f32[1024]{0:T(1024)S(1)}, f32[1024]{0:T(1024)}, u32[]{:S(2)}) copy-start(f32[1024]{0:T(1024)} %param.28) | copy-start | bytes 12292
  27.9 46.9 %copy-start.9 = (bf16[1024,352]{0,1:T(8,128)(2,1)S(1)}, bf16[1024,352]{0,1:T(8,128)(2,1)}, u32[]{:S(2)}) copy-start(bf16[1024,352]{0,1:T(8,128)(2,1)} %param.29) | copy-start | bytes 2162692
  73.7 16.6 %copy-start.10 = (bf16[352,1024]{1,0:T(8,128)(2,1)S(1)}, bf16[352,1024]{1,0:T(8,128)(2,1)}, u32[]{:S(2)}) copy-start(bf16[352,1024]{1,0:T(8,128)(2,1)} %param.31) | copy-start | bytes 2162692
  75.9 97.1 %reduce-scatter.2.cloned.1.call-start = ((), (), s32[]{:S(2)}) async-start(), calls=%async_computation.1 | async-start | bytes 1114112 | tf_op jit(solution)/shard_map/reduce_scatter | solution.py:96
Sparse Core Ops, SparseCore 0:
  76.0 14.2 all-reduce.2
  93.0 79.9 reduce-scatter.1
where the time goes:
time: 182 us; the launch traced here: 181 us
  waiting for transfers between devices  91.8 us (50%)
  blocking collectives  52 us (29%)
  matrix products  15.8 us (9%)
  between operations  14.3 us (8%)
  other arithmetic  6.72 us (4%)
    reduce_scatter x1, waiting for transfers between devices, per_device(): lax.psum_scatter(jnp.dot(hidden, w_down, preferred_element_type=jnp.float...  80.1 us
    all_gather x1, blocking collectives, per_device(): every_row = lax.all_gather(resid, 'kv', axis=0, tiled=True)  45.4 us
    psum x1, waiting for transfers between devices, per_device(): lax.psum(up_part.astype(jnp.bfloat16), 'tp').astype(jnp.float32)  11.7 us
    dot_general x4, matrix products, project(): jnp.dot(normed, weight, preferred_element_type=jnp.float32)  6.65 us
    add x1, other arithmetic, per_device(): keep_weight[..., None, None] * memory  3.72 us
    dot_general x1, matrix products, per_device(): jnp.einsum('bhd,bhdv->bhv', queries, new_memory, precision=lax.Precision....  3.66 us
  transfers between devices with their start and end apart: 2, of which 2 were waited for; matrix products, arithmetic and copies ran while one was open for 0% of the time, Pallas kernels for 0%

commit v1 on v0

v1 whole, which is shorter than its diff:
```python
import jax
import jax.numpy as jnp
from jax import lax
from jax.sharding import PartitionSpec as P

BF16 = jnp.bfloat16
F32 = jnp.float32


def shifted(x, axis, size, step):
    return lax.ppermute(x, axis, [(i, (i + step) % size) for i in range(size)])


def gather_columns(x, axis, size):
    if size != 2:
        return lax.all_gather(x, axis, axis=1, tiled=True)
    other = shifted(x, axis, size, 1)
    first = lax.axis_index(axis) == 0
    return jnp.concatenate([jnp.where(first, x, other), jnp.where(first, other, x)], axis=1)


def gather_rows(x, axis, size):
    copies = jnp.broadcast_to(x[None], (size,) + x.shape)
    return lax.all_to_all(copies, axis, 0, 0).reshape(size * x.shape[0], x.shape[1])


def make(kv, tp):
    def per_device(
        tokens,
        norm_gain,
        w_query,
        w_key,
        w_value,
        w_outgate,
        w_input_gate,
        w_forget_gate,
        memory,
        normalizer,
        memory_max,
        w_output,
        ffn_gain,
        w_gate,
        w_up,
        w_down,
    ):
        rows, own_channels = tokens.shape
        heads, head_dim = memory.shape[1], memory.shape[2]
        channels = own_channels * tp
        hidden_units = w_gate.shape[1]

        full_rows = gather_columns(tokens, "tp", tp).astype(F32)
        row_scale = lax.rsqrt(jnp.mean(full_rows * full_rows, axis=-1, keepdims=True) + 1e-06)
        normed = (full_rows * row_scale * norm_gain).astype(BF16)

        def project(weight):
            return jnp.dot(normed, weight, preferred_element_type=F32)

        def by_head(x):
            return x.reshape(rows, heads, head_dim)

        queries = by_head(project(w_query)) * head_dim ** (-0.5)
        key_vec = by_head(project(w_key))
        values = by_head(project(w_value))
        outgate = by_head(project(w_outgate))
        first_head = lax.axis_index("tp") * heads
        igate = lax.dynamic_slice_in_dim(project(w_input_gate), first_head, heads, 1)
        forget_pre = lax.dynamic_slice_in_dim(project(w_forget_gate), first_head, heads, 1)
        lforget = jax.nn.log_sigmoid(forget_pre)
        new_max = jnp.maximum(lforget + memory_max, igate)
        keep = jnp.exp(lforget + memory_max - new_max)
        admit = jnp.exp(igate - new_max)
        new_normalizer = keep[..., None] * normalizer + admit[..., None] * key_vec
        old_part = jnp.einsum("bhd,bhdv->bhv", queries, memory, precision=lax.Precision.HIGHEST)
        query_key = jnp.sum(queries * key_vec, axis=-1)
        numerator = keep[..., None] * old_part + (admit * query_key)[..., None] * values
        denominator = jnp.sum(queries * new_normalizer, axis=-1)
        cell_out = numerator / jnp.maximum(jnp.abs(denominator), jnp.exp(-new_max))[..., None]
        head_mean = jnp.mean(cell_out, axis=-1, keepdims=True)
        centered = cell_out - head_mean
        head_var = jnp.mean(centered * centered, axis=-1, keepdims=True)
        mixed = jax.nn.sigmoid(outgate) * centered * lax.rsqrt(head_var + 1e-05)
        mixed = mixed.reshape(rows, heads * head_dim).astype(BF16)

        branch_out = jnp.dot(gather_columns(mixed, "tp", tp), w_output, preferred_element_type=F32)
        resid = (tokens.astype(F32) + branch_out).astype(BF16)
        every_row = gather_rows(resid, "kv", kv)
        new_memory = keep[..., None, None] * memory + admit[..., None, None] * (
            key_vec[..., :, None] * values[..., None, :]
        )

        every_f = every_row.astype(F32)
        squares = jnp.sum(every_f * every_f, axis=-1, keepdims=True)
        squares_hi = squares.astype(BF16)
        squares_lo = (squares - squares_hi.astype(F32)).astype(BF16)
        ffn_in = (every_f * ffn_gain).astype(BF16)
        gate_part = jnp.dot(ffn_in, w_gate, preferred_element_type=F32)
        up_part = jnp.dot(ffn_in, w_up, preferred_element_type=F32)
        packed = jnp.concatenate([gate_part.astype(BF16), up_part.astype(BF16), squares_hi, squares_lo], axis=1)
        for step in range(1, tp):
            other = shifted(packed, "tp", tp, step).astype(F32)
            gate_part = gate_part + other[:, :hidden_units]
            up_part = up_part + other[:, hidden_units : 2 * hidden_units]
            squares = squares + jnp.sum(other[:, 2 * hidden_units :], axis=1, keepdims=True)
        ffn_scale = lax.rsqrt(squares / channels + 1e-06)
        hidden = (jax.nn.silu(ffn_scale * gate_part) * (ffn_scale * up_part)).astype(BF16)
        down_part = jnp.dot(hidden, w_down, preferred_element_type=F32).astype(BF16)
        pieces = lax.all_to_all(down_part.reshape(kv, rows, own_channels), "kv", 0, 0)
        down_out = jnp.sum(pieces.astype(F32), axis=0)
        result = (resid.astype(F32) + down_out).astype(BF16)
        return (result, new_memory, new_normalizer, new_max)

    return per_device


def solution(mesh):
    placed = (
        P("kv", "tp"),
        P(),
        P(None, "tp"),
        P(None, "tp"),
        P(None, "tp"),
        P(None, "tp"),
        P(),
        P(),
        P("kv", "tp", None, None),
        P("kv", "tp", None),
        P("kv", "tp"),
        P(None, "tp"),
        P("tp"),
        P("tp", "kv"),
        P("tp", "kv"),
        P("kv", "tp"),
    )
    return jax.shard_map(
        make(mesh.shape["kv"], mesh.shape["tp"]),
        mesh=mesh,
        in_specs=placed,
        out_specs=(P("kv", "tp"), P("kv", "tp", None, None), P("kv", "tp", None), P("kv", "tp")),
        check_vma=False,
    )
```

time: 182 us -> 71.4 us (0.39)
  waiting for transfers between devices: 91.8 us -> 13 us
  blocking collectives: 52 us -> 23.5 us
  between operations: 14.3 us -> 0.99 us
  starting transfers between devices: 0.08 us -> 4.99 us
  other arithmetic: 6.72 us -> 9.29 us
  local copies, waits for them, and re-layouts: 0.54 us -> 2.66 us
    reduce_scatter x1 -> x0, waiting for transfers between devices: 80.1 us -> none  [per_device(): lax.psum_scatter(jnp.dot(hidden, w_down, preferred_element_type=jnp.float...]
    all_gather x3 -> x0, blocking collectives: 49.6 us -> none  [the longest x1 45.4 us: per_device(): every_row = lax.all_gather(resid, 'kv', axis=0, tiled=True)]
    all_to_all x0 -> x1, blocking collectives: none -> 23.5 us  [gather_rows(): lax.all_to_all(copies, axis, 0, 0).reshape(size * x.shape[0], x.shape[1])]
    psum x1 -> x0, waiting for transfers between devices: 11.7 us -> none  [per_device(): lax.psum(up_part.astype(jnp.bfloat16), 'tp').astype(jnp.float32)]
    all_to_all x0 -> x1, waiting for transfers between devices: none -> 10.8 us  [per_device(): lax.all_to_all(down_part.reshape(kv, rows, own_channels), 'kv', 0, 0)]
    all_to_all x0 -> x1, starting transfers between devices: none -> 3.95 us  [per_device(): lax.all_to_all(down_part.reshape(kv, rows, own_channels), 'kv', 0, 0)]
    psum x1 -> x0, blocking collectives: 2.47 us -> none  [per_device(): lax.psum(square_part.astype(jnp.bfloat16), 'tp').astype(jnp.float32)]
    ppermute x0 -> x3, waiting for transfers between devices: none -> 2.22 us  [shifted(): return lax.ppermute(x, axis, [(i, (i + step) % size) for i in range(size)])]
  transfers between devices with their start and end apart: 2 -> 4, of which waited for: 2 -> 4; matrix products, arithmetic and copies ran while one was open for 0% -> 8% of each run, Pallas kernels for 0% -> 0%
where the time goes in v1:
time: 71.4 us; the launch traced here: 70.9 us
  blocking collectives  23.5 us (33%)
  matrix products  16.4 us (23%)
  waiting for transfers between devices  13 us (18%)
  other arithmetic  9.29 us (13%)
  starting transfers between devices  4.99 us (7%)
  local copies, waits for them, and re-layouts  2.66 us (4%)
  between operations  0.99 us (1%)
    all_to_all x1, blocking collectives, gather_rows(): lax.all_to_all(copies, axis, 0, 0).reshape(size * x.shape[0], x.shape[1])  23.5 us
    all_to_all x1, waiting for transfers between devices, per_device(): lax.all_to_all(down_part.reshape(kv, rows, own_channels), 'kv', 0, 0)  10.8 us
    dot_general x6, matrix products, project(): return jnp.dot(normed, weight, preferred_element_type=F32)  6.7 us
    dot_general x1, matrix products, per_device(): jnp.einsum('bhd,bhdv->bhv', queries, memory, precision=lax.Precision.HIGH...  5.28 us
    add x1, other arithmetic, per_device(): keep[..., None, None] * memory  4.59 us
    all_to_all x1, starting transfers between devices, per_device(): lax.all_to_all(down_part.reshape(kv, rows, own_channels), 'kv', 0, 0)  3.95 us
    dot_general x1, matrix products, per_device(): down_part = jnp.dot(hidden, w_down, preferred_element_type=F32).astype(BF16)  2.53 us
    ppermute x3, waiting for transfers between devices, shifted(): return lax.ppermute(x, axis, [(i, (i + step) % size) for i in range(size)])  2.22 us
  transfers between devices with their start and end apart: 4, of which 4 were waited for; matrix products, arithmetic and copies ran while one was open for 8% of the time, Pallas kernels for 0%

profile of v1, /device:TPU:0, one launch (start us, length us, event | category | flops | bytes accessed | tf_op | source)
XLA Modules:
  0.0 70.9 jit_solution(4676911320061926078)
XLA Ops:
  0.7 0.6 collective-permute-start
  1.2 1.1 %collective-permute-done = bf16[16,1024]{1,0:T(8,128)(2,1)S(1)} collective-permute-done((bf16[16,1024]{1,0:T(8,128)(2,1)}, bf16[16,1024]{1,0:T(8,128)(2,1)S(1)}, u32[]{:S(2)}, u32[]{:S(2)}) %collective-permute-start) | collective-permute-done | bytes 32800 | tf_op jit(solution)/shard_map/ppermute | solution.py:11
  2.3 0.8 %broadcast_select_fusion.1 = (bf16[16,1024]{1,0:T(8,128)(2,1)S(1)}, bf16[16,1024]{1,0:T(8,128)(2,1)S(1)}) fusion(bf16[16,1024]{1,0:T(8,128)(2,1)} %param.16, bf16[16,1024]{1,0:T(8,128)(2,1)S(1)} %collective-permute-done, pred[]{:T(512)S(6)} %eq.4), kind=kLoop, calls=%fused_computation.39 | loop fusion | flops 32768 | bytes 131073 | tf_op jit(solution)/shard_map/jit(_where)/select_n | solution.py:19
  3.1 0.1 fusion.12
  3.2 0.8 %fusion.14 = bf16[16,2048]{1,0:T(8,128)(2,1)S(1)} fusion(f32[2048]{0:T(1024)} %param.17, f32[16]{0:T(128)S(1)} %add_rsqrt_fusion.2, bf16[16,1024]{1,0:T(8,128)(2,1)S(1)} %get-tuple-element.12, bf16[16,1024]{1,0:T(8,128)(2,1)S(1)} %get-tuple-element.11), kind=kLoop, calls=%fused_computation.26 | loop fusion | flops 229376 | bytes 139328 | tf_op jit(solution)/shard_map/convert_element_type | solution.py:53
  4.0 2.0 %convolution_multiply_fusion = f32[16,512]{1,0:T(8,128)S(1)} fusion(bf16[16,2048]{1,0:T(8,128)(2,1)S(1)} %fusion.14, bf16[2048,512]{1,0:T(8,128)(2,1)} %param.18), kind=kOutput, calls=%fused_computation.4 | convolution fusion | flops 33562624 | bytes 2195456 | tf_op jit(solution)/shard_map/dot_general | solution.py:56
  6.0 0.1 fusion.27
  6.2 0.1 fusion.26
  6.5 2.0 %fusion.30 = f32[16,512]{1,0:T(8,128)S(1)} fusion(bf16[16,2048]{1,0:T(8,128)(2,1)S(1)} %fusion.14, bf16[2048,512]{1,0:T(8,128)(2,1)} %param.20), kind=kOutput, calls=%fused_computation.66 | convolution fusion | flops 33554432 | bytes 2195456 | tf_op jit(solution)/shard_map/dot_general | solution.py:56
  8.6 2.1 %fusion.29 = f32[16,512]{1,0:T(8,128)S(1)} fusion(bf16[16,2048]{1,0:T(8,128)(2,1)S(1)} %fusion.14, bf16[2048,512]{1,0:T(8,128)(2,1)} %param.19), kind=kOutput, calls=%fused_computation.65 | convolution fusion | flops 33554432 | bytes 2195456 | tf_op jit(solution)/shard_map/dot_general | solution.py:56
  10.8 0.4 fusion.3
  11.3 0.7 %multiply_reduce_fusion.3 = (f32[16,4]{1,0:T(8,128)S(1)}, f32[16,4]{1,0:T(8,128)S(1)}, f32[16,4,128]{2,1,0:T(4,128)}) fusion(f32[16,4,128]{2,1,0:T(4,128)S(1)} %mul.155, f32[16,4,128]{2,1,0:T(4,128)S(1)} %reshape.114, f32[16,4]{1,0:T(8,128)S(1)} %copy.37, f32[16,4,128]{2,1,0:T(4,128)S(1)} %copy-done.17, f32[16,4]{1,0:T(8,128)S(1)} %copy.34), kind=kLoop, calls=%fused_computation.37 | loop fusion | flops 57216 | bytes 132096 | tf_op jit(solution)/shard_map/reduce_sum | solution.py:74
  12.3 5.3 %fusion.28 = f32[16,4,1,128]{3,2,1,0:T(1,128)S(1)} fusion(f32[16,4,128,1]{2,3,1,0:T(1,128)S(1)} %bitcast.38, f32[16,4,128,128]{3,2,1,0:T(8,128)} %param.24), kind=kOutput, calls=%fused_computation.64 | convolution fusion | flops 12582912 | bytes 4259840 | tf_op jit(solution)/shard_map/bhd,bhdv->bhv/dot_general | solution.py:73
  17.6 0.2 fusion.22
  17.8 0.2 multiply_reduce_fusion.1
  18.1 0.4 collective-permute-start.1
  18.5 0.8 %collective-permute-done.1 = bf16[16,512]{1,0:T(8,128)(2,1)S(1)} collective-permute-done((bf16[16,512]{1,0:T(8,128)(2,1)S(1)}, bf16[16,512]{1,0:T(8,128)(2,1)S(1)}, u32[]{:S(2)}, u32[]{:S(2)}) %collective-permute-start.1) | collective-permute-done | bytes 16416 | tf_op jit(solution)/shard_map/ppermute | solution.py:11
  19.4 0.4 fusion
  19.9 23.5 %all_to_all.10 = bf16[16,16,1024]{2,1,0:T(8,128)(2,1)S(1)} all-to-all(bf16[16,16,1024]{2,1,0:T(8,128)(2,1)S(1)} %broadcast_in_dim.2), channel_id=1, replica_groups=mesh['kv'=16,'tp'=2] {'kv'}, dimensions={0} | all-to-all | bytes 1048576 | tf_op jit(solution)/shard_map/all_to_all | solution.py:24
  43.4 0.2 multiply_reduce_fusion
  43.7 0.1 fusion.4
  43.8 0.4 copy-done.12
  44.2 1.1 %fusion.25 = (bf16[256,352]{0,1:T(8,128)(2,1)S(1)}, f32[256,352]{0,1:T(8,128)}) fusion(bf16[256,1024]{1,0:T(8,128)(2,1)S(1)} %fusion.4, bf16[1024,352]{0,1:T(8,128)(2,1)S(1)} %copy-done.2), kind=kOutput, calls=%fused_computation.61 | convolution fusion | flops 184639488 | bytes 1785856 | tf_op jit(solution)/shard_map/dot_general | solution.py:96
  45.3 0.4 fusion.24
  45.8 1.4 %reduce_sum.82 = f32[256]{0:T(256)} reshape(f32[16,16]{1,0:T(8,128)} %copy-done.12) | data formatting | bytes 2048 | tf_op jit(solution)/shard_map/reduce_sum | solution.py:92
  47.2 0.3 collective-permute-done.2
  47.6 0.7 add_rsqrt_fusion.1
  48.3 2.5 %convolution_convert_fusion = bf16[256,1024]{1,0:T(8,128)(2,1)} fusion(bf16[352,1024]{1,0:T(8,128)(2,1)} %param.31, f32[256,352]{0,1:T(8,128)S(1)} %get-tuple-element.18, f32[256,706]{0,1:T(8,128)S(1)} %convert_element_type.107, f32[256,352]{0,1:T(8,128)S(1)} %copy-done.4, f32[256]{0:T(256)S(1)} %add_rsqrt_fusion.1), kind=kOutput, calls=%fused_computation.1 | convolution fusion | flops 185712640 | bytes 2688000 | tf_op jit(solution)/shard_map/dot_general | solution.py:106
  50.8 3.9 %all-to-all-start.1 = ((bf16[16,16,1024]{2,1,0:T(8,128)(2,1)}), bf16[16,16,1024]{2,1,0:T(8,128)(2,1)S(1)}, u32[]{:S(2)}, u32[]{:S(2)}) async-start(bf16[16,16,1024]{2,1,0:T(8,128)(2,1)} %bitcast.4), calls=%async_computation.1 | async-start | bytes 1048576 | tf_op jit(solution)/shard_map/all_to_all | solution.py:107
  54.8 4.6 %multiply_add_fusion = f32[16,4,128,128]{3,2,1,0:T(8,128)} fusion(f32[16,4,128,128]{3,2,1,0:T(8,128)} %param.24, f32[16,4,128]{2,1,0:T(4,128)S(1)} %copy-done.10, f32[16,4,128]{2,1,0:T(4,128)S(1)} %copy-done.6, f32[16,4]{1,0:T(8,128)S(1)} %copy-done.14, f32[16,4]{1,0:T(8,128)S(1)} %copy.34), kind=kLoop, calls=%fused_computation | loop fusion | flops 4194304 | bytes 8454656 | tf_op jit(solution)/shard_map/add | solution.py:87
  59.4 10.8 %all-to-all-done.1 = bf16[16,16,1024]{2,1,0:T(8,128)(2,1)S(1)} async-done(((bf16[16,16,1024]{2,1,0:T(8,128)(2,1)}), bf16[16,16,1024]{2,1,0:T(8,128)(2,1)S(1)}, u32[]{:S(2)}, u32[]{:S(2)}) %all-to-all-start.1) | async-done | bytes 524320 | tf_op jit(solution)/shard_map/all_to_all | solution.py:107
  70.3 0.6 add_convert_fusion
  (70 shorter events, 1.3 us)
Async XLA Ops:
  0.6 18.8 %copy-start = (bf16[1024,1024]{1,0:T(8,128)(2,1)S(1)}, bf16[1024,1024]{1,0:T(8,128)(2,1)}, u32[]{:S(2)}) copy-start(bf16[1024,1024]{1,0:T(8,128)(2,1)} %param.27) | copy-start | bytes 6291460
  0.6 5.4 %copy-start.15 = (bf16[2048,8]{0,1:T(8,128)(2,1)S(1)}, bf16[2048,8]{0,1:T(8,128)(2,1)}, u32[]{:S(2)}) copy-start(bf16[2048,8]{0,1:T(8,128)(2,1)} %param.22) | copy-start | bytes 98308
  0.7 5.5 %copy-start.16 = (bf16[2048,8]{0,1:T(8,128)(2,1)S(1)}, bf16[2048,8]{0,1:T(8,128)(2,1)}, u32[]{:S(2)}) copy-start(bf16[2048,8]{0,1:T(8,128)(2,1)} %param.23) | copy-start | bytes 98308
  0.7 5.6 %copy-start.20 = (f32[16,4]{0,1:T(4,128)S(1)}, f32[16,4]{0,1:T(4,128)}, u32[]{:S(2)}) copy-start(f32[16,4]{0,1:T(4,128)} %param.26) | copy-start | bytes 772
  0.7 1.6 %collective-permute-start = (bf16[16,1024]{1,0:T(8,128)(2,1)}, bf16[16,1024]{1,0:T(8,128)(2,1)S(1)}, u32[]{:S(2)}, u32[]{:S(2)}) collective-permute-start(bf16[16,1024]{1,0:T(8,128)(2,1)} %param.16), channel_id=1, source_target_pairs={{0,1},{1,0},{2,3},{3,2},{4,5},{5,4},{6,7},{7,6},{8,9},{9,8},{10,11... | collective-permute-start | bytes 98312 | tf_op jit(solution)/shard_map/ppermute | solution.py:11
  6.3 5.8 %copy-start.18 = (f32[16,4]{0,1:T(4,128)}, f32[16,4]{0,1:T(4,128)S(1)}, u32[]{:S(2)}) copy-start(f32[16,4]{0,1:T(4,128)S(1)} %get-tuple-element.10) | copy-start | bytes 772
  6.5 4.7 %copy-start.13 = (f32[16,4]{1,0:T(8,128)}, f32[16,4]{1,0:T(8,128)S(1)}, u32[]{:S(2)}) copy-start(f32[16,4]{1,0:T(8,128)S(1)} %copy.37) | copy-start | bytes 772
  8.5 9.1 %copy-start.9 = (f32[16,4,128]{2,1,0:T(4,128)}, f32[16,4,128]{2,1,0:T(4,128)S(1)}, u32[]{:S(2)}) copy-start(f32[16,4,128]{2,1,0:T(4,128)S(1)} %reshape.115) | copy-start | bytes 98308
  8.5 2.2 %copy-start.1 = (bf16[2048,512]{1,0:T(8,128)(2,1)S(1)}, bf16[2048,512]{1,0:T(8,128)(2,1)}, u32[]{:S(2)}) copy-start(bf16[2048,512]{1,0:T(8,128)(2,1)} %param.21) | copy-start | bytes 6291460
  8.6 2.7 %copy-start.17 = (f32[16,4,128]{2,1,0:T(4,128)S(1)}, f32[16,4,128]{2,1,0:T(4,128)}, u32[]{:S(2)}) copy-start(f32[16,4,128]{2,1,0:T(4,128)} %param.25) | copy-start | bytes 98308
  11.2 6.4 %copy-start.5 = (f32[16,4,128]{2,1,0:T(4,128)}, f32[16,4,128]{2,1,0:T(4,128)S(1)}, u32[]{:S(2)}) copy-start(f32[16,4,128]{2,1,0:T(4,128)S(1)} %reshape.114) | copy-start | bytes 98308
  12.3 7.1 %copy-start.11 = (bf16[16,1024]{1,0:T(8,128)(2,1)S(1)}, bf16[16,1024]{1,0:T(8,128)(2,1)}, u32[]{:S(2)}) copy-start(bf16[16,1024]{1,0:T(8,128)(2,1)} %param.16) | copy-start | bytes 98308
  18.1 1.3 %collective-permute-start.1 = (bf16[16,512]{1,0:T(8,128)(2,1)S(1)}, bf16[16,512]{1,0:T(8,128)(2,1)S(1)}, u32[]{:S(2)}, u32[]{:S(2)}) collective-permute-start(bf16[16,512]{1,0:T(8,128)(2,1)S(1)} %bitcast.40), channel_id=1, source_target_pairs={{0,1},{1,0},{2,3},{3,2},{4,5},{5,4},{6,7},{7,6},{8,9},{9,8},{10,11... | collective-permute-start | bytes 49160 | tf_op jit(solution)/shard_map/ppermute | solution.py:11
  19.4 24.3 %copy-start.19 = (f32[1024]{0:T(1024)S(1)}, f32[1024]{0:T(1024)}, u32[]{:S(2)}) copy-start(f32[1024]{0:T(1024)} %param.28) | copy-start | bytes 12292
  19.8 23.6 %copy-start.7 = (bf16[16,1024]{1,0:T(8,128)(2,1)}, bf16[16,1024]{1,0:T(8,128)(2,1)S(1)}, u32[]{:S(2)}) copy-start(bf16[16,1024]{1,0:T(8,128)(2,1)S(1)} %fusion) | copy-start | bytes 98308
  19.8 24.4 %copy-start.2 = (bf16[1024,352]{0,1:T(8,128)(2,1)S(1)}, bf16[1024,352]{0,1:T(8,128)(2,1)}, u32[]{:S(2)}) copy-start(bf16[1024,352]{0,1:T(8,128)(2,1)} %param.29) | copy-start | bytes 2162692
  43.6 0.6 copy-start.12
  43.7 1.6 %copy-start.3 = (bf16[1024,352]{0,1:T(8,128)(2,1)S(1)}, bf16[1024,352]{0,1:T(8,128)(2,1)}, u32[]{:S(2)}) copy-start(bf16[1024,352]{0,1:T(8,128)(2,1)} %param.30) | copy-start | bytes 2162692
  45.3 2.9 %copy-start.4 = (f32[256,352]{0,1:T(8,128)S(1)}, f32[256,352]{0,1:T(8,128)}, u32[]{:S(2)}) copy-start(f32[256,352]{0,1:T(8,128)} %get-tuple-element.20) | copy-start | bytes 1081348
  45.8 1.7 %collective-permute-start.2 = (bf16[256,706]{0,1:T(8,128)(2,1)S(1)}, bf16[256,706]{0,1:T(8,128)(2,1)S(1)}, u32[]{:S(2)}, u32[]{:S(2)}) collective-permute-start(bf16[256,706]{0,1:T(8,128)(2,1)S(1)} %pad_maximum_fusion), channel_id=1, source_target_pairs={{0,1},{1,0},{2,3},{3,2},{4,5},{5,4},{6,7},{7,6},{8,9},{9,8},{10,11... | collective-permute-start | bytes 1084424 | tf_op jit(solution)/shard_map/ppermute | solution.py:11
  48.2 6.5 %copy-start.6 = (f32[16,4,128]{2,1,0:T(4,128)S(1)}, f32[16,4,128]{2,1,0:T(4,128)}, u32[]{:S(2)}) copy-start(f32[16,4,128]{2,1,0:T(4,128)} %copy-done.5) | copy-start | bytes 98308
  48.3 6.5 %copy-start.10 = (f32[16,4,128]{2,1,0:T(4,128)S(1)}, f32[16,4,128]{2,1,0:T(4,128)}, u32[]{:S(2)}) copy-start(f32[16,4,128]{2,1,0:T(4,128)} %copy-done.9) | copy-start | bytes 98308
  48.3 6.5 %copy-start.14 = (f32[16,4]{1,0:T(8,128)S(1)}, f32[16,4]{1,0:T(8,128)}, u32[]{:S(2)}) copy-start(f32[16,4]{1,0:T(8,128)} %copy-done.13) | copy-start | bytes 772
  50.8 19.4 %all-to-all-start.1 = ((bf16[16,16,1024]{2,1,0:T(8,128)(2,1)}), bf16[16,16,1024]{2,1,0:T(8,128)(2,1)S(1)}, u32[]{:S(2)}, u32[]{:S(2)}) async-start(bf16[16,16,1024]{2,1,0:T(8,128)(2,1)} %bitcast.4), calls=%async_computation.1 | async-start | bytes 1048576 | tf_op jit(solution)/shard_map/all_to_all | solution.py:107
  54.8 15.5 %copy-start.8 = (bf16[16,1024]{1,0:T(8,128)(2,1)S(1)}, bf16[16,1024]{1,0:T(8,128)(2,1)}, u32[]{:S(2)}) copy-start(bf16[16,1024]{1,0:T(8,128)(2,1)} %copy-done.7) | copy-start | bytes 98308

commit v2 on v1

v2 whole, which is shorter than its diff:
```python
import functools

import jax
import jax.numpy as jnp
from jax import lax
from jax.experimental import pallas as pl
from jax.experimental.pallas import tpu as pltpu
from jax.sharding import PartitionSpec as P

BF16 = jnp.bfloat16
F32 = jnp.float32
LANES = 128
W_PARTS = 4
IN_FLIGHT = 9
CELL_VMEM = 24 * 2**20
HBM = pl.BlockSpec(memory_space=pltpu.HBM)
VMEM = pl.BlockSpec(memory_space=pltpu.VMEM)
NT = (((1,), (1,)), ((), ()))


def shifted(x, axis, size, step):
    return lax.ppermute(x, axis, [(i, (i + step) % size) for i in range(size)])


def column_pieces(x, axis, size):
    if size != 2:
        return [lax.all_gather(x, axis, axis=1, tiled=True)]
    return [x, shifted(x, axis, size, 1)]


def in_hbm(x):
    return pltpu.with_memory_space_constraint(x, pltpu.HBM)


def piece_starts(refs, axis):
    if len(refs) == 1:
        return [0]
    me, width = lax.axis_index(axis), refs[0].shape[1]
    return [pl.multiple_of(me * width, LANES), pl.multiple_of((1 - me) * width, LANES)]


def load_kernel(count, *refs):
    sources, targets, sem = refs[:count], refs[count : 2 * count], refs[-1]
    copies = [pltpu.make_async_copy(a, b, sem.at[i]) for i, (a, b) in enumerate(zip(sources, targets))]
    for copy in copies:
        copy.start()
    for copy in copies:
        copy.wait()


def load(arrays):
    return pl.pallas_call(
        functools.partial(load_kernel, len(arrays)),
        name="load",
        out_shape=[pltpu.VMEM(x.shape, x.dtype) for x in arrays],
        in_specs=[HBM] * len(arrays),
        out_specs=[VMEM] * len(arrays),
        scratch_shapes=[pltpu.SemaphoreType.DMA((len(arrays),))],
        compiler_params=pltpu.CompilerParams(vmem_limit_bytes=4 * 2**20),
        cost_estimate=pl.CostEstimate(flops=2**28, bytes_accessed=2**18, transcendentals=0),
    )(*map(in_hbm, arrays))


def cell_kernel(pieces, *refs):
    partner_refs, refs = refs[: pieces - 1], refs[pieces - 1 :]
    (own, gain, wi, wf, normalizer, old_max_t, wq, wk, wv, wo, memory, *refs) = refs
    (mixed, new_normalizer, new_max_t, keep_out, admit_out, key_out, value_out, *refs) = refs
    (full, w_buf, m_buf, old_part, w_sem, m_sem) = refs
    rows, heads, dim = normalizer.shape
    blocks = m_buf.shape[0]
    block_rows = rows // blocks
    depth = w_buf.shape[1] // W_PARTS

    w_copies = [
        [
            pltpu.make_async_copy(
                w.at[pl.ds(p * depth, depth)], w_buf.at[i, pl.ds(p * depth, depth)], w_sem.at[i, p]
            )
            for p in range(W_PARTS)
        ]
        for i, w in enumerate([wq, wk, wv, wo])
    ]
    m_copies = [
        pltpu.make_async_copy(memory.at[pl.ds(i * block_rows, block_rows)], m_buf.at[i], m_sem.at[i])
        for i in range(blocks)
    ]
    stream = w_copies[0] + m_copies + w_copies[1] + w_copies[2] + w_copies[3]
    for copy in stream[:IN_FLIGHT]:
        copy.start()
    waiting = list(stream)
    later = list(stream[IN_FLIGHT:])

    def arrive():
        waiting.pop(0).wait()
        if later:
            later.pop(0).start()

    token_refs = [own, *partner_refs]
    for ref, start in zip(token_refs, piece_starts(token_refs, "tp")):
        full[:, pl.ds(start, ref.shape[1])] = ref[...].astype(F32)
    x = full[...]
    scale = lax.rsqrt(jnp.mean(x * x, axis=1, keepdims=True) + 1e-06)
    normed = (x * scale * gain[...]).astype(BF16)

    def nt(a, b):
        return lax.dot_general(a, b, NT, preferred_element_type=F32)

    all_heads = wi.shape[0]
    me = lax.axis_index("tp")

    def own_heads(x):
        out = x[:heads]
        for i in range(1, all_heads // heads):
            out = jnp.where(me == i, x[i * heads : (i + 1) * heads], out)
        return out

    igate = own_heads(nt(wi[...], normed))
    lforget = jax.nn.log_sigmoid(own_heads(nt(wf[...], normed)))
    old_max = old_max_t[...]
    max_t = jnp.maximum(lforget + old_max, igate)
    new_max_t[...] = max_t
    keep = jnp.exp(lforget + old_max - max_t).T
    admit = jnp.exp(igate - max_t).T
    floor = jnp.exp(-max_t).T
    keep_out[...] = keep
    admit_out[...] = admit

    def project(i):
        total = None
        for p in range(W_PARTS):
            arrive()
            part = jnp.dot(
                normed[:, p * depth : (p + 1) * depth],
                w_buf[i, p * depth : (p + 1) * depth, :],
                preferred_element_type=F32,
            )
            total = part if total is None else total + part
        return total

    def head(x, h):
        return x[:, h * dim : (h + 1) * dim]

    queries = project(0) * dim ** (-0.5)
    columns = [head(queries, h).T for h in range(heads)]
    for block in range(blocks):
        arrive()
        for r in range(block_rows):
            b = block * block_rows + r
            for h in range(heads):
                part = jnp.sum(m_buf[block, r, h] * columns[h][:, b : b + 1], axis=0, keepdims=True)
                old_part[h, b : b + 1, :] = part

    keys = project(1)
    key_out[...] = keys
    scales = []
    for h in range(heads):
        q, k = head(queries, h), head(keys, h)
        kw, aw = keep[:, h : h + 1], admit[:, h : h + 1]
        norm = kw * normalizer[:, h, :] + aw * k
        new_normalizer[:, h, :] = norm
        query_key = jnp.sum(q * k, axis=1, keepdims=True)
        denominator = jnp.sum(q * norm, axis=1, keepdims=True)
        scales.append((aw * query_key, jnp.maximum(jnp.abs(denominator), floor[:, h : h + 1])))
    values = project(2)
    value_out[...] = values
    normalised = []
    for h in range(heads):
        weight, divisor = scales[h]
        numerator = keep[:, h : h + 1] * old_part[h] + weight * head(values, h)
        cell_out = numerator / divisor
        centered = cell_out - jnp.mean(cell_out, axis=1, keepdims=True)
        variance = jnp.mean(centered * centered, axis=1, keepdims=True)
        normalised.append(centered * lax.rsqrt(variance + 1e-05))
    outgate = jax.nn.sigmoid(project(3))
    for h in range(heads):
        mixed[:, h * dim : (h + 1) * dim] = (head(outgate, h) * normalised[h]).astype(BF16)


def run_cell(token_pieces, gain, wi, wf, normalizer, old_max, weights, memory):
    rows, heads, dim = normalizer.shape
    depth, inner = weights[0].shape
    blocks = 8 if rows % 8 == 0 else 1
    own, *partners = token_pieces
    flops = 2 * rows * depth * inner * 4
    return pl.pallas_call(
        functools.partial(cell_kernel, len(token_pieces)),
        name="cell",
        out_shape=[
            pltpu.VMEM((rows, inner), BF16),
            jax.ShapeDtypeStruct((rows, heads, dim), F32),
            jax.ShapeDtypeStruct((heads, rows), F32),
            pltpu.VMEM((rows, heads), F32),
            pltpu.VMEM((rows, heads), F32),
            pltpu.VMEM((rows, inner), F32),
            pltpu.VMEM((rows, inner), F32),
        ],
        in_specs=[VMEM] * (len(partners) + 6) + [HBM] * 5,
        out_specs=[VMEM] * 7,
        scratch_shapes=[
            pltpu.VMEM((rows, depth), F32),
            pltpu.VMEM((4, depth, inner), BF16),
            pltpu.VMEM((blocks, rows // blocks, heads, dim, dim), F32),
            pltpu.VMEM((heads, rows, dim), F32),
            pltpu.SemaphoreType.DMA((4, W_PARTS)),
            pltpu.SemaphoreType.DMA((blocks,)),
        ],
        compiler_params=pltpu.CompilerParams(vmem_limit_bytes=CELL_VMEM),
        cost_estimate=pl.CostEstimate(flops=flops * 64, bytes_accessed=13 * 2**20, transcendentals=0),
    )(*partners, *load([own, gain, wi, wf, normalizer, old_max.T]), *map(in_hbm, [*weights, memory]))


def out_kernel(pieces, *refs):
    mixed_refs, (tokens, w_output, resid, copies) = refs[:pieces], refs[pieces:]
    total = tokens[...].astype(F32)
    for ref, start in zip(mixed_refs, piece_starts(mixed_refs, "tp")):
        weight = w_output[pl.ds(start, ref.shape[1]), :]
        total = total + jnp.dot(ref[...], weight, preferred_element_type=F32)
    out = total.astype(BF16)
    resid[...] = out
    for i in range(copies.shape[0]):
        copies[i] = out


def run_out(mixed_pieces, tokens, w_output, kv):
    rows, width = tokens.shape
    return pl.pallas_call(
        functools.partial(out_kernel, len(mixed_pieces)),
        name="out_projection",
        out_shape=[jax.ShapeDtypeStruct((rows, width), BF16), jax.ShapeDtypeStruct((kv, rows, width), BF16)],
        in_specs=[VMEM] * (len(mixed_pieces) + 2),
        out_specs=[VMEM, VMEM],
        compiler_params=pltpu.CompilerParams(vmem_limit_bytes=24 * 2**20),
        cost_estimate=pl.CostEstimate(
            flops=2 * rows * w_output.size, bytes_accessed=2 * w_output.size, transcendentals=0
        ),
    )(*mixed_pieces, tokens, w_output)


def up_kernel(rows_ref, gain, w_gate, w_up, own, sent):
    hidden = w_gate.shape[0]
    half = own.shape[1] // 2
    x = rows_ref[...].astype(F32)
    squares = jnp.sum(x * x, axis=1, keepdims=True)
    ffn_in = (x * gain[...]).astype(BF16)
    own[...] = jnp.zeros_like(own)
    for weight, first in [(w_gate, 0), (w_up, half)]:
        own[:, first : first + hidden] = lax.dot_general(ffn_in, weight[...], NT, preferred_element_type=F32)
    lane = lax.broadcasted_iota(jnp.int32, (x.shape[0], LANES), 1)
    high = squares.astype(BF16).astype(F32)
    first = hidden // LANES * LANES
    tile = own[:, first : first + LANES]
    spot = hidden - first
    own[:, first : first + LANES] = jnp.where(lane == spot, squares, tile)
    sent[...] = own[...].astype(BF16)
    tile = jnp.where(lane == spot, high, jnp.where(lane == spot + 1, squares - high, tile))
    sent[:, first : first + LANES] = tile.astype(BF16)


def run_up(every_row, gain, w_gate, w_up):
    rows, depth = every_row.shape
    hidden = w_gate.shape[1]
    half = (hidden + 2 + LANES - 1) // LANES * LANES
    return pl.pallas_call(
        up_kernel,
        name="gate_up",
        out_shape=[jax.ShapeDtypeStruct((rows, 2 * half), F32), jax.ShapeDtypeStruct((rows, 2 * half), BF16)],
        in_specs=[VMEM] * 4,
        out_specs=[VMEM, VMEM],
        compiler_params=pltpu.CompilerParams(vmem_limit_bytes=24 * 2**20),
        cost_estimate=pl.CostEstimate(flops=4 * rows * depth * hidden, bytes_accessed=4 * 2**20, transcendentals=0),
    )(every_row, gain, w_gate.T, w_up.T)


def down_kernel(others, channels, own, *refs):
    other_refs, (w_down, out) = refs[:others], refs[others:]
    hidden = w_down.shape[0]
    half = own.shape[1] // 2
    gate, up = own[:, :half], own[:, half:]
    squares = gate[:, hidden : hidden + 1]
    for ref in other_refs:
        theirs = ref[...].astype(F32)
        gate, up = gate + theirs[:, :half], up + theirs[:, half:]
        squares = squares + theirs[:, hidden : hidden + 1] + theirs[:, hidden + 1 : hidden + 2]
    scale = lax.rsqrt(squares / channels + 1e-06)
    gate = scale * gate[:, :hidden]
    act = (gate * jax.nn.sigmoid(gate) * (scale * up[:, :hidden])).astype(BF16)
    out[...] = jnp.dot(act, w_down[...], preferred_element_type=F32).astype(BF16)


def run_down(own, others, w_down, channels):
    rows = own.shape[0]
    hidden, width = w_down.shape
    return pl.pallas_call(
        functools.partial(down_kernel, len(others), channels),
        name="down",
        out_shape=jax.ShapeDtypeStruct((rows, width), BF16),
        in_specs=[VMEM] * (2 + len(others)),
        out_specs=VMEM,
        compiler_params=pltpu.CompilerParams(vmem_limit_bytes=24 * 2**20),
        cost_estimate=pl.CostEstimate(flops=2 * rows * width * hidden, bytes_accessed=2 * 2**20, transcendentals=0),
    )(own, *others, w_down)


def make(kv, tp):
    def per_device(
        tokens,
        norm_gain,
        w_query,
        w_key,
        w_value,
        w_outgate,
        w_input_gate,
        w_forget_gate,
        memory,
        normalizer,
        memory_max,
        w_output,
        ffn_gain,
        w_gate,
        w_up,
        w_down,
    ):
        rows, own_channels = tokens.shape
        heads, head_dim = memory.shape[1], memory.shape[2]
        pieces = column_pieces(tokens, "tp", tp)
        mixed, new_normalizer, new_max_t, keep, admit, keys, values = run_cell(
            pieces,
            norm_gain[None],
            w_input_gate.T,
            w_forget_gate.T,
            normalizer,
            memory_max,
            [w_query, w_key, w_value, w_outgate],
            memory,
        )
        pieces = column_pieces(mixed, "tp", tp)
        resid, copies = run_out(pieces, tokens, w_output, kv)
        every_row = lax.all_to_all(copies, "kv", 0, 0).reshape(kv * rows, own_channels)
        by_head = (rows, heads, head_dim)
        keys, values = keys.reshape(by_head), values.reshape(by_head)
        new_memory = keep[..., None, None] * memory + admit[..., None, None] * (
            keys[..., :, None] * values[..., None, :]
        )

        own, sent = run_up(every_row, ffn_gain[None], w_gate, w_up)
        others = [shifted(sent, "tp", tp, step) for step in range(1, tp)]
        down_part = run_down(own, others, w_down, own_channels * tp)
        pieces = lax.all_to_all(down_part.reshape(kv, rows, own_channels), "kv", 0, 0)
        down_out = jnp.sum(pieces.astype(F32), axis=0)
        result = (resid.astype(F32) + down_out).astype(BF16)
        return (result, new_memory, new_normalizer, new_max_t.T)

    return per_device


def solution(mesh):
    placed = (
        P("kv", "tp"),
        P(),
        P(None, "tp"),
        P(None, "tp"),
        P(None, "tp"),
        P(None, "tp"),
        P(),
        P(),
        P("kv", "tp", None, None),
        P("kv", "tp", None),
        P("kv", "tp"),
        P(None, "tp"),
        P("tp"),
        P("tp", "kv"),
        P("tp", "kv"),
        P("kv", "tp"),
    )
    return jax.shard_map(
        make(mesh.shape["kv"], mesh.shape["tp"]),
        mesh=mesh,
        in_specs=placed,
        out_specs=(P("kv", "tp"), P("kv", "tp", None, None), P("kv", "tp", None), P("kv", "tp")),
        check_vma=False,
    )
```

time: 71.4 us -> 58.6 us (0.82)
  matrix products: 16.4 us -> 0 us
  Pallas kernels: 0 us -> 10.3 us
  other arithmetic: 9.29 us -> 5.29 us
  local copies, waits for them, and re-layouts: 2.66 us -> 0.06 us
    dot_general x11 -> x0, matrix products: 16.4 us -> none  [the longest x6 6.7 us: project(): return jnp.dot(normed, weight, preferred_element_type=F32)]
    pallas_call x0 -> x5, Pallas kernels: none -> 10.3 us  [the longest x1 6.84 us: run_cell(): pl.pallas_call(functools.partial(cell_kernel, len(token_pieces)), name='c...]
    reduce_sum x4 -> x0, local copies, waits for them, and re-layouts: 1.59 us -> none  [the longest x2 1.43 us: per_device(): squares = jnp.sum(every_f * every_f, axis=-1, keepdims=True)]
    reduce_sum x6 -> x0, other arithmetic: 1.41 us -> none  [the longest x1 0.72 us: per_device(): query_key = jnp.sum(queries * key_vec, axis=-1)]
    convert_element_type x5 -> x0, other arithmetic: 1.04 us -> none  [the longest x1 0.78 us: per_device(): normed = (full_rows * row_scale * norm_gain).astype(BF16)]
    select_n x2 -> x0, other arithmetic: 0.77 us -> none  [gather_columns(): jnp.where(first, x, other)]
  transfers between devices with their start and end apart: 4 -> 4, of which waited for: 4 -> 4; matrix products, arithmetic and copies ran while one was open for 8% -> 8% of each run, Pallas kernels for 0% -> 2%
where the time goes in v2:
time: 58.6 us; the launch traced here: 58.3 us
  blocking collectives  23.4 us (40%)
  waiting for transfers between devices  13.5 us (23%)
  Pallas kernels  10.3 us (18%)
  other arithmetic  5.29 us (9%)
  starting transfers between devices  5 us (9%)
  between operations  0.72 us (1%)
    all_to_all x1, blocking collectives, per_device(): lax.all_to_all(copies, 'kv', 0, 0).reshape(kv * rows, own_channels)  23.4 us
    all_to_all x1, waiting for transfers between devices, per_device(): lax.all_to_all(down_part.reshape(kv, rows, own_channels), 'kv', 0, 0)  10.8 us
    pallas_call x1, Pallas kernels, run_cell(): pl.pallas_call(functools.partial(cell_kernel, len(token_pieces)), name='c...  6.84 us
    add x1, other arithmetic, per_device(): keep[..., None, None] * memory  4.59 us
    all_to_all x1, starting transfers between devices, per_device(): lax.all_to_all(down_part.reshape(kv, rows, own_channels), 'kv', 0, 0)  3.95 us
    ppermute x3, waiting for transfers between devices, shifted(): return lax.ppermute(x, axis, [(i, (i + step) % size) for i in range(size)])  2.74 us
    pallas_call x1, Pallas kernels, run_down(): pl.pallas_call(functools.partial(down_kernel, len(others), channels), nam...  1.43 us
  transfers between devices with their start and end apart: 4, of which 4 were waited for; matrix products, arithmetic and copies ran while one was open for 8% of the time, Pallas kernels for 2%

profile of v2, /device:TPU:0, one launch (start us, length us, event | category | flops | bytes accessed | tf_op | source)
XLA Modules:
  0.0 58.3 jit_solution(7628820449532856580)
XLA Ops:
  0.6 0.6 collective-permute-start
  1.2 0.9 %load.1 = (bf16[16,1024]{1,0:T(8,128)(2,1)S(1)}, f32[1,2048]{1,0:T(1,128)S(1)}, bf16[8,2048]{1,0:T(8,128)(2,1)S(1)}, bf16[8,2048]{1,0:T(8,128)(2,1)S(1)}, f32[16...) custom-call(bf16[16,1024]{1,0:T(8,128)(2,1)} %refs_2_.1, f32[1,2048]{1,0:T(1,128)} %bitcast.16, bf16[8,2048]{1,0:T(8,128)(2,1)} %bitcast.14, ...), custom_call_target="tpu_custom_call" | custom-call | flops 268435456 | bytes 262144 | tf_op jit(solution)/shard_map/load/pallas_call | solution.py:52
  2.1 0.2 collective-permute-done.refs_0_
  2.3 0.0 copy-start
  2.3 0.0 copy-start.4
  2.3 0.0 copy-start.2
  2.3 0.0 copy-start.3
  2.3 0.0 copy-start.5
  2.3 6.8 %cell.1 = (bf16[16,512]{1,0:T(8,128)(2,1)S(1)}, f32[16,4,128]{2,1,0:T(4,128)}, f32[4,16]{1,0:T(4,128)}, f32[16,4]{1,0:T(8,128)S(1)}, f32[16,4]{1,0:T(8,128)S(1)}...) custom-call(bf16[16,1024]{1,0:T(8,128)(2,1)S(1)} %collective-permute-done.refs_0_, ...), custom_call_target="tpu_custom_call" | custom-call | flops 8589934592 | bytes 13631488 | tf_op jit(solution)/shard_map/cell/pallas_call | solution.py:185
  9.1 0.0 copy-start.1
  9.1 0.4 collective-permute-start.1
  9.6 0.8 %collective-permute-done.1.refs_1_ = bf16[16,512]{1,0:T(8,128)(2,1)S(1)} collective-permute-done((bf16[16,512]{1,0:T(8,128)(2,1)S(1)}, bf16[16,512]{1,0:T(8,128)(2,1)S(1)}, u32[]{:S(2)}, u32[]{:S(2)}) %collective-permute-start.1) | collective-permute-done | bytes 16416 | tf_op jit(solution)/shard_map/ppermute | solution.py:22
  10.4 0.0 copy-done
  10.4 0.0 copy-done.4
  10.4 0.4 out_projection.1
  10.8 23.4 %all_to_all.10 = bf16[16,16,1024]{2,1,0:T(8,128)(2,1)S(1)} all-to-all(bf16[16,16,1024]{2,1,0:T(8,128)(2,1)S(1)} %get-tuple-element.29), channel_id=1, replica_groups=mesh['kv'=16,'tp'=2] {'kv'}, dimensions={0} | all-to-all | bytes 1048576 | tf_op jit(solution)/shard_map/all_to_all | solution.py:338
  34.2 0.0 copy-done.2
  34.2 0.0 copy-done.3
  34.2 0.0 copy-done.5
  34.2 0.8 %gate_up.1 = (f32[256,768]{1,0:T(8,128)S(1)}, bf16[256,768]{1,0:T(8,128)(2,1)S(1)}) custom-call(bf16[256,1024]{1,0:T(8,128)(2,1)S(1)} %bitcast.10, f32[1,1024]{1,0:T(1,128)S(1)} %bitcast.13, bf16[352,1024]{1,0:T(8,128)(2,1)S(1)} %bitcast.11, bf16[352,1024]{1,0:T(8,128)(2,1)S(1)} %bitcast.12), custom_call_target="tpu_custom_call" | custom-call | flops 369098752 | bytes 4194304 | tf_op jit(solution)/shard_map/gate_up/pallas_call | solution.py:263
  35.0 0.1 collective-permute-start.2
  35.1 1.7 %collective-permute-done.2.refs_0_ = bf16[256,768]{1,0:T(8,128)(2,1)S(1)} collective-permute-done((bf16[256,768]{1,0:T(8,128)(2,1)S(1)}, bf16[256,768]{1,0:T(8,128)(2,1)S(1)}, u32[]{:S(2)}, u32[]{:S(2)}) %collective-permute-start.2) | collective-permute-done | bytes 393248 | tf_op jit(solution)/shard_map/ppermute | solution.py:22
  36.8 0.0 copy-done.1
  36.8 1.4 %down.1 = bf16[256,1024]{1,0:T(8,128)(2,1)} custom-call(f32[256,768]{1,0:T(8,128)S(1)} %get-tuple-element.30.own, bf16[256,768]{1,0:T(8,128)(2,1)S(1)} %collective-permute-done.2.refs_0_, bf16[352,1024]{1,0:T(8,128)(2,1)S(1)} %copy-done.1), custom_call_target="tpu_custom_call" | custom-call | flops 184549376 | bytes 2097152 | tf_op jit(solution)/shard_map/down/pallas_call | solution.py:293
  38.2 3.9 %all-to-all-start.1 = ((bf16[16,16,1024]{2,1,0:T(8,128)(2,1)}), bf16[16,16,1024]{2,1,0:T(8,128)(2,1)S(1)}, u32[]{:S(2)}, u32[]{:S(2)}) async-start(bf16[16,16,1024]{2,1,0:T(8,128)(2,1)} %bitcast.8), calls=%async_computation.1 | async-start | bytes 1048576 | tf_op jit(solution)/shard_map/all_to_all | solution.py:348
  42.2 4.6 %multiply_add_fusion = f32[16,4,128,128]{3,2,1,0:T(8,128)} fusion(f32[16,4,128,128]{3,2,1,0:T(8,128)} %refs_11_.1, f32[16,4,128]{2,1,0:T(4,128)S(1)} %mul.38, f32[16,4,128]{2,1,0:T(4,128)S(1)} %mul.36, f32[16,4]{1,0:T(8,128)S(1)} %get-tuple-element.33, f32[16,4]{1,0:T(8,128)S(1)} %get-tuple-element.32), kind=kLoop, calls=%fused_computation | loop fusion | flops 4194304 | bytes 8454656 | tf_op jit(solution)/shard_map/add | solution.py:341
  46.8 10.8 %all-to-all-done.1 = bf16[16,16,1024]{2,1,0:T(8,128)(2,1)S(1)} async-done(((bf16[16,16,1024]{2,1,0:T(8,128)(2,1)}), bf16[16,16,1024]{2,1,0:T(8,128)(2,1)S(1)}, u32[]{:S(2)}, u32[]{:S(2)}) %all-to-all-start.1) | async-done | bytes 524320 | tf_op jit(solution)/shard_map/all_to_all | solution.py:348
  57.6 0.1 convert_reduce_fusion
  57.7 0.6 %add_convert_fusion = bf16[16,1024]{1,0:T(8,128)(2,1)} fusion(f32[16,1024]{1,0:T(8,128)S(1)} %convert_reduce_fusion, bf16[16,1024]{1,0:T(8,128)(2,1)S(1)} %get-tuple-element.28), kind=kLoop, calls=%fused_computation.2 | loop fusion | flops 49152 | bytes 131072 | tf_op jit(solution)/shard_map/convert_element_type | solution.py:350
  (2 shorter events, 0.0 us)
Async XLA Ops:
  0.6 1.6 %collective-permute-start = (bf16[16,1024]{1,0:T(8,128)(2,1)}, bf16[16,1024]{1,0:T(8,128)(2,1)S(1)}, u32[]{:S(2)}, u32[]{:S(2)}) collective-permute-start(bf16[16,1024]{1,0:T(8,128)(2,1)} %refs_2_.1), channel_id=1, source_target_pairs={{0,1},{1,0},{2,3},{3,2},{4,5},{5,4},{6,7},{7,6},{8,9},{9,8},{10,11... | collective-permute-start | bytes 98312 | tf_op jit(solution)/shard_map/ppermute | solution.py:22
  2.3 8.1 %copy-start = (bf16[1024,1024]{1,0:T(8,128)(2,1)S(1)}, bf16[1024,1024]{1,0:T(8,128)(2,1)}, u32[]{:S(2)}) copy-start(bf16[1024,1024]{1,0:T(8,128)(2,1)} %refs_3_.1) | copy-start | bytes 6291460
  2.3 8.1 %copy-start.4 = (bf16[16,1024]{1,0:T(8,128)(2,1)S(1)}, bf16[16,1024]{1,0:T(8,128)(2,1)}, u32[]{:S(2)}) copy-start(bf16[16,1024]{1,0:T(8,128)(2,1)} %refs_2_.1) | copy-start | bytes 98308
  2.3 32.0 %copy-start.2 = (bf16[1024,352]{0,1:T(8,128)(2,1)S(1)}, bf16[1024,352]{0,1:T(8,128)(2,1)}, u32[]{:S(2)}) copy-start(bf16[1024,352]{0,1:T(8,128)(2,1)} %param.29) | copy-start | bytes 2162692
  2.3 32.0 %copy-start.3 = (bf16[1024,352]{0,1:T(8,128)(2,1)S(1)}, bf16[1024,352]{0,1:T(8,128)(2,1)}, u32[]{:S(2)}) copy-start(bf16[1024,352]{0,1:T(8,128)(2,1)} %param.30) | copy-start | bytes 2162692
  2.3 32.0 %copy-start.5 = (f32[1024]{0:T(1024)S(1)}, f32[1024]{0:T(1024)}, u32[]{:S(2)}) copy-start(f32[1024]{0:T(1024)} %param.28) | copy-start | bytes 12292
  9.1 27.7 %copy-start.1 = (bf16[352,1024]{1,0:T(8,128)(2,1)S(1)}, bf16[352,1024]{1,0:T(8,128)(2,1)}, u32[]{:S(2)}) copy-start(bf16[352,1024]{1,0:T(8,128)(2,1)} %refs_1_.1) | copy-start | bytes 2162692
  9.1 1.3 %collective-permute-start.1 = (bf16[16,512]{1,0:T(8,128)(2,1)S(1)}, bf16[16,512]{1,0:T(8,128)(2,1)S(1)}, u32[]{:S(2)}, u32[]{:S(2)}) collective-permute-start(bf16[16,512]{1,0:T(8,128)(2,1)S(1)} %get-tuple-element.27.refs_0_), channel_id=1, source_target_pairs={{0,1},{1,0},{2,3},{3,2},{4,5},{5,4},{6,7},{7,6},{8,9},{9,8},{10,11... | collective-permute-start | bytes 49160 | tf_op jit(solution)/shard_map/ppermute | solution.py:22
  35.0 1.8 %collective-permute-start.2 = (bf16[256,768]{1,0:T(8,128)(2,1)S(1)}, bf16[256,768]{1,0:T(8,128)(2,1)S(1)}, u32[]{:S(2)}, u32[]{:S(2)}) collective-permute-start(bf16[256,768]{1,0:T(8,128)(2,1)S(1)} %get-tuple-element.31), channel_id=1, source_target_pairs={{0,1},{1,0},{2,3},{3,2},{4,5},{5,4},{6,7},{7,6},{8,9},{9,8},{10,11... | collective-permute-start | bytes 1179656 | tf_op jit(solution)/shard_map/ppermute | solution.py:22
  38.2 19.3 %all-to-all-start.1 = ((bf16[16,16,1024]{2,1,0:T(8,128)(2,1)}), bf16[16,16,1024]{2,1,0:T(8,128)(2,1)S(1)}, u32[]{:S(2)}, u32[]{:S(2)}) async-start(bf16[16,16,1024]{2,1,0:T(8,128)(2,1)} %bitcast.8), calls=%async_computation.1 | async-start | bytes 1048576 | tf_op jit(solution)/shard_map/all_to_all | solution.py:348

commit v3 on v2

--- a/solution.py
+++ b/solution.py
@@ -10,9 +10,7 @@
 BF16 = jnp.bfloat16
 F32 = jnp.float32
 LANES = 128
-W_PARTS = 4
-IN_FLIGHT = 9
-CELL_VMEM = 24 * 2**20
+COVER = 2**36
 HBM = pl.BlockSpec(memory_space=pltpu.HBM)
 VMEM = pl.BlockSpec(memory_space=pltpu.VMEM)
 NT = (((1,), (1,)), ((), ()))
@@ -26,6 +24,10 @@
     if size != 2:
         return [lax.all_gather(x, axis, axis=1, tiled=True)]
     return [x, shifted(x, axis, size, 1)]
+
+
+def in_vmem(x):
+    return pltpu.with_memory_space_constraint(x, pltpu.VMEM)
 
 
 def in_hbm(x):
@@ -57,50 +59,22 @@
         out_specs=[VMEM] * len(arrays),
         scratch_shapes=[pltpu.SemaphoreType.DMA((len(arrays),))],
         compiler_params=pltpu.CompilerParams(vmem_limit_bytes=4 * 2**20),
-        cost_estimate=pl.CostEstimate(flops=2**28, bytes_accessed=2**18, transcendentals=0),
+        cost_estimate=pl.CostEstimate(flops=COVER, bytes_accessed=2**18, transcendentals=0),
     )(*map(in_hbm, arrays))
 
 
-def cell_kernel(pieces, *refs):
-    partner_refs, refs = refs[: pieces - 1], refs[pieces - 1 :]
-    (own, gain, wi, wf, normalizer, old_max_t, wq, wk, wv, wo, memory, *refs) = refs
-    (mixed, new_normalizer, new_max_t, keep_out, admit_out, key_out, value_out, *refs) = refs
-    (full, w_buf, m_buf, old_part, w_sem, m_sem) = refs
-    rows, heads, dim = normalizer.shape
-    blocks = m_buf.shape[0]
-    block_rows = rows // blocks
-    depth = w_buf.shape[1] // W_PARTS
-
-    w_copies = [
-        [
-            pltpu.make_async_copy(
-                w.at[pl.ds(p * depth, depth)], w_buf.at[i, pl.ds(p * depth, depth)], w_sem.at[i, p]
-            )
-            for p in range(W_PARTS)
-        ]
-        for i, w in enumerate([wq, wk, wv, wo])
-    ]
-    m_copies = [
-        pltpu.make_async_copy(memory.at[pl.ds(i * block_rows, block_rows)], m_buf.at[i], m_sem.at[i])
-        for i in range(blocks)
-    ]
-    stream = w_copies[0] + m_copies + w_copies[1] + w_copies[2] + w_copies[3]
-    for copy in stream[:IN_FLIGHT]:
-        copy.start()
-    waiting = list(stream)
-    later = list(stream[IN_FLIGHT:])
-
-    def arrive():
-        waiting.pop(0).wait()
-        if later:
-            later.pop(0).start()
-
-    token_refs = [own, *partner_refs]
+def read_kernel(pieces, *refs):
+    token_refs, refs = refs[:pieces], refs[pieces:]
+    (gain, wi, wf, old_max_t, wq, memory, *refs) = refs
+    (normed_out, query_out, old_part, keep_out, admit_out, floor_out, new_max_t, full) = refs
+    rows, heads, dim = memory.shape[:3]
+
     for ref, start in zip(token_refs, piece_starts(token_refs, "tp")):
         full[:, pl.ds(start, ref.shape[1])] = ref[...].astype(F32)
     x = full[...]
     scale = lax.rsqrt(jnp.mean(x * x, axis=1, keepdims=True) + 1e-06)
     normed = (x * scale * gain[...]).astype(BF16)
+    normed_out[...] = normed
 
     def nt(a, b):
         return lax.dot_general(a, b, NT, preferred_element_type=F32)
@@ -114,99 +88,95 @@
             out = jnp.where(me == i, x[i * heads : (i + 1) * heads], out)
         return out
 
+    queries = jnp.dot(normed, wq[...], preferred_element_type=F32) * dim ** (-0.5)
+    query_out[...] = queries
     igate = own_heads(nt(wi[...], normed))
     lforget = jax.nn.log_sigmoid(own_heads(nt(wf[...], normed)))
     old_max = old_max_t[...]
     max_t = jnp.maximum(lforget + old_max, igate)
     new_max_t[...] = max_t
-    keep = jnp.exp(lforget + old_max - max_t).T
-    admit = jnp.exp(igate - max_t).T
-    floor = jnp.exp(-max_t).T
-    keep_out[...] = keep
-    admit_out[...] = admit
-
-    def project(i):
-        total = None
-        for p in range(W_PARTS):
-            arrive()
-            part = jnp.dot(
-                normed[:, p * depth : (p + 1) * depth],
-                w_buf[i, p * depth : (p + 1) * depth, :],
-                preferred_element_type=F32,
-            )
-            total = part if total is None else total + part
-        return total
+    keep_out[...] = jnp.exp(lforget + old_max - max_t).T
+    admit_out[...] = jnp.exp(igate - max_t).T
+    floor_out[...] = jnp.exp(-max_t).T
+
+    columns = [queries[:, h * dim : (h + 1) * dim].T for h in range(heads)]
+    for b in range(rows):
+        for h in range(heads):
+            part = jnp.sum(memory[b, h] * columns[h][:, b : b + 1], axis=0, keepdims=True)
+            old_part[h, b : b + 1, :] = part
+
+
+def run_read(token_pieces, gain, wi, wf, old_max_t, wq, memory):
+    rows, heads, dim = memory.shape[:3]
+    depth, inner = wq.shape
+    flops = 2 * rows * depth * inner
+    return pl.pallas_call(
+        functools.partial(read_kernel, len(token_pieces)),
+        name="read",
+        out_shape=[
+            pltpu.VMEM((rows, depth), BF16),
+            pltpu.VMEM((rows, inner), F32),
+            pltpu.VMEM((heads, rows, dim), F32),
+            pltpu.VMEM((rows, heads), F32),
+            pltpu.VMEM((rows, heads), F32),
+            pltpu.VMEM((rows, heads), F32),
+            jax.ShapeDtypeStruct((heads, rows), F32),
+        ],
+        in_specs=[VMEM] * (len(token_pieces) + 6),
+        out_specs=[VMEM] * 7,
+        scratch_shapes=[pltpu.VMEM((rows, depth), F32)],
+        compiler_params=pltpu.CompilerParams(vmem_limit_bytes=16 * 2**20),
+        cost_estimate=pl.CostEstimate(flops=flops * 32, bytes_accessed=6 * 2**20, transcendentals=0),
+    )(*token_pieces, gain, wi, wf, old_max_t, *map(in_vmem, [wq, memory]))
+
+
+def mix_kernel(*refs):
+    (normed, query, old_part, keep, admit, floor, normalizer, wk, wv, wo, *refs) = refs
+    (mixed, new_normalizer, key_out, value_out) = refs
+    rows, heads, dim = normalizer.shape
 
     def head(x, h):
         return x[:, h * dim : (h + 1) * dim]
 
-    queries = project(0) * dim ** (-0.5)
-    columns = [head(queries, h).T for h in range(heads)]
-    for block in range(blocks):
-        arrive()
-        for r in range(block_rows):
-            b = block * block_rows + r
-            for h in range(heads):
-                part = jnp.sum(m_buf[block, r, h] * columns[h][:, b : b + 1], axis=0, keepdims=True)
-                old_part[h, b : b + 1, :] = part
-
-    keys = project(1)
+    x = normed[...]
+    keys = jnp.dot(x, wk[...], preferred_element_type=F32)
+    values = jnp.dot(x, wv[...], preferred_element_type=F32)
+    outgate = jax.nn.sigmoid(jnp.dot(x, wo[...], preferred_element_type=F32))
     key_out[...] = keys
-    scales = []
+    value_out[...] = values
     for h in range(heads):
-        q, k = head(queries, h), head(keys, h)
+        q, k, v = head(query[...], h), head(keys, h), head(values, h)
         kw, aw = keep[:, h : h + 1], admit[:, h : h + 1]
         norm = kw * normalizer[:, h, :] + aw * k
         new_normalizer[:, h, :] = norm
         query_key = jnp.sum(q * k, axis=1, keepdims=True)
         denominator = jnp.sum(q * norm, axis=1, keepdims=True)
-        scales.append((aw * query_key, jnp.maximum(jnp.abs(denominator), floor[:, h : h + 1])))
-    values = project(2)
-    value_out[...] = values
-    normalised = []
-    for h in range(heads):
-        weight, divisor = scales[h]
-        numerator = keep[:, h : h + 1] * old_part[h] + weight * head(values, h)
-        cell_out = numerator / divisor
+        numerator = kw * old_part[h] + (aw * query_key) * v
+        cell_out = numerator / jnp.maximum(jnp.abs(denominator), floor[:, h : h + 1])
         centered = cell_out - jnp.mean(cell_out, axis=1, keepdims=True)
         variance = jnp.mean(centered * centered, axis=1, keepdims=True)
-        normalised.append(centered * lax.rsqrt(variance + 1e-05))
-    outgate = jax.nn.sigmoid(project(3))
-    for h in range(heads):
-        mixed[:, h * dim : (h + 1) * dim] = (head(outgate, h) * normalised[h]).astype(BF16)
-
-
-def run_cell(token_pieces, gain, wi, wf, normalizer, old_max, weights, memory):
+        gated = head(outgate, h) * centered * lax.rsqrt(variance + 1e-05)
+        mixed[:, h * dim : (h + 1) * dim] = gated.astype(BF16)
+
+
+def run_mix(normed, query, old_part, keep, admit, floor, normalizer, weights):
     rows, heads, dim = normalizer.shape
     depth, inner = weights[0].shape
-    blocks = 8 if rows % 8 == 0 else 1
-    own, *partners = token_pieces
-    flops = 2 * rows * depth * inner * 4
-    return pl.pallas_call(
-        functools.partial(cell_kernel, len(token_pieces)),
-        name="cell",
+    flops = 2 * rows * depth * inner * len(weights)
+    return pl.pallas_call(
+        mix_kernel,
+        name="mix",
         out_shape=[
             pltpu.VMEM((rows, inner), BF16),
             jax.ShapeDtypeStruct((rows, heads, dim), F32),
-            jax.ShapeDtypeStruct((heads, rows), F32),
-            pltpu.VMEM((rows, heads), F32),
-            pltpu.VMEM((rows, heads), F32),
             pltpu.VMEM((rows, inner), F32),
             pltpu.VMEM((rows, inner), F32),
         ],
-        in_specs=[VMEM] * (len(partners) + 6) + [HBM] * 5,
-        out_specs=[VMEM] * 7,
-        scratch_shapes=[
-            pltpu.VMEM((rows, depth), F32),
-            pltpu.VMEM((4, depth, inner), BF16),
-            pltpu.VMEM((blocks, rows // blocks, heads, dim, dim), F32),
-            pltpu.VMEM((heads, rows, dim), F32),
-            pltpu.SemaphoreType.DMA((4, W_PARTS)),
-            pltpu.SemaphoreType.DMA((blocks,)),
-        ],
-        compiler_params=pltpu.CompilerParams(vmem_limit_bytes=CELL_VMEM),
-        cost_estimate=pl.CostEstimate(flops=flops * 64, bytes_accessed=13 * 2**20, transcendentals=0),
-    )(*partners, *load([own, gain, wi, wf, normalizer, old_max.T]), *map(in_hbm, [*weights, memory]))
+        in_specs=[VMEM] * 10,
+        out_specs=[VMEM] * 4,
+        compiler_params=pltpu.CompilerParams(vmem_limit_bytes=16 * 2**20),
+        cost_estimate=pl.CostEstimate(flops=flops * 32, bytes_accessed=6 * 2**20, transcendentals=0),
+    )(normed, query, old_part, keep, admit, floor, normalizer, *map(in_vmem, weights))
 
 
 def out_kernel(pieces, *refs):
@@ -322,16 +292,15 @@
     ):
         rows, own_channels = tokens.shape
         heads, head_dim = memory.shape[1], memory.shape[2]
-        pieces = column_pieces(tokens, "tp", tp)
-        mixed, new_normalizer, new_max_t, keep, admit, keys, values = run_cell(
-            pieces,
-            norm_gain[None],
-            w_input_gate.T,
-            w_forget_gate.T,
-            normalizer,
-            memory_max,
-            [w_query, w_key, w_value, w_outgate],
-            memory,
+        own, gain, wi, wf, old_normalizer, old_max_t = load(
+            [tokens, norm_gain[None], w_input_gate.T, w_forget_gate.T, normalizer, memory_max.T]
+        )
+        pieces = column_pieces(own, "tp", tp)
+        normed, query, old_part, keep, admit, floor, new_max_t = run_read(
+            pieces, gain, wi, wf, old_max_t, w_query, memory
+        )
+        mixed, new_normalizer, keys, values = run_mix(
+            normed, query, old_part, keep, admit, floor, old_normalizer, [w_key, w_value, w_outgate]
         )
         pieces = column_pieces(mixed, "tp", tp)
         resid, copies = run_out(pieces, tokens, w_output, kv)

time: 58.6 us -> 56.2 us (0.959)
  Pallas kernels: 10.3 us -> 6.69 us
  waiting for transfers between devices: 13.5 us -> 14.2 us
    pallas_call x1 -> x2, Pallas kernels: 6.84 us -> 3.04 us  [the longest x1 1.93 us: run_read(): pl.pallas_call(functools.partial(read_kernel, len(token_pieces)), name='r...]
    ppermute x3, waiting for transfers between devices: 2.74 us -> 3.41 us  [shifted(): return lax.ppermute(x, axis, [(i, (i + step) % size) for i in range(size)])]
  transfers between devices with their start and end apart: 4 -> 4, of which waited for: 4 -> 4; matrix products, arithmetic and copies ran while one was open for 8% -> 8% of each run, Pallas kernels for 2% -> 0%
where the time goes in v3:
time: 56.2 us; the launch traced here: 56 us
  blocking collectives  23.4 us (42%)
  waiting for transfers between devices  14.2 us (25%)
  Pallas kernels  6.69 us (12%)
  other arithmetic  5.29 us (9%)
  starting transfers between devices  5.07 us (9%)
  between operations  0.77 us (1%)
  local copies, waits for them, and re-layouts  0.6 us (1%)
    all_to_all x1, blocking collectives, per_device(): lax.all_to_all(copies, 'kv', 0, 0).reshape(kv * rows, own_channels)  23.4 us
    all_to_all x1, waiting for transfers between devices, per_device(): lax.all_to_all(down_part.reshape(kv, rows, own_channels), 'kv', 0, 0)  10.8 us
    add x1, other arithmetic, per_device(): keep[..., None, None] * memory  4.59 us
    all_to_all x1, starting transfers between devices, per_device(): lax.all_to_all(down_part.reshape(kv, rows, own_channels), 'kv', 0, 0)  3.95 us
    ppermute x3, waiting for transfers between devices, shifted(): return lax.ppermute(x, axis, [(i, (i + step) % size) for i in range(size)])  3.41 us
    pallas_call x1, Pallas kernels, run_read(): pl.pallas_call(functools.partial(read_kernel, len(token_pieces)), name='r...  1.93 us
    pallas_call x1, Pallas kernels, run_down(): pl.pallas_call(functools.partial(down_kernel, len(others), channels), nam...  1.43 us
  transfers between devices with their start and end apart: 4, of which 4 were waited for; matrix products, arithmetic and copies ran while one was open for 8% of the time, Pallas kernels for 0%

profile of v3, /device:TPU:0, one launch (start us, length us, event | category | flops | bytes accessed | tf_op | source)
XLA Modules:
  0.0 56.0 jit_solution(7781131539445340792)
XLA Ops:
  0.6 0.0 copy-start
  0.6 0.0 copy-start.1
  0.7 1.0 %load.1 = (bf16[16,1024]{1,0:T(8,128)(2,1)S(1)}, f32[1,2048]{1,0:T(1,128)S(1)}, bf16[8,2048]{1,0:T(8,128)(2,1)S(1)}, bf16[8,2048]{1,0:T(8,128)(2,1)S(1)}, f32[16...) custom-call(bf16[16,1024]{1,0:T(8,128)(2,1)} %refs_2_.1, f32[1,2048]{1,0:T(1,128)} %bitcast.16, bf16[8,2048]{1,0:T(8,128)(2,1)} %bitcast.14, ...), custom_call_target="tpu_custom_call" | custom-call | flops 68719476736 | bytes 262144 | tf_op jit(solution)/shard_map/load/pallas_call | solution.py:54
  1.7 0.0 copy-start.8
  1.7 0.0 copy-start.9
  1.7 0.0 copy-start.10
  1.7 0.6 collective-permute-start
  2.3 0.9 %collective-permute-done.refs_1_ = bf16[16,1024]{1,0:T(8,128)(2,1)S(1)} collective-permute-done((bf16[16,1024]{1,0:T(8,128)(2,1)S(1)}, bf16[16,1024]{1,0:T(8,128)(2,1)S(1)}, u32[]{:S(2)}, u32[]{:S(2)}) %collective-permute-start) | collective-permute-done | bytes 32800 | tf_op jit(solution)/shard_map/ppermute | solution.py:20
  3.1 0.0 copy-done
  3.2 0.4 copy-done.1
  3.6 1.9 %read.1 = (bf16[16,2048]{1,0:T(8,128)(2,1)S(1)}, f32[16,512]{1,0:T(8,128)S(1)}, f32[4,16,128]{2,1,0:T(8,128)S(1)}, f32[16,4]{1,0:T(8,128)S(1)}, f32[16,4]{1,0:T(...) custom-call(bf16[16,1024]{1,0:T(8,128)(2,1)S(1)} %get-tuple-element.25.refs_0_, ...), custom_call_target="tpu_custom_call" | custom-call | flops 1073741824 | bytes 6291456 | tf_op jit(solution)/shard_map/read/pallas_call | solution.py:113
  5.5 0.0 copy-done.8
  5.5 0.0 copy-done.9
  5.6 0.1 copy-done.10
  5.6 0.0 copy-start.7
  5.7 1.1 %mix.1 = (bf16[16,512]{1,0:T(8,128)(2,1)S(1)}, f32[16,4,128]{2,1,0:T(4,128)}, f32[16,512]{1,0:T(8,128)S(1)}, f32[16,512]{1,0:T(8,128)S(1)}) custom-call(bf16[16,2048]{1,0:T(8,128)(2,1)S(1)} %get-tuple-element.30.refs_0_, f32[16,512]{1,0:T(8,128)S(1)} %get-tuple-element.31.refs_1_, f32[4,16,128]{2,1,0:T(8,128)S(1)} %get-tuple-element.32.refs_2_, ...), custom_call_target="tpu_custom_call" | custom-call | flops 3221225472 | bytes 6291456 | tf_op jit(solution)/shard_map/mix/pallas_call | solution.py:166
  6.8 0.5 collective-permute-start.1
  7.3 0.8 %collective-permute-done.1.refs_1_ = bf16[16,512]{1,0:T(8,128)(2,1)S(1)} collective-permute-done((bf16[16,512]{1,0:T(8,128)(2,1)S(1)}, bf16[16,512]{1,0:T(8,128)(2,1)S(1)}, u32[]{:S(2)}, u32[]{:S(2)}) %collective-permute-start.1) | collective-permute-done | bytes 16416 | tf_op jit(solution)/shard_map/ppermute | solution.py:20
  8.1 0.0 copy-done.2
  8.1 0.4 out_projection.1
  8.5 23.4 %all_to_all.10 = bf16[16,16,1024]{2,1,0:T(8,128)(2,1)S(1)} all-to-all(bf16[16,16,1024]{2,1,0:T(8,128)(2,1)S(1)} %get-tuple-element.39), channel_id=1, replica_groups=mesh['kv'=16,'tp'=2] {'kv'}, dimensions={0} | all-to-all | bytes 1048576 | tf_op jit(solution)/shard_map/all_to_all | solution.py:307
  31.9 0.0 copy-done.5
  31.9 0.8 %gate_up.1 = (f32[256,768]{1,0:T(8,128)S(1)}, bf16[256,768]{1,0:T(8,128)(2,1)S(1)}) custom-call(bf16[256,1024]{1,0:T(8,128)(2,1)S(1)} %bitcast.10, f32[1,1024]{1,0:T(1,128)S(1)} %bitcast.13, bf16[352,1024]{1,0:T(8,128)(2,1)S(1)} %bitcast.11, bf16[352,1024]{1,0:T(8,128)(2,1)S(1)} %bitcast.12), custom_call_target="tpu_custom_call" | custom-call | flops 369098752 | bytes 4194304 | tf_op jit(solution)/shard_map/gate_up/pallas_call | solution.py:233
  32.7 0.1 collective-permute-start.2
  32.8 1.7 %collective-permute-done.2.refs_0_ = bf16[256,768]{1,0:T(8,128)(2,1)S(1)} collective-permute-done((bf16[256,768]{1,0:T(8,128)(2,1)S(1)}, bf16[256,768]{1,0:T(8,128)(2,1)S(1)}, u32[]{:S(2)}, u32[]{:S(2)}) %collective-permute-start.2) | collective-permute-done | bytes 393248 | tf_op jit(solution)/shard_map/ppermute | solution.py:20
  34.5 0.0 copy-done.3
  34.5 1.4 %down.1 = bf16[256,1024]{1,0:T(8,128)(2,1)} custom-call(f32[256,768]{1,0:T(8,128)S(1)} %get-tuple-element.40.own, bf16[256,768]{1,0:T(8,128)(2,1)S(1)} %collective-permute-done.2.refs_0_, bf16[352,1024]{1,0:T(8,128)(2,1)S(1)} %copy-done.3), custom_call_target="tpu_custom_call" | custom-call | flops 184549376 | bytes 2097152 | tf_op jit(solution)/shard_map/down/pallas_call | solution.py:263
  35.9 4.0 %all-to-all-start.1 = ((bf16[16,16,1024]{2,1,0:T(8,128)(2,1)}), bf16[16,16,1024]{2,1,0:T(8,128)(2,1)S(1)}, u32[]{:S(2)}, u32[]{:S(2)}) async-start(bf16[16,16,1024]{2,1,0:T(8,128)(2,1)} %bitcast.8), calls=%async_computation.1 | async-start | bytes 1048576 | tf_op jit(solution)/shard_map/all_to_all | solution.py:317
  39.9 4.6 %multiply_add_fusion = f32[16,4,128,128]{3,2,1,0:T(8,128)} fusion(f32[16,4,128,128]{3,2,1,0:T(8,128)} %refs_7_.2, f32[16,4,128]{2,1,0:T(4,128)S(1)} %mul.38, f32[16,4,128]{2,1,0:T(4,128)S(1)} %mul.36, f32[16,4]{1,0:T(8,128)S(1)} %get-tuple-element.34.refs_4_, f32[16,4]{1,0:T(8,128)S(1)} %get-tuple-element.33.refs_3_), kind=kLoop, calls=%fused_computation | loop fusion | flops 4194304 | bytes 8454656 | tf_op jit(solution)/shard_map/add | solution.py:310
  44.5 10.8 %all-to-all-done.1 = bf16[16,16,1024]{2,1,0:T(8,128)(2,1)S(1)} async-done(((bf16[16,16,1024]{2,1,0:T(8,128)(2,1)}), bf16[16,16,1024]{2,1,0:T(8,128)(2,1)S(1)}, u32[]{:S(2)}, u32[]{:S(2)}) %all-to-all-start.1) | async-done | bytes 524320 | tf_op jit(solution)/shard_map/all_to_all | solution.py:317
  55.3 0.1 convert_reduce_fusion
  55.4 0.6 %add_convert_fusion = bf16[16,1024]{1,0:T(8,128)(2,1)} fusion(f32[16,1024]{1,0:T(8,128)S(1)} %convert_reduce_fusion, bf16[16,1024]{1,0:T(8,128)(2,1)S(1)} %get-tuple-element.38), kind=kLoop, calls=%fused_computation.2 | loop fusion | flops 49152 | bytes 131072 | tf_op jit(solution)/shard_map/convert_element_type | solution.py:319
  (10 shorter events, 0.0 us)
Async XLA Ops:
  0.6 2.5 %copy-start = (f32[16,4,128,128]{3,2,1,0:T(8,128)S(1)}, f32[16,4,128,128]{3,2,1,0:T(8,128)}, u32[]{:S(2)}) copy-start(f32[16,4,128,128]{3,2,1,0:T(8,128)} %refs_7_.2) | copy-start | bytes 12582916
  0.6 3.0 %copy-start.1 = (bf16[2048,512]{1,0:T(8,128)(2,1)S(1)}, bf16[2048,512]{1,0:T(8,128)(2,1)}, u32[]{:S(2)}) copy-start(bf16[2048,512]{1,0:T(8,128)(2,1)} %refs_6_.1) | copy-start | bytes 6291460
  1.7 3.8 %copy-start.8 = (bf16[2048,512]{1,0:T(8,128)(2,1)S(1)}, bf16[2048,512]{1,0:T(8,128)(2,1)}, u32[]{:S(2)}) copy-start(bf16[2048,512]{1,0:T(8,128)(2,1)} %refs_7_.3) | copy-start | bytes 6291460
  1.7 3.8 %copy-start.9 = (bf16[2048,512]{1,0:T(8,128)(2,1)S(1)}, bf16[2048,512]{1,0:T(8,128)(2,1)}, u32[]{:S(2)}) copy-start(bf16[2048,512]{1,0:T(8,128)(2,1)} %refs_8_.1) | copy-start | bytes 6291460
  1.7 3.9 %copy-start.10 = (bf16[2048,512]{1,0:T(8,128)(2,1)S(1)}, bf16[2048,512]{1,0:T(8,128)(2,1)}, u32[]{:S(2)}) copy-start(bf16[2048,512]{1,0:T(8,128)(2,1)} %refs_9_.1) | copy-start | bytes 6291460
  1.7 1.4 %collective-permute-start = (bf16[16,1024]{1,0:T(8,128)(2,1)S(1)}, bf16[16,1024]{1,0:T(8,128)(2,1)S(1)}, u32[]{:S(2)}, u32[]{:S(2)}) collective-permute-start(bf16[16,1024]{1,0:T(8,128)(2,1)S(1)} %get-tuple-element.25.refs_0_), channel_id=1, source_target_pairs={{0,1},{1,0},{2,3},{3,2},{4,5},{5,4},{6,7},{7,6},{8,9},{9,8},{10,11... | collective-permute-start | bytes 98312 | tf_op jit(solution)/shard_map/ppermute | solution.py:20
  5.6 2.5 %copy-start.2 = (bf16[1024,1024]{1,0:T(8,128)(2,1)S(1)}, bf16[1024,1024]{1,0:T(8,128)(2,1)}, u32[]{:S(2)}) copy-start(bf16[1024,1024]{1,0:T(8,128)(2,1)} %refs_3_.1) | copy-start | bytes 6291460
  5.6 2.5 %copy-start.6 = (bf16[16,1024]{1,0:T(8,128)(2,1)S(1)}, bf16[16,1024]{1,0:T(8,128)(2,1)}, u32[]{:S(2)}) copy-start(bf16[16,1024]{1,0:T(8,128)(2,1)} %refs_2_.1) | copy-start | bytes 98308
  5.6 26.3 %copy-start.4 = (bf16[1024,352]{0,1:T(8,128)(2,1)S(1)}, bf16[1024,352]{0,1:T(8,128)(2,1)}, u32[]{:S(2)}) copy-start(bf16[1024,352]{0,1:T(8,128)(2,1)} %param.29) | copy-start | bytes 2162692
  5.6 26.3 %copy-start.5 = (bf16[1024,352]{0,1:T(8,128)(2,1)S(1)}, bf16[1024,352]{0,1:T(8,128)(2,1)}, u32[]{:S(2)}) copy-start(bf16[1024,352]{0,1:T(8,128)(2,1)} %param.30) | copy-start | bytes 2162692
  5.6 26.3 %copy-start.7 = (f32[1024]{0:T(1024)S(1)}, f32[1024]{0:T(1024)}, u32[]{:S(2)}) copy-start(f32[1024]{0:T(1024)} %param.28) | copy-start | bytes 12292
  6.8 27.8 %copy-start.3 = (bf16[352,1024]{1,0:T(8,128)(2,1)S(1)}, bf16[352,1024]{1,0:T(8,128)(2,1)}, u32[]{:S(2)}) copy-start(bf16[352,1024]{1,0:T(8,128)(2,1)} %refs_1_.1) | copy-start | bytes 2162692
  6.8 1.3 %collective-permute-start.1 = (bf16[16,512]{1,0:T(8,128)(2,1)S(1)}, bf16[16,512]{1,0:T(8,128)(2,1)S(1)}, u32[]{:S(2)}, u32[]{:S(2)}) collective-permute-start(bf16[16,512]{1,0:T(8,128)(2,1)S(1)} %get-tuple-element.37.refs_0_), channel_id=1, source_target_pairs={{0,1},{1,0},{2,3},{3,2},{4,5},{5,4},{6,7},{7,6},{8,9},{9,8},{10,11... | collective-permute-start | bytes 49160 | tf_op jit(solution)/shard_map/ppermute | solution.py:20
  32.7 1.8 %collective-permute-start.2 = (bf16[256,768]{1,0:T(8,128)(2,1)S(1)}, bf16[256,768]{1,0:T(8,128)(2,1)S(1)}, u32[]{:S(2)}, u32[]{:S(2)}) collective-permute-start(bf16[256,768]{1,0:T(8,128)(2,1)S(1)} %get-tuple-element.41), channel_id=1, source_target_pairs={{0,1},{1,0},{2,3},{3,2},{4,5},{5,4},{6,7},{7,6},{8,9},{9,8},{10,11... | collective-permute-start | bytes 1179656 | tf_op jit(solution)/shard_map/ppermute | solution.py:20
  35.9 19.3 %all-to-all-start.1 = ((bf16[16,16,1024]{2,1,0:T(8,128)(2,1)}), bf16[16,16,1024]{2,1,0:T(8,128)(2,1)S(1)}, u32[]{:S(2)}, u32[]{:S(2)}) async-start(bf16[16,16,1024]{2,1,0:T(8,128)(2,1)} %bitcast.8), calls=%async_computation.1 | async-start | bytes 1048576 | tf_op jit(solution)/shard_map/all_to_all | solution.py:317

commit v4 on v3

--- a/solution.py
+++ b/solution.py
@@ -18,6 +18,27 @@
 
 def shifted(x, axis, size, step):
     return lax.ppermute(x, axis, [(i, (i + step) % size) for i in range(size)])
+
+
+def partner(i, step, size):
+    return i ^ step if size & (size - 1) == 0 else (i + step) % size
+
+
+def group_sizes(size):
+    low = 1
+    while low * low < size:
+        low *= 2
+    return (size // low, low) if size % low == 0 else (size, 1)
+
+
+def exchange(x, axis, size, low, step, inner):
+    pairs = []
+    for k in range(size):
+        a, b = divmod(k, low)
+        b2 = partner(b, step, low) if inner else b
+        a2 = a if inner else partner(a, step, size // low)
+        pairs.append((k, a2 * low + b2))
+    return lax.ppermute(x, axis, pairs)
 
 
 def column_pieces(x, axis, size):
@@ -180,25 +201,22 @@
 
 
 def out_kernel(pieces, *refs):
-    mixed_refs, (tokens, w_output, resid, copies) = refs[:pieces], refs[pieces:]
+    mixed_refs, (tokens, w_output, resid) = refs[:pieces], refs[pieces:]
     total = tokens[...].astype(F32)
     for ref, start in zip(mixed_refs, piece_starts(mixed_refs, "tp")):
         weight = w_output[pl.ds(start, ref.shape[1]), :]
         total = total + jnp.dot(ref[...], weight, preferred_element_type=F32)
-    out = total.astype(BF16)
-    resid[...] = out
-    for i in range(copies.shape[0]):
-        copies[i] = out
-
-
-def run_out(mixed_pieces, tokens, w_output, kv):
+    resid[...] = total.astype(BF16)
+
+
+def run_out(mixed_pieces, tokens, w_output):
     rows, width = tokens.shape
     return pl.pallas_call(
         functools.partial(out_kernel, len(mixed_pieces)),
         name="out_projection",
-        out_shape=[jax.ShapeDtypeStruct((rows, width), BF16), jax.ShapeDtypeStruct((kv, rows, width), BF16)],
+        out_shape=pltpu.VMEM((rows, width), BF16),
         in_specs=[VMEM] * (len(mixed_pieces) + 2),
-        out_specs=[VMEM, VMEM],
+        out_specs=VMEM,
         compiler_params=pltpu.CompilerParams(vmem_limit_bytes=24 * 2**20),
         cost_estimate=pl.CostEstimate(
             flops=2 * rows * w_output.size, bytes_accessed=2 * w_output.size, transcendentals=0
@@ -206,10 +224,30 @@
     )(*mixed_pieces, tokens, w_output)
 
 
-def up_kernel(rows_ref, gain, w_gate, w_up, own, sent):
+def stack_kernel(low, *refs):
+    *pieces, out = refs
+    me = lax.div(lax.axis_index("kv"), low)
+    for step, ref in enumerate(pieces):
+        out[partner(me, step, out.shape[0])] = ref[...]
+
+
+def run_stack(pieces, low):
+    return pl.pallas_call(
+        functools.partial(stack_kernel, low),
+        name="stack",
+        out_shape=pltpu.VMEM((len(pieces), *pieces[0].shape), BF16),
+        in_specs=[VMEM] * len(pieces),
+        out_specs=VMEM,
+        compiler_params=pltpu.CompilerParams(vmem_limit_bytes=16 * 2**20),
+        cost_estimate=pl.CostEstimate(flops=2**20, bytes_accessed=2**18, transcendentals=0),
+    )(*pieces)
+
+
+def up_kernel(pieces, *refs):
+    piece_refs, (gain, w_gate, w_up, own, sent) = refs[:pieces], refs[pieces:]
     hidden = w_gate.shape[0]
     half = own.shape[1] // 2
-    x = rows_ref[...].astype(F32)
+    x = jnp.concatenate([ref[...].reshape(-1, ref.shape[2]) for ref in piece_refs], axis=0).astype(F32)
     squares = jnp.sum(x * x, axis=1, keepdims=True)
     ffn_in = (x * gain[...]).astype(BF16)
     own[...] = jnp.zeros_like(own)
@@ -226,23 +264,24 @@
     sent[:, first : first + LANES] = tile.astype(BF16)
 
 
-def run_up(every_row, gain, w_gate, w_up):
-    rows, depth = every_row.shape
+def run_up(pieces, gain, w_gate, w_up):
+    rows, depth = sum(x.shape[0] * x.shape[1] for x in pieces), pieces[0].shape[2]
     hidden = w_gate.shape[1]
     half = (hidden + 2 + LANES - 1) // LANES * LANES
     return pl.pallas_call(
-        up_kernel,
+        functools.partial(up_kernel, len(pieces)),
         name="gate_up",
         out_shape=[jax.ShapeDtypeStruct((rows, 2 * half), F32), jax.ShapeDtypeStruct((rows, 2 * half), BF16)],
-        in_specs=[VMEM] * 4,
+        in_specs=[VMEM] * (len(pieces) + 3),
         out_specs=[VMEM, VMEM],
         compiler_params=pltpu.CompilerParams(vmem_limit_bytes=24 * 2**20),
         cost_estimate=pl.CostEstimate(flops=4 * rows * depth * hidden, bytes_accessed=4 * 2**20, transcendentals=0),
-    )(every_row, gain, w_gate.T, w_up.T)
-
-
-def down_kernel(others, channels, own, *refs):
-    other_refs, (w_down, out) = refs[:others], refs[others:]
+    )(*pieces, gain, w_gate.T, w_up.T)
+
+
+def down_kernel(others, channels, low, own, *refs):
+    other_refs, (w_down, *refs) = refs[:others], refs[others:]
+    kept, *sent = refs
     hidden = w_down.shape[0]
     half = own.shape[1] // 2
     gate, up = own[:, :half], own[:, half:]
@@ -254,21 +293,51 @@
     scale = lax.rsqrt(squares / channels + 1e-06)
     gate = scale * gate[:, :hidden]
     act = (gate * jax.nn.sigmoid(gate) * (scale * up[:, :hidden])).astype(BF16)
-    out[...] = jnp.dot(act, w_down[...], preferred_element_type=F32).astype(BF16)
-
-
-def run_down(own, others, w_down, channels):
-    rows = own.shape[0]
+    full = jnp.dot(act, w_down[...], preferred_element_type=F32).reshape(low, *kept.shape)
+    kept[...] = full[0]
+    for step, ref in enumerate(sent, 1):
+        ref[...] = full[step].astype(BF16)
+
+
+def run_down(own, others, w_down, channels, high, low):
+    rows = own.shape[0] // (high * low)
     hidden, width = w_down.shape
     return pl.pallas_call(
-        functools.partial(down_kernel, len(others), channels),
+        functools.partial(down_kernel, len(others), channels, low),
         name="down",
-        out_shape=jax.ShapeDtypeStruct((rows, width), BF16),
+        out_shape=[pltpu.VMEM((high, rows, width), F32)] + [pltpu.VMEM((high, rows, width), BF16)] * (low - 1),
         in_specs=[VMEM] * (2 + len(others)),
-        out_specs=VMEM,
+        out_specs=[VMEM] * low,
         compiler_params=pltpu.CompilerParams(vmem_limit_bytes=24 * 2**20),
-        cost_estimate=pl.CostEstimate(flops=2 * rows * width * hidden, bytes_accessed=2 * 2**20, transcendentals=0),
+        cost_estimate=pl.CostEstimate(flops=2 * own.shape[0] * width * hidden, bytes_accessed=2**21, transcendentals=0),
     )(own, *others, w_down)
+
+
+def fold_kernel(count, low, kept, *refs):
+    received, (own, *sent), total = refs[:count], refs[count:-1], refs[-1]
+    x = kept[...]
+    for ref in received:
+        x = x + ref[...].astype(F32)
+    total[...] = x
+    high = kept.shape[0]
+    me = lax.div(lax.axis_index("kv"), low)
+    own[...] = total[me]
+    for step, ref in enumerate(sent, 1):
+        ref[...] = total[partner(me, step, high)].astype(BF16)
+
+
+def run_fold(kept, received, low):
+    high, rows, width = kept.shape
+    return pl.pallas_call(
+        functools.partial(fold_kernel, len(received), low),
+        name="fold",
+        out_shape=[pltpu.VMEM((rows, width), F32)] + [pltpu.VMEM((rows, width), BF16)] * (high - 1),
+        in_specs=[VMEM] * (1 + len(received)),
+        out_specs=[VMEM] * high,
+        scratch_shapes=[pltpu.VMEM(kept.shape, F32)],
+        compiler_params=pltpu.CompilerParams(vmem_limit_bytes=16 * 2**20),
+        cost_estimate=pl.CostEstimate(flops=2**24, bytes_accessed=2**20, transcendentals=0),
+    )(kept, *received)
 
 
 def make(kv, tp):
@@ -303,8 +372,11 @@
             normed, query, old_part, keep, admit, floor, old_normalizer, [w_key, w_value, w_outgate]
         )
         pieces = column_pieces(mixed, "tp", tp)
-        resid, copies = run_out(pieces, tokens, w_output, kv)
-        every_row = lax.all_to_all(copies, "kv", 0, 0).reshape(kv * rows, own_channels)
+        resid = run_out(pieces, tokens, w_output)
+        high, low = group_sizes(kv)
+        column = [resid] + [exchange(resid, "kv", kv, low, step, False) for step in range(1, high)]
+        block = run_stack(column, low)
+        every_row = [block] + [exchange(block, "kv", kv, low, step, True) for step in range(1, low)]
         by_head = (rows, heads, head_dim)
         keys, values = keys.reshape(by_head), values.reshape(by_head)
         new_memory = keep[..., None, None] * memory + admit[..., None, None] * (
@@ -313,9 +385,14 @@
 
         own, sent = run_up(every_row, ffn_gain[None], w_gate, w_up)
         others = [shifted(sent, "tp", tp, step) for step in range(1, tp)]
-        down_part = run_down(own, others, w_down, own_channels * tp)
-        pieces = lax.all_to_all(down_part.reshape(kv, rows, own_channels), "kv", 0, 0)
-        down_out = jnp.sum(pieces.astype(F32), axis=0)
+        kept, *sent = run_down(own, others, w_down, own_channels * tp, high, low)
+        received = [exchange(x, "kv", kv, low, step, True) for step, x in enumerate(sent, 1)]
+        *received, new_memory = lax.optimization_barrier((*received, new_memory))
+        kept, *sent = run_fold(kept, received, low)
+        received = [exchange(x, "kv", kv, low, step, False) for step, x in enumerate(sent, 1)]
+        down_out = kept
+        for x in received:
+            down_out = down_out + x.astype(F32)
         result = (resid.astype(F32) + down_out).astype(BF16)
         return (result, new_memory, new_normalizer, new_max_t.T)
 

time: 56.2 us -> 48.2 us (0.86)
  blocking collectives: 23.4 us -> 0 us
  starting transfers between devices: 5.07 us -> 18.2 us
  waiting for transfers between devices: 14.2 us -> 17.3 us
  Pallas kernels: 6.69 us -> 5.93 us
    all_to_all x1 -> x0, blocking collectives: 23.4 us -> none  [per_device(): lax.all_to_all(copies, 'kv', 0, 0).reshape(kv * rows, own_channels)]
    ppermute x0 -> x12, starting transfers between devices: none -> 17.1 us  [exchange(): return lax.ppermute(x, axis, pairs)]
    ppermute x0 -> x12, waiting for transfers between devices: none -> 13.9 us  [exchange(): return lax.ppermute(x, axis, pairs)]
    all_to_all x1 -> x0, waiting for transfers between devices: 10.8 us -> none  [per_device(): lax.all_to_all(down_part.reshape(kv, rows, own_channels), 'kv', 0, 0)]
    all_to_all x1 -> x0, starting transfers between devices: 3.95 us -> none  [per_device(): lax.all_to_all(down_part.reshape(kv, rows, own_channels), 'kv', 0, 0)]
    pallas_call x2 -> x4, Pallas kernels: 2.21 us -> 1.48 us  [the longest x1 0.77 us: run_up(): pl.pallas_call(functools.partial(up_kernel, len(pieces)), name='gate_up',...]
  transfers between devices with their start and end apart: 4 -> 15, of which waited for: 4 -> 11; matrix products, arithmetic and copies ran while one was open for 8% -> 10% of each run, Pallas kernels for 0% -> 0%
where the time goes in v4:
time: 48.2 us; the launch traced here: 48 us
  starting transfers between devices  18.2 us (38%)
  waiting for transfers between devices  17.3 us (36%)
  Pallas kernels  5.93 us (12%)
  other arithmetic  5.22 us (11%)
  between operations  0.78 us (2%)
  local copies, waits for them, and re-layouts  0.6 us (1%)
    ppermute x12, starting transfers between devices, exchange(): return lax.ppermute(x, axis, pairs)  17.1 us
    ppermute x12, waiting for transfers between devices, exchange(): return lax.ppermute(x, axis, pairs)  13.9 us
    add x1, other arithmetic, per_device(): keep[..., None, None] * memory  4.58 us
    ppermute x3, waiting for transfers between devices, shifted(): return lax.ppermute(x, axis, [(i, (i + step) % size) for i in range(size)])  3.37 us
    pallas_call x1, Pallas kernels, run_read(): pl.pallas_call(functools.partial(read_kernel, len(token_pieces)), name='r...  1.93 us
    ppermute x3, starting transfers between devices, shifted(): return lax.ppermute(x, axis, [(i, (i + step) % size) for i in range(size)])  1.12 us
    pallas_call x1, Pallas kernels, run_mix(): pl.pallas_call(mix_kernel, name='mix', out_shape=[pltpu.VMEM((rows, inner...  1.11 us
    pallas_call x1, Pallas kernels, load(): pl.pallas_call(functools.partial(load_kernel, len(arrays)), name='load',...  1.03 us
  transfers between devices with their start and end apart: 15, of which 11 were waited for; matrix products, arithmetic and copies ran while one was open for 10% of the time, Pallas kernels for 0%

profile of v4, /device:TPU:0, one launch (start us, length us, event | category | flops | bytes accessed | tf_op | source)
XLA Modules:
  0.0 48.0 jit_solution(5803398581661478765)
XLA Ops:
  0.7 1.0 %load.1 = (bf16[16,1024]{1,0:T(8,128)(2,1)S(1)}, f32[1,2048]{1,0:T(1,128)S(1)}, bf16[8,2048]{1,0:T(8,128)(2,1)S(1)}, bf16[8,2048]{1,0:T(8,128)(2,1)S(1)}, f32[16...) custom-call(bf16[16,1024]{1,0:T(8,128)(2,1)} %refs_2_.1, f32[1,2048]{1,0:T(1,128)} %bitcast.13, bf16[8,2048]{1,0:T(8,128)(2,1)} %bitcast.11, ...), custom_call_target="tpu_custom_call" | custom-call | flops 68719476736 | bytes 262144 | tf_op jit(solution)/shard_map/load/pallas_call | solution.py:75
  1.7 0.6 %collective-permute-start = (bf16[16,1024]{1,0:T(8,128)(2,1)S(1)}, bf16[16,1024]{1,0:T(8,128)(2,1)S(1)}, u32[]{:S(2)}, u32[]{:S(2)}) collective-permute-start(bf16[16,1024]{1,0:T(8,128)(2,1)S(1)} %get-tuple-element.35.refs_0_), channel_id=1, source_target_pairs={{0,1},{1,0},{2,3},{3,2},{4,5},{5,4},{6,7},{7,6},{8,9},{9,8},{10,11... | collective-permute-start | bytes 98312 | tf_op jit(solution)/shard_map/ppermute | solution.py:20
  2.3 0.9 %collective-permute-done.refs_1_ = bf16[16,1024]{1,0:T(8,128)(2,1)S(1)} collective-permute-done((bf16[16,1024]{1,0:T(8,128)(2,1)S(1)}, bf16[16,1024]{1,0:T(8,128)(2,1)S(1)}, u32[]{:S(2)}, u32[]{:S(2)}) %collective-permute-start) | collective-permute-done | bytes 32800 | tf_op jit(solution)/shard_map/ppermute | solution.py:20
  3.2 0.4 copy-done.1
  3.6 1.9 %read.1 = (bf16[16,2048]{1,0:T(8,128)(2,1)S(1)}, f32[16,512]{1,0:T(8,128)S(1)}, f32[4,16,128]{2,1,0:T(8,128)S(1)}, f32[16,4]{1,0:T(8,128)S(1)}, f32[16,4]{1,0:T(...) custom-call(bf16[16,1024]{1,0:T(8,128)(2,1)S(1)} %get-tuple-element.35.refs_0_, ...), custom_call_target="tpu_custom_call" | custom-call | flops 1073741824 | bytes 6291456 | tf_op jit(solution)/shard_map/read/pallas_call | solution.py:134
  5.7 1.1 %mix.1 = (bf16[16,512]{1,0:T(8,128)(2,1)S(1)}, f32[16,4,128]{2,1,0:T(4,128)}, f32[16,512]{1,0:T(8,128)S(1)}, f32[16,512]{1,0:T(8,128)S(1)}) custom-call(bf16[16,2048]{1,0:T(8,128)(2,1)S(1)} %get-tuple-element.40.refs_0_, f32[16,512]{1,0:T(8,128)S(1)} %get-tuple-element.41.refs_1_, f32[4,16,128]{2,1,0:T(8,128)S(1)} %get-tuple-element.42.refs_2_, ...), custom_call_target="tpu_custom_call" | custom-call | flops 3221225472 | bytes 6291456 | tf_op jit(solution)/shard_map/mix/pallas_call | solution.py:187
  6.8 0.5 %collective-permute-start.1 = (bf16[16,512]{1,0:T(8,128)(2,1)S(1)}, bf16[16,512]{1,0:T(8,128)(2,1)S(1)}, u32[]{:S(2)}, u32[]{:S(2)}) collective-permute-start(bf16[16,512]{1,0:T(8,128)(2,1)S(1)} %get-tuple-element.47.refs_0_), channel_id=1, source_target_pairs={{0,1},{1,0},{2,3},{3,2},{4,5},{5,4},{6,7},{7,6},{8,9},{9,8},{10,11... | collective-permute-start | bytes 49160 | tf_op jit(solution)/shard_map/ppermute | solution.py:20
  7.3 0.8 %collective-permute-done.1.refs_1_ = bf16[16,512]{1,0:T(8,128)(2,1)S(1)} collective-permute-done((bf16[16,512]{1,0:T(8,128)(2,1)S(1)}, bf16[16,512]{1,0:T(8,128)(2,1)S(1)}, u32[]{:S(2)}, u32[]{:S(2)}) %collective-permute-start.1) | collective-permute-done | bytes 16416 | tf_op jit(solution)/shard_map/ppermute | solution.py:20
  8.1 0.4 out_projection.1.refs_0_
  8.5 4.9 %collective-permute-start.4 = (bf16[16,1024]{1,0:T(8,128)(2,1)S(1)}, bf16[16,1024]{1,0:T(8,128)(2,1)S(1)}, u32[]{:S(2)}, u32[]{:S(2)}) collective-permute-start(bf16[16,1024]{1,0:T(8,128)(2,1)S(1)} %out_projection.1.refs_0_), channel_id=1, source_target_pairs={{0,24},{2,26},{4,28},{6,30},{8,16},{10,18},{12,20},{14,22},{16,8},... | collective-permute-start | bytes 98312 | tf_op jit(solution)/shard_map/ppermute | solution.py:41
  13.4 0.6 %collective-permute-start.2 = (bf16[16,1024]{1,0:T(8,128)(2,1)S(1)}, bf16[16,1024]{1,0:T(8,128)(2,1)S(1)}, u32[]{:S(2)}, u32[]{:S(2)}) collective-permute-start(bf16[16,1024]{1,0:T(8,128)(2,1)S(1)} %out_projection.1.refs_0_), channel_id=1, source_target_pairs={{0,8},{2,10},{4,12},{6,14},{8,0},{10,2},{12,4},{14,6},{16,24},{18,... | collective-permute-start | bytes 98312 | tf_op jit(solution)/shard_map/ppermute | solution.py:41
  14.0 1.3 %collective-permute-done.4.refs_3_ = bf16[16,1024]{1,0:T(8,128)(2,1)S(1)} collective-permute-done((bf16[16,1024]{1,0:T(8,128)(2,1)S(1)}, bf16[16,1024]{1,0:T(8,128)(2,1)S(1)}, u32[]{:S(2)}, u32[]{:S(2)}) %collective-permute-start.4) | collective-permute-done | bytes 32800 | tf_op jit(solution)/shard_map/ppermute | solution.py:41
  15.3 2.9 %collective-permute-done.3.refs_2_ = bf16[16,1024]{1,0:T(8,128)(2,1)S(1)} collective-permute-done((bf16[16,1024]{1,0:T(8,128)(2,1)S(1)}, bf16[16,1024]{1,0:T(8,128)(2,1)S(1)}, u32[]{:S(2)}, u32[]{:S(2)}) %collective-permute-start.3) | collective-permute-done | bytes 32800 | tf_op jit(solution)/shard_map/ppermute | solution.py:41
  18.3 2.5 %collective-permute-start.7 = (bf16[4,16,1024]{2,1,0:T(8,128)(2,1)S(1)}, bf16[4,16,1024]{2,1,0:T(8,128)(2,1)S(1)}, u32[]{:S(2)}, u32[]{:S(2)}) collective-permute-start(bf16[4,16,1024]{2,1,0:T(8,128)(2,1)S(1)} %stack.1.refs_0_), channel_id=1, source_target_pairs={{0,6},{2,4},{4,2},{6,0},{8,14},{10,12},{12,10},{14,8},{16,22},{18,... | collective-permute-start | bytes 393224 | tf_op jit(solution)/shard_map/ppermute | solution.py:41
  20.8 0.5 %collective-permute-start.6 = (bf16[4,16,1024]{2,1,0:T(8,128)(2,1)S(1)}, bf16[4,16,1024]{2,1,0:T(8,128)(2,1)S(1)}, u32[]{:S(2)}, u32[]{:S(2)}) collective-permute-start(bf16[4,16,1024]{2,1,0:T(8,128)(2,1)S(1)} %stack.1.refs_0_), channel_id=1, source_target_pairs={{0,4},{2,6},{4,0},{6,2},{8,12},{10,14},{12,8},{14,10},{16,20},{18,... | collective-permute-start | bytes 393224 | tf_op jit(solution)/shard_map/ppermute | solution.py:41
  21.3 0.5 %collective-permute-start.5 = (bf16[4,16,1024]{2,1,0:T(8,128)(2,1)S(1)}, bf16[4,16,1024]{2,1,0:T(8,128)(2,1)S(1)}, u32[]{:S(2)}, u32[]{:S(2)}) collective-permute-start(bf16[4,16,1024]{2,1,0:T(8,128)(2,1)S(1)} %stack.1.refs_0_), channel_id=1, source_target_pairs={{0,2},{2,0},{4,6},{6,4},{8,10},{10,8},{12,14},{14,12},{16,18},{18,... | collective-permute-start | bytes 393224 | tf_op jit(solution)/shard_map/ppermute | solution.py:41
  21.8 3.2 %collective-permute-done.7.refs_3_ = bf16[4,16,1024]{2,1,0:T(8,128)(2,1)S(1)} collective-permute-done((bf16[4,16,1024]{2,1,0:T(8,128)(2,1)S(1)}, bf16[4,16,1024]{2,1,0:T(8,128)(2,1)S(1)}, u32[]{:S(2)}, u32[]{:S(2)}) %collective-permute-start.7) | collective-permute-done | bytes 131104 | tf_op jit(solution)/shard_map/ppermute | solution.py:41
  25.0 1.5 %collective-permute-done.6.refs_2_ = bf16[4,16,1024]{2,1,0:T(8,128)(2,1)S(1)} collective-permute-done((bf16[4,16,1024]{2,1,0:T(8,128)(2,1)S(1)}, bf16[4,16,1024]{2,1,0:T(8,128)(2,1)S(1)}, u32[]{:S(2)}, u32[]{:S(2)}) %collective-permute-start.6) | collective-permute-done | bytes 131104 | tf_op jit(solution)/shard_map/ppermute | solution.py:41
  26.6 0.8 %gate_up.1 = (f32[256,768]{1,0:T(8,128)S(1)}, bf16[256,768]{1,0:T(8,128)(2,1)S(1)}) custom-call(bf16[4,16,1024]{2,1,0:T(8,128)(2,1)S(1)} %stack.1.refs_0_, bf16[4,16,1024]{2,1,0:T(8,128)(2,1)S(1)} %collective-permute-done.5.refs_1_, bf16[4,16,1024]{2,1,0:T(8,128)(2,1)S(1)} %collective-permute-done.6.refs_2_, ...), custom_call_target="tpu_custom_call" | custom-call | flops 369098752 | bytes 4194304 | tf_op jit(solution)/shard_map/gate_up/pallas_call | solution.py:271
  27.5 1.7 %collective-permute-done.8.refs_0_ = bf16[256,768]{1,0:T(8,128)(2,1)S(1)} collective-permute-done((bf16[256,768]{1,0:T(8,128)(2,1)S(1)}, bf16[256,768]{1,0:T(8,128)(2,1)S(1)}, u32[]{:S(2)}, u32[]{:S(2)}) %collective-permute-start.8) | collective-permute-done | bytes 393248 | tf_op jit(solution)/shard_map/ppermute | solution.py:20
  29.2 0.6 %down.1 = (f32[4,16,1024]{2,1,0:T(8,128)S(1)}, bf16[4,16,1024]{2,1,0:T(8,128)(2,1)S(1)}, bf16[4,16,1024]{2,1,0:T(8,128)(2,1)S(1)}, bf16[4,16,1024]{2,1,0:T(8,128)(2,1)S(1)}) custom-call(f32[256,768]{1,0:T(8,128)S(1)} %get-tuple-element.48.own, bf16[256,768]{1,0:T(8,128)(2,1)S(1)} %collective-permute-done.8.refs_0_, bf16[352,1024]{1,0:T(8,128)(2,1)S(1)} %copy-done.5), custom_call_target="tpu_custom_call" | custom-call | flops 184549376 | bytes 2097152 | tf_op jit(solution)/shard_map/down/pallas_call | solution.py:305
  29.8 1.6 %collective-permute-start.9 = (bf16[4,16,1024]{2,1,0:T(8,128)(2,1)S(1)}, bf16[4,16,1024]{2,1,0:T(8,128)(2,1)S(1)}, u32[]{:S(2)}, u32[]{:S(2)}) collective-permute-start(bf16[4,16,1024]{2,1,0:T(8,128)(2,1)S(1)} %get-tuple-element.51), channel_id=1, source_target_pairs={{0,2},{2,0},{4,6},{6,4},{8,10},{10,8},{12,14},{14,12},{16,18},{18,... | collective-permute-start | bytes 393224 | tf_op jit(solution)/shard_map/ppermute | solution.py:41
  31.4 0.7 %collective-permute-start.10 = (bf16[4,16,1024]{2,1,0:T(8,128)(2,1)S(1)}, bf16[4,16,1024]{2,1,0:T(8,128)(2,1)S(1)}, u32[]{:S(2)}, u32[]{:S(2)}) collective-permute-start(bf16[4,16,1024]{2,1,0:T(8,128)(2,1)S(1)} %get-tuple-element.52), channel_id=1, source_target_pairs={{0,4},{2,6},{4,0},{6,2},{8,12},{10,14},{12,8},{14,10},{16,20},{18,... | collective-permute-start | bytes 393224 | tf_op jit(solution)/shard_map/ppermute | solution.py:41
  32.1 1.3 %collective-permute-start.11 = (bf16[4,16,1024]{2,1,0:T(8,128)(2,1)S(1)}, bf16[4,16,1024]{2,1,0:T(8,128)(2,1)S(1)}, u32[]{:S(2)}, u32[]{:S(2)}) collective-permute-start(bf16[4,16,1024]{2,1,0:T(8,128)(2,1)S(1)} %get-tuple-element.53), channel_id=1, source_target_pairs={{0,6},{2,4},{4,2},{6,0},{8,14},{10,12},{12,10},{14,8},{16,22},{18,... | collective-permute-start | bytes 393224 | tf_op jit(solution)/shard_map/ppermute | solution.py:41
  33.4 4.6 %multiply_add_fusion = f32[16,4,128,128]{3,2,1,0:T(8,128)} fusion(f32[16,4,128,128]{3,2,1,0:T(8,128)} %refs_7_.2, f32[16,4,128]{2,1,0:T(4,128)S(1)} %mul.38, f32[16,4,128]{2,1,0:T(4,128)S(1)} %mul.36, f32[16,4]{1,0:T(8,128)S(1)} %get-tuple-element.44.refs_4_, f32[16,4]{1,0:T(8,128)S(1)} %get-tuple-element.43.refs_3_), kind=kLoop, calls=%fused_computation | loop fusion | flops 4194304 | bytes 8454656 | tf_op jit(solution)/shard_map/add | solution.py:382
  38.0 1.5 %collective-permute-done.10.refs_1_ = bf16[4,16,1024]{2,1,0:T(8,128)(2,1)S(1)} collective-permute-done((bf16[4,16,1024]{2,1,0:T(8,128)(2,1)S(1)}, bf16[4,16,1024]{2,1,0:T(8,128)(2,1)S(1)}, u32[]{:S(2)}, u32[]{:S(2)}) %collective-permute-start.10) | collective-permute-done | bytes 131104 | tf_op jit(solution)/shard_map/ppermute | solution.py:41
  39.6 0.3 collective-permute-start.12
  39.9 1.8 %collective-permute-start.13 = (bf16[16,1024]{1,0:T(8,128)(2,1)S(1)}, bf16[16,1024]{1,0:T(8,128)(2,1)S(1)}, u32[]{:S(2)}, u32[]{:S(2)}) collective-permute-start(bf16[16,1024]{1,0:T(8,128)(2,1)S(1)} %get-tuple-element.61), channel_id=1, source_target_pairs={{0,16},{2,18},{4,20},{6,22},{8,24},{10,26},{12,28},{14,30},{16,0},... | collective-permute-start | bytes 98312 | tf_op jit(solution)/shard_map/ppermute | solution.py:41
  41.7 2.3 %collective-permute-start.14 = (bf16[16,1024]{1,0:T(8,128)(2,1)S(1)}, bf16[16,1024]{1,0:T(8,128)(2,1)S(1)}, u32[]{:S(2)}, u32[]{:S(2)}) collective-permute-start(bf16[16,1024]{1,0:T(8,128)(2,1)S(1)} %get-tuple-element.62), channel_id=1, source_target_pairs={{0,24},{2,26},{4,28},{6,30},{8,16},{10,18},{12,20},{14,22},{16,8},... | collective-permute-start | bytes 98312 | tf_op jit(solution)/shard_map/ppermute | solution.py:41
  44.0 1.0 %collective-permute-done.13 = bf16[16,1024]{1,0:T(8,128)(2,1)S(1)} collective-permute-done((bf16[16,1024]{1,0:T(8,128)(2,1)S(1)}, bf16[16,1024]{1,0:T(8,128)(2,1)S(1)}, u32[]{:S(2)}, u32[]{:S(2)}) %collective-permute-start.13) | collective-permute-done | bytes 32800 | tf_op jit(solution)/shard_map/ppermute | solution.py:41
  45.0 2.4 %collective-permute-done.14 = bf16[16,1024]{1,0:T(8,128)(2,1)S(1)} collective-permute-done((bf16[16,1024]{1,0:T(8,128)(2,1)S(1)}, bf16[16,1024]{1,0:T(8,128)(2,1)S(1)}, u32[]{:S(2)}, u32[]{:S(2)}) %collective-permute-start.14) | collective-permute-done | bytes 32800 | tf_op jit(solution)/shard_map/ppermute | solution.py:41
  47.4 0.6 %add_convert_fusion = bf16[16,1024]{1,0:T(8,128)(2,1)} fusion(bf16[16,1024]{1,0:T(8,128)(2,1)S(1)} %collective-permute-done.14, bf16[16,1024]{1,0:T(8,128)(2,1)S(1)} %collective-permute-done.13, f32[16,1024]{1,0:T(8,128)S(1)} %get-tuple-element.59, bf16[16,1024]{1,0:T(8,128)(2,1)S(1)} %collective-permute-done.12, bf16[16,1024]{1,0:T(8,128)(2,1)S(1)} %out_projection.1.refs_0_), kind=kLoop, calls=%fused_computation.1 | loop fusion | flops 147456 | bytes 229376 | tf_op jit(solution)/shard_map/convert_element_type | solution.py:396
  (32 shorter events, 0.4 us)
Async XLA Ops:
  0.6 2.5 %copy-start = (f32[16,4,128,128]{3,2,1,0:T(8,128)S(1)}, f32[16,4,128,128]{3,2,1,0:T(8,128)}, u32[]{:S(2)}) copy-start(f32[16,4,128,128]{3,2,1,0:T(8,128)} %refs_7_.2) | copy-start | bytes 12582916
  0.6 3.0 %copy-start.1 = (bf16[2048,512]{1,0:T(8,128)(2,1)S(1)}, bf16[2048,512]{1,0:T(8,128)(2,1)}, u32[]{:S(2)}) copy-start(bf16[2048,512]{1,0:T(8,128)(2,1)} %refs_6_.1) | copy-start | bytes 6291460
  1.7 3.8 %copy-start.8 = (bf16[2048,512]{1,0:T(8,128)(2,1)S(1)}, bf16[2048,512]{1,0:T(8,128)(2,1)}, u32[]{:S(2)}) copy-start(bf16[2048,512]{1,0:T(8,128)(2,1)} %refs_7_.3) | copy-start | bytes 6291460
  1.7 3.8 %copy-start.9 = (bf16[2048,512]{1,0:T(8,128)(2,1)S(1)}, bf16[2048,512]{1,0:T(8,128)(2,1)}, u32[]{:S(2)}) copy-start(bf16[2048,512]{1,0:T(8,128)(2,1)} %refs_8_.1) | copy-start | bytes 6291460
  1.7 3.9 %copy-start.10 = (bf16[2048,512]{1,0:T(8,128)(2,1)S(1)}, bf16[2048,512]{1,0:T(8,128)(2,1)}, u32[]{:S(2)}) copy-start(bf16[2048,512]{1,0:T(8,128)(2,1)} %refs_9_.1) | copy-start | bytes 6291460
  1.7 1.4 %collective-permute-start = (bf16[16,1024]{1,0:T(8,128)(2,1)S(1)}, bf16[16,1024]{1,0:T(8,128)(2,1)S(1)}, u32[]{:S(2)}, u32[]{:S(2)}) collective-permute-start(bf16[16,1024]{1,0:T(8,128)(2,1)S(1)} %get-tuple-element.35.refs_0_), channel_id=1, source_target_pairs={{0,1},{1,0},{2,3},{3,2},{4,5},{5,4},{6,7},{7,6},{8,9},{9,8},{10,11... | collective-permute-start | bytes 98312 | tf_op jit(solution)/shard_map/ppermute | solution.py:20
  5.6 2.5 %copy-start.2 = (bf16[1024,1024]{1,0:T(8,128)(2,1)S(1)}, bf16[1024,1024]{1,0:T(8,128)(2,1)}, u32[]{:S(2)}) copy-start(bf16[1024,1024]{1,0:T(8,128)(2,1)} %refs_3_.1) | copy-start | bytes 6291460
  5.6 2.5 %copy-start.6 = (bf16[16,1024]{1,0:T(8,128)(2,1)S(1)}, bf16[16,1024]{1,0:T(8,128)(2,1)}, u32[]{:S(2)}) copy-start(bf16[16,1024]{1,0:T(8,128)(2,1)} %refs_2_.1) | copy-start | bytes 98308
  5.6 21.0 %copy-start.3 = (bf16[1024,352]{0,1:T(8,128)(2,1)S(1)}, bf16[1024,352]{0,1:T(8,128)(2,1)}, u32[]{:S(2)}) copy-start(bf16[1024,352]{0,1:T(8,128)(2,1)} %param.29) | copy-start | bytes 2162692
  5.6 21.0 %copy-start.4 = (bf16[1024,352]{0,1:T(8,128)(2,1)S(1)}, bf16[1024,352]{0,1:T(8,128)(2,1)}, u32[]{:S(2)}) copy-start(bf16[1024,352]{0,1:T(8,128)(2,1)} %param.30) | copy-start | bytes 2162692
  5.6 21.0 %copy-start.7 = (f32[1024]{0:T(1024)S(1)}, f32[1024]{0:T(1024)}, u32[]{:S(2)}) copy-start(f32[1024]{0:T(1024)} %param.28) | copy-start | bytes 12292
  6.8 22.5 %copy-start.5 = (bf16[352,1024]{1,0:T(8,128)(2,1)S(1)}, bf16[352,1024]{1,0:T(8,128)(2,1)}, u32[]{:S(2)}) copy-start(bf16[352,1024]{1,0:T(8,128)(2,1)} %refs_1_.1) | copy-start | bytes 2162692
  6.8 1.3 %collective-permute-start.1 = (bf16[16,512]{1,0:T(8,128)(2,1)S(1)}, bf16[16,512]{1,0:T(8,128)(2,1)S(1)}, u32[]{:S(2)}, u32[]{:S(2)}) collective-permute-start(bf16[16,512]{1,0:T(8,128)(2,1)S(1)} %get-tuple-element.47.refs_0_), channel_id=1, source_target_pairs={{0,1},{1,0},{2,3},{3,2},{4,5},{5,4},{6,7},{7,6},{8,9},{9,8},{10,11... | collective-permute-start | bytes 49160 | tf_op jit(solution)/shard_map/ppermute | solution.py:20
  8.5 6.8 %collective-permute-start.4 = (bf16[16,1024]{1,0:T(8,128)(2,1)S(1)}, bf16[16,1024]{1,0:T(8,128)(2,1)S(1)}, u32[]{:S(2)}, u32[]{:S(2)}) collective-permute-start(bf16[16,1024]{1,0:T(8,128)(2,1)S(1)} %out_projection.1.refs_0_), channel_id=1, source_target_pairs={{0,24},{2,26},{4,28},{6,30},{8,16},{10,18},{12,20},{14,22},{16,8},... | collective-permute-start | bytes 98312 | tf_op jit(solution)/shard_map/ppermute | solution.py:41
  13.4 4.8 %collective-permute-start.3 = (bf16[16,1024]{1,0:T(8,128)(2,1)S(1)}, bf16[16,1024]{1,0:T(8,128)(2,1)S(1)}, u32[]{:S(2)}, u32[]{:S(2)}) collective-permute-start(bf16[16,1024]{1,0:T(8,128)(2,1)S(1)} %out_projection.1.refs_0_), channel_id=1, source_target_pairs={{0,16},{2,18},{4,20},{6,22},{8,24},{10,26},{12,28},{14,30},{16,0},... | collective-permute-start | bytes 98312 | tf_op jit(solution)/shard_map/ppermute | solution.py:41
  13.4 4.8 %collective-permute-start.2 = (bf16[16,1024]{1,0:T(8,128)(2,1)S(1)}, bf16[16,1024]{1,0:T(8,128)(2,1)S(1)}, u32[]{:S(2)}, u32[]{:S(2)}) collective-permute-start(bf16[16,1024]{1,0:T(8,128)(2,1)S(1)} %out_projection.1.refs_0_), channel_id=1, source_target_pairs={{0,8},{2,10},{4,12},{6,14},{8,0},{10,2},{12,4},{14,6},{16,24},{18,... | collective-permute-start | bytes 98312 | tf_op jit(solution)/shard_map/ppermute | solution.py:41
  18.3 6.8 %collective-permute-start.7 = (bf16[4,16,1024]{2,1,0:T(8,128)(2,1)S(1)}, bf16[4,16,1024]{2,1,0:T(8,128)(2,1)S(1)}, u32[]{:S(2)}, u32[]{:S(2)}) collective-permute-start(bf16[4,16,1024]{2,1,0:T(8,128)(2,1)S(1)} %stack.1.refs_0_), channel_id=1, source_target_pairs={{0,6},{2,4},{4,2},{6,0},{8,14},{10,12},{12,10},{14,8},{16,22},{18,... | collective-permute-start | bytes 393224 | tf_op jit(solution)/shard_map/ppermute | solution.py:41
  20.8 5.8 %collective-permute-start.6 = (bf16[4,16,1024]{2,1,0:T(8,128)(2,1)S(1)}, bf16[4,16,1024]{2,1,0:T(8,128)(2,1)S(1)}, u32[]{:S(2)}, u32[]{:S(2)}) collective-permute-start(bf16[4,16,1024]{2,1,0:T(8,128)(2,1)S(1)} %stack.1.refs_0_), channel_id=1, source_target_pairs={{0,4},{2,6},{4,0},{6,2},{8,12},{10,14},{12,8},{14,10},{16,20},{18,... | collective-permute-start | bytes 393224 | tf_op jit(solution)/shard_map/ppermute | solution.py:41
  21.3 5.3 %collective-permute-start.5 = (bf16[4,16,1024]{2,1,0:T(8,128)(2,1)S(1)}, bf16[4,16,1024]{2,1,0:T(8,128)(2,1)S(1)}, u32[]{:S(2)}, u32[]{:S(2)}) collective-permute-start(bf16[4,16,1024]{2,1,0:T(8,128)(2,1)S(1)} %stack.1.refs_0_), channel_id=1, source_target_pairs={{0,2},{2,0},{4,6},{6,4},{8,10},{10,8},{12,14},{14,12},{16,18},{18,... | collective-permute-start | bytes 393224 | tf_op jit(solution)/shard_map/ppermute | solution.py:41
  27.4 1.8 %collective-permute-start.8 = (bf16[256,768]{1,0:T(8,128)(2,1)S(1)}, bf16[256,768]{1,0:T(8,128)(2,1)S(1)}, u32[]{:S(2)}, u32[]{:S(2)}) collective-permute-start(bf16[256,768]{1,0:T(8,128)(2,1)S(1)} %get-tuple-element.49), channel_id=1, source_target_pairs={{0,1},{1,0},{2,3},{3,2},{4,5},{5,4},{6,7},{7,6},{8,9},{9,8},{10,11... | collective-permute-start | bytes 1179656 | tf_op jit(solution)/shard_map/ppermute | solution.py:20
  29.8 8.1 %collective-permute-start.9 = (bf16[4,16,1024]{2,1,0:T(8,128)(2,1)S(1)}, bf16[4,16,1024]{2,1,0:T(8,128)(2,1)S(1)}, u32[]{:S(2)}, u32[]{:S(2)}) collective-permute-start(bf16[4,16,1024]{2,1,0:T(8,128)(2,1)S(1)} %get-tuple-element.51), channel_id=1, source_target_pairs={{0,2},{2,0},{4,6},{6,4},{8,10},{10,8},{12,14},{14,12},{16,18},{18,... | collective-permute-start | bytes 393224 | tf_op jit(solution)/shard_map/ppermute | solution.py:41
  31.4 8.1 %collective-permute-start.10 = (bf16[4,16,1024]{2,1,0:T(8,128)(2,1)S(1)}, bf16[4,16,1024]{2,1,0:T(8,128)(2,1)S(1)}, u32[]{:S(2)}, u32[]{:S(2)}) collective-permute-start(bf16[4,16,1024]{2,1,0:T(8,128)(2,1)S(1)} %get-tuple-element.52), channel_id=1, source_target_pairs={{0,4},{2,6},{4,0},{6,2},{8,12},{10,14},{12,8},{14,10},{16,20},{18,... | collective-permute-start | bytes 393224 | tf_op jit(solution)/shard_map/ppermute | solution.py:41
  32.1 7.3 %collective-permute-start.11 = (bf16[4,16,1024]{2,1,0:T(8,128)(2,1)S(1)}, bf16[4,16,1024]{2,1,0:T(8,128)(2,1)S(1)}, u32[]{:S(2)}, u32[]{:S(2)}) collective-permute-start(bf16[4,16,1024]{2,1,0:T(8,128)(2,1)S(1)} %get-tuple-element.53), channel_id=1, source_target_pairs={{0,6},{2,4},{4,2},{6,0},{8,14},{10,12},{12,10},{14,8},{16,22},{18,... | collective-permute-start | bytes 393224 | tf_op jit(solution)/shard_map/ppermute | solution.py:41
  39.6 4.5 %collective-permute-start.12 = (bf16[16,1024]{1,0:T(8,128)(2,1)S(1)}, bf16[16,1024]{1,0:T(8,128)(2,1)S(1)}, u32[]{:S(2)}, u32[]{:S(2)}) collective-permute-start(bf16[16,1024]{1,0:T(8,128)(2,1)S(1)} %get-tuple-element.60), channel_id=1, source_target_pairs={{0,8},{2,10},{4,12},{6,14},{8,0},{10,2},{12,4},{14,6},{16,24},{18,... | collective-permute-start | bytes 98312 | tf_op jit(solution)/shard_map/ppermute | solution.py:41
  39.9 5.2 %collective-permute-start.13 = (bf16[16,1024]{1,0:T(8,128)(2,1)S(1)}, bf16[16,1024]{1,0:T(8,128)(2,1)S(1)}, u32[]{:S(2)}, u32[]{:S(2)}) collective-permute-start(bf16[16,1024]{1,0:T(8,128)(2,1)S(1)} %get-tuple-element.61), channel_id=1, source_target_pairs={{0,16},{2,18},{4,20},{6,22},{8,24},{10,26},{12,28},{14,30},{16,0},... | collective-permute-start | bytes 98312 | tf_op jit(solution)/shard_map/ppermute | solution.py:41
  41.7 5.7 %collective-permute-start.14 = (bf16[16,1024]{1,0:T(8,128)(2,1)S(1)}, bf16[16,1024]{1,0:T(8,128)(2,1)S(1)}, u32[]{:S(2)}, u32[]{:S(2)}) collective-permute-start(bf16[16,1024]{1,0:T(8,128)(2,1)S(1)} %get-tuple-element.62), channel_id=1, source_target_pairs={{0,24},{2,26},{4,28},{6,30},{8,16},{10,18},{12,20},{14,22},{16,8},... | collective-permute-start | bytes 98312 | tf_op jit(solution)/shard_map/ppermute | solution.py:41

commit v5 on v4

--- a/solution.py
+++ b/solution.py
@@ -6,6 +6,7 @@
 from jax.experimental import pallas as pl
 from jax.experimental.pallas import tpu as pltpu
 from jax.sharding import PartitionSpec as P
+
 
 BF16 = jnp.bfloat16
 F32 = jnp.float32
@@ -39,6 +40,13 @@
         a2 = a if inner else partner(a, step, size // low)
         pairs.append((k, a2 * low + b2))
     return lax.ppermute(x, axis, pairs)
+
+
+def staged(sent, size, low, inner):
+    received = []
+    for step, x in enumerate(sent, 1):
+        received.append(exchange(x, "kv", size, low, step, inner))
+    return received
 
 
 def column_pieces(x, axis, size):
@@ -130,7 +138,6 @@
 def run_read(token_pieces, gain, wi, wf, old_max_t, wq, memory):
     rows, heads, dim = memory.shape[:3]
     depth, inner = wq.shape
-    flops = 2 * rows * depth * inner
     return pl.pallas_call(
         functools.partial(read_kernel, len(token_pieces)),
         name="read",
@@ -147,14 +154,14 @@
         out_specs=[VMEM] * 7,
         scratch_shapes=[pltpu.VMEM((rows, depth), F32)],
         compiler_params=pltpu.CompilerParams(vmem_limit_bytes=16 * 2**20),
-        cost_estimate=pl.CostEstimate(flops=flops * 32, bytes_accessed=6 * 2**20, transcendentals=0),
+        cost_estimate=pl.CostEstimate(flops=2**30, bytes_accessed=6 * 2**20, transcendentals=0),
     )(*token_pieces, gain, wi, wf, old_max_t, *map(in_vmem, [wq, memory]))
 
 
 def mix_kernel(*refs):
     (normed, query, old_part, keep, admit, floor, normalizer, wk, wv, wo, *refs) = refs
     (mixed, new_normalizer, key_out, value_out) = refs
-    rows, heads, dim = normalizer.shape
+    _, heads, dim = normalizer.shape
 
     def head(x, h):
         return x[:, h * dim : (h + 1) * dim]
@@ -374,22 +381,18 @@
         pieces = column_pieces(mixed, "tp", tp)
         resid = run_out(pieces, tokens, w_output)
         high, low = group_sizes(kv)
-        column = [resid] + [exchange(resid, "kv", kv, low, step, False) for step in range(1, high)]
+        column = [resid] + staged([resid] * (high - 1), kv, low, False)
         block = run_stack(column, low)
-        every_row = [block] + [exchange(block, "kv", kv, low, step, True) for step in range(1, low)]
+        every_row = [block] + staged([block] * (low - 1), kv, low, True)
         by_head = (rows, heads, head_dim)
-        keys, values = keys.reshape(by_head), values.reshape(by_head)
-        new_memory = keep[..., None, None] * memory + admit[..., None, None] * (
-            keys[..., :, None] * values[..., None, :]
-        )
-
+        outer = keys.reshape(by_head)[..., :, None] * values.reshape(by_head)[..., None, :]
+        new_memory = keep[..., None, None] * memory + admit[..., None, None] * outer
         own, sent = run_up(every_row, ffn_gain[None], w_gate, w_up)
         others = [shifted(sent, "tp", tp, step) for step in range(1, tp)]
         kept, *sent = run_down(own, others, w_down, own_channels * tp, high, low)
-        received = [exchange(x, "kv", kv, low, step, True) for step, x in enumerate(sent, 1)]
-        *received, new_memory = lax.optimization_barrier((*received, new_memory))
+        received = staged(sent, kv, low, True)
         kept, *sent = run_fold(kept, received, low)
-        received = [exchange(x, "kv", kv, low, step, False) for step, x in enumerate(sent, 1)]
+        received = staged(sent, kv, low, False)
         down_out = kept
         for x in received:
             down_out = down_out + x.astype(F32)
@@ -418,8 +421,10 @@
         P("tp", "kv"),
         P("kv", "tp"),
     )
+    body = make(mesh.shape["kv"], mesh.shape["tp"])
+
     return jax.shard_map(
-        make(mesh.shape["kv"], mesh.shape["tp"]),
+        body,
         mesh=mesh,
         in_specs=placed,
         out_specs=(P("kv", "tp"), P("kv", "tp", None, None), P("kv", "tp", None), P("kv", "tp")),

time: 48.2 us -> 49.4 us (1.025)
  waiting for transfers between devices: 17.3 us -> 18.5 us
    ppermute x12, waiting for transfers between devices: 13.9 us -> 15.1 us  [exchange(): return lax.ppermute(x, axis, pairs)]
  transfers between devices with their start and end apart: 15 -> 15, of which waited for: 11 -> 10; matrix products, arithmetic and copies ran while one was open for 10% -> 9% of each run, Pallas kernels for 0% -> 0%
where the time goes in v5:
time: 49.4 us; the launch traced here: 49.2 us
  waiting for transfers between devices  18.5 us (37%)
  starting transfers between devices  18.2 us (37%)
  Pallas kernels  5.94 us (12%)
  other arithmetic  5.22 us (11%)
  between operations  0.78 us (2%)
  local copies, waits for them, and re-layouts  0.6 us (1%)
    ppermute x12, starting transfers between devices, exchange(): return lax.ppermute(x, axis, pairs)  17.1 us
    ppermute x12, waiting for transfers between devices, exchange(): return lax.ppermute(x, axis, pairs)  15.1 us
    add x1, other arithmetic, per_device(): new_memory = keep[..., None, None] * memory + admit[..., None, None] * outer  4.58 us
    ppermute x3, waiting for transfers between devices, shifted(): return lax.ppermute(x, axis, [(i, (i + step) % size) for i in range(size)])  3.41 us
    pallas_call x1, Pallas kernels, run_read(): pl.pallas_call(functools.partial(read_kernel, len(token_pieces)), name='r...  1.93 us
    ppermute x3, starting transfers between devices, shifted(): return lax.ppermute(x, axis, [(i, (i + step) % size) for i in range(size)])  1.12 us
    pallas_call x1, Pallas kernels, run_mix(): pl.pallas_call(mix_kernel, name='mix', out_shape=[pltpu.VMEM((rows, inner...  1.11 us
    pallas_call x1, Pallas kernels, load(): pl.pallas_call(functools.partial(load_kernel, len(arrays)), name='load',...  1.03 us
  transfers between devices with their start and end apart: 15, of which 10 were waited for; matrix products, arithmetic and copies ran while one was open for 9% of the time, Pallas kernels for 0%

profile of v5, /device:TPU:0, one launch (start us, length us, event | category | flops | bytes accessed | tf_op | source)
XLA Modules:
  0.0 49.2 jit_solution(4071286417812997038)
XLA Ops:
  0.7 1.0 %load.1 = (bf16[16,1024]{1,0:T(8,128)(2,1)S(1)}, f32[1,2048]{1,0:T(1,128)S(1)}, bf16[8,2048]{1,0:T(8,128)(2,1)S(1)}, bf16[8,2048]{1,0:T(8,128)(2,1)S(1)}, f32[16...) custom-call(bf16[16,1024]{1,0:T(8,128)(2,1)} %refs_2_.1, f32[1,2048]{1,0:T(1,128)} %bitcast.13, bf16[8,2048]{1,0:T(8,128)(2,1)} %bitcast.11, ...), custom_call_target="tpu_custom_call" | custom-call | flops 68719476736 | bytes 262144 | tf_op jit(solution)/shard_map/load/pallas_call | solution.py:83
  1.7 0.6 %collective-permute-start = (bf16[16,1024]{1,0:T(8,128)(2,1)S(1)}, bf16[16,1024]{1,0:T(8,128)(2,1)S(1)}, u32[]{:S(2)}, u32[]{:S(2)}) collective-permute-start(bf16[16,1024]{1,0:T(8,128)(2,1)S(1)} %get-tuple-element.31.refs_0_), channel_id=1, source_target_pairs={{0,1},{1,0},{2,3},{3,2},{4,5},{5,4},{6,7},{7,6},{8,9},{9,8},{10,11... | collective-permute-start | bytes 98312 | tf_op jit(solution)/shard_map/ppermute | solution.py:21
  2.3 0.9 %collective-permute-done.refs_1_ = bf16[16,1024]{1,0:T(8,128)(2,1)S(1)} collective-permute-done((bf16[16,1024]{1,0:T(8,128)(2,1)S(1)}, bf16[16,1024]{1,0:T(8,128)(2,1)S(1)}, u32[]{:S(2)}, u32[]{:S(2)}) %collective-permute-start) | collective-permute-done | bytes 32800 | tf_op jit(solution)/shard_map/ppermute | solution.py:21
  3.2 0.4 copy-done.1
  3.6 1.9 %read.1 = (bf16[16,2048]{1,0:T(8,128)(2,1)S(1)}, f32[16,512]{1,0:T(8,128)S(1)}, f32[4,16,128]{2,1,0:T(8,128)S(1)}, f32[16,4]{1,0:T(8,128)S(1)}, f32[16,4]{1,0:T(...) custom-call(bf16[16,1024]{1,0:T(8,128)(2,1)S(1)} %get-tuple-element.31.refs_0_, ...), custom_call_target="tpu_custom_call" | custom-call | flops 1073741824 | bytes 6291456 | tf_op jit(solution)/shard_map/read/pallas_call | solution.py:141
  5.7 1.1 %mix.1 = (bf16[16,512]{1,0:T(8,128)(2,1)S(1)}, f32[16,4,128]{2,1,0:T(4,128)}, f32[16,512]{1,0:T(8,128)S(1)}, f32[16,512]{1,0:T(8,128)S(1)}) custom-call(bf16[16,2048]{1,0:T(8,128)(2,1)S(1)} %get-tuple-element.36.refs_0_, f32[16,512]{1,0:T(8,128)S(1)} %get-tuple-element.37.refs_1_, f32[4,16,128]{2,1,0:T(8,128)S(1)} %get-tuple-element.38.refs_2_, ...), custom_call_target="tpu_custom_call" | custom-call | flops 3221225472 | bytes 6291456 | tf_op jit(solution)/shard_map/mix/pallas_call | solution.py:194
  6.8 0.5 %collective-permute-start.1 = (bf16[16,512]{1,0:T(8,128)(2,1)S(1)}, bf16[16,512]{1,0:T(8,128)(2,1)S(1)}, u32[]{:S(2)}, u32[]{:S(2)}) collective-permute-start(bf16[16,512]{1,0:T(8,128)(2,1)S(1)} %get-tuple-element.43.refs_0_), channel_id=1, source_target_pairs={{0,1},{1,0},{2,3},{3,2},{4,5},{5,4},{6,7},{7,6},{8,9},{9,8},{10,11... | collective-permute-start | bytes 49160 | tf_op jit(solution)/shard_map/ppermute | solution.py:21
  7.3 0.8 %collective-permute-done.1.refs_1_ = bf16[16,512]{1,0:T(8,128)(2,1)S(1)} collective-permute-done((bf16[16,512]{1,0:T(8,128)(2,1)S(1)}, bf16[16,512]{1,0:T(8,128)(2,1)S(1)}, u32[]{:S(2)}, u32[]{:S(2)}) %collective-permute-start.1) | collective-permute-done | bytes 16416 | tf_op jit(solution)/shard_map/ppermute | solution.py:21
  8.1 0.4 out_projection.1.refs_0_
  8.5 4.9 %collective-permute-start.4 = (bf16[16,1024]{1,0:T(8,128)(2,1)S(1)}, bf16[16,1024]{1,0:T(8,128)(2,1)S(1)}, u32[]{:S(2)}, u32[]{:S(2)}) collective-permute-start(bf16[16,1024]{1,0:T(8,128)(2,1)S(1)} %out_projection.1.refs_0_), channel_id=1, source_target_pairs={{0,24},{2,26},{4,28},{6,30},{8,16},{10,18},{12,20},{14,22},{16,8},... | collective-permute-start | bytes 98312 | tf_op jit(solution)/shard_map/ppermute | solution.py:42
  13.4 0.6 %collective-permute-start.2 = (bf16[16,1024]{1,0:T(8,128)(2,1)S(1)}, bf16[16,1024]{1,0:T(8,128)(2,1)S(1)}, u32[]{:S(2)}, u32[]{:S(2)}) collective-permute-start(bf16[16,1024]{1,0:T(8,128)(2,1)S(1)} %out_projection.1.refs_0_), channel_id=1, source_target_pairs={{0,8},{2,10},{4,12},{6,14},{8,0},{10,2},{12,4},{14,6},{16,24},{18,... | collective-permute-start | bytes 98312 | tf_op jit(solution)/shard_map/ppermute | solution.py:42
  14.0 1.3 %collective-permute-done.4.refs_3_ = bf16[16,1024]{1,0:T(8,128)(2,1)S(1)} collective-permute-done((bf16[16,1024]{1,0:T(8,128)(2,1)S(1)}, bf16[16,1024]{1,0:T(8,128)(2,1)S(1)}, u32[]{:S(2)}, u32[]{:S(2)}) %collective-permute-start.4) | collective-permute-done | bytes 32800 | tf_op jit(solution)/shard_map/ppermute | solution.py:42
  15.3 2.9 %collective-permute-done.3.refs_2_ = bf16[16,1024]{1,0:T(8,128)(2,1)S(1)} collective-permute-done((bf16[16,1024]{1,0:T(8,128)(2,1)S(1)}, bf16[16,1024]{1,0:T(8,128)(2,1)S(1)}, u32[]{:S(2)}, u32[]{:S(2)}) %collective-permute-start.3) | collective-permute-done | bytes 32800 | tf_op jit(solution)/shard_map/ppermute | solution.py:42
  18.3 2.5 %collective-permute-start.7 = (bf16[4,16,1024]{2,1,0:T(8,128)(2,1)S(1)}, bf16[4,16,1024]{2,1,0:T(8,128)(2,1)S(1)}, u32[]{:S(2)}, u32[]{:S(2)}) collective-permute-start(bf16[4,16,1024]{2,1,0:T(8,128)(2,1)S(1)} %stack.1.refs_0_), channel_id=1, source_target_pairs={{0,6},{2,4},{4,2},{6,0},{8,14},{10,12},{12,10},{14,8},{16,22},{18,... | collective-permute-start | bytes 393224 | tf_op jit(solution)/shard_map/ppermute | solution.py:42
  20.8 0.5 %collective-permute-start.6 = (bf16[4,16,1024]{2,1,0:T(8,128)(2,1)S(1)}, bf16[4,16,1024]{2,1,0:T(8,128)(2,1)S(1)}, u32[]{:S(2)}, u32[]{:S(2)}) collective-permute-start(bf16[4,16,1024]{2,1,0:T(8,128)(2,1)S(1)} %stack.1.refs_0_), channel_id=1, source_target_pairs={{0,4},{2,6},{4,0},{6,2},{8,12},{10,14},{12,8},{14,10},{16,20},{18,... | collective-permute-start | bytes 393224 | tf_op jit(solution)/shard_map/ppermute | solution.py:42
  21.3 0.5 %collective-permute-start.5 = (bf16[4,16,1024]{2,1,0:T(8,128)(2,1)S(1)}, bf16[4,16,1024]{2,1,0:T(8,128)(2,1)S(1)}, u32[]{:S(2)}, u32[]{:S(2)}) collective-permute-start(bf16[4,16,1024]{2,1,0:T(8,128)(2,1)S(1)} %stack.1.refs_0_), channel_id=1, source_target_pairs={{0,2},{2,0},{4,6},{6,4},{8,10},{10,8},{12,14},{14,12},{16,18},{18,... | collective-permute-start | bytes 393224 | tf_op jit(solution)/shard_map/ppermute | solution.py:42
  21.8 3.2 %collective-permute-done.7.refs_3_ = bf16[4,16,1024]{2,1,0:T(8,128)(2,1)S(1)} collective-permute-done((bf16[4,16,1024]{2,1,0:T(8,128)(2,1)S(1)}, bf16[4,16,1024]{2,1,0:T(8,128)(2,1)S(1)}, u32[]{:S(2)}, u32[]{:S(2)}) %collective-permute-start.7) | collective-permute-done | bytes 131104 | tf_op jit(solution)/shard_map/ppermute | solution.py:42
  25.0 1.5 %collective-permute-done.6.refs_2_ = bf16[4,16,1024]{2,1,0:T(8,128)(2,1)S(1)} collective-permute-done((bf16[4,16,1024]{2,1,0:T(8,128)(2,1)S(1)}, bf16[4,16,1024]{2,1,0:T(8,128)(2,1)S(1)}, u32[]{:S(2)}, u32[]{:S(2)}) %collective-permute-start.6) | collective-permute-done | bytes 131104 | tf_op jit(solution)/shard_map/ppermute | solution.py:42
  26.5 0.1 collective-permute-done.5.refs_1_
  26.6 0.8 %gate_up.1 = (f32[256,768]{1,0:T(8,128)S(1)}, bf16[256,768]{1,0:T(8,128)(2,1)S(1)}) custom-call(bf16[4,16,1024]{2,1,0:T(8,128)(2,1)S(1)} %stack.1.refs_0_, bf16[4,16,1024]{2,1,0:T(8,128)(2,1)S(1)} %collective-permute-done.5.refs_1_, bf16[4,16,1024]{2,1,0:T(8,128)(2,1)S(1)} %collective-permute-done.6.refs_2_, ...), custom_call_target="tpu_custom_call" | custom-call | flops 369098752 | bytes 4194304 | tf_op jit(solution)/shard_map/gate_up/pallas_call | solution.py:278
  27.5 1.7 %collective-permute-done.8.refs_0_ = bf16[256,768]{1,0:T(8,128)(2,1)S(1)} collective-permute-done((bf16[256,768]{1,0:T(8,128)(2,1)S(1)}, bf16[256,768]{1,0:T(8,128)(2,1)S(1)}, u32[]{:S(2)}, u32[]{:S(2)}) %collective-permute-start.8) | collective-permute-done | bytes 393248 | tf_op jit(solution)/shard_map/ppermute | solution.py:21
  29.2 0.6 %down.1 = (f32[4,16,1024]{2,1,0:T(8,128)S(1)}, bf16[4,16,1024]{2,1,0:T(8,128)(2,1)S(1)}, bf16[4,16,1024]{2,1,0:T(8,128)(2,1)S(1)}, bf16[4,16,1024]{2,1,0:T(8,128)(2,1)S(1)}) custom-call(f32[256,768]{1,0:T(8,128)S(1)} %get-tuple-element.44.own, bf16[256,768]{1,0:T(8,128)(2,1)S(1)} %collective-permute-done.8.refs_0_, bf16[352,1024]{1,0:T(8,128)(2,1)S(1)} %copy-done.5), custom_call_target="tpu_custom_call" | custom-call | flops 184549376 | bytes 2097152 | tf_op jit(solution)/shard_map/down/pallas_call | solution.py:312
  29.8 1.6 %collective-permute-start.9 = (bf16[4,16,1024]{2,1,0:T(8,128)(2,1)S(1)}, bf16[4,16,1024]{2,1,0:T(8,128)(2,1)S(1)}, u32[]{:S(2)}, u32[]{:S(2)}) collective-permute-start(bf16[4,16,1024]{2,1,0:T(8,128)(2,1)S(1)} %get-tuple-element.47), channel_id=1, source_target_pairs={{0,2},{2,0},{4,6},{6,4},{8,10},{10,8},{12,14},{14,12},{16,18},{18,... | collective-permute-start | bytes 393224 | tf_op jit(solution)/shard_map/ppermute | solution.py:42
  31.4 0.7 %collective-permute-start.10 = (bf16[4,16,1024]{2,1,0:T(8,128)(2,1)S(1)}, bf16[4,16,1024]{2,1,0:T(8,128)(2,1)S(1)}, u32[]{:S(2)}, u32[]{:S(2)}) collective-permute-start(bf16[4,16,1024]{2,1,0:T(8,128)(2,1)S(1)} %get-tuple-element.48), channel_id=1, source_target_pairs={{0,4},{2,6},{4,0},{6,2},{8,12},{10,14},{12,8},{14,10},{16,20},{18,... | collective-permute-start | bytes 393224 | tf_op jit(solution)/shard_map/ppermute | solution.py:42
  32.1 1.3 %collective-permute-start.11 = (bf16[4,16,1024]{2,1,0:T(8,128)(2,1)S(1)}, bf16[4,16,1024]{2,1,0:T(8,128)(2,1)S(1)}, u32[]{:S(2)}, u32[]{:S(2)}) collective-permute-start(bf16[4,16,1024]{2,1,0:T(8,128)(2,1)S(1)} %get-tuple-element.49), channel_id=1, source_target_pairs={{0,6},{2,4},{4,2},{6,0},{8,14},{10,12},{12,10},{14,8},{16,22},{18,... | collective-permute-start | bytes 393224 | tf_op jit(solution)/shard_map/ppermute | solution.py:42
  33.4 2.4 %collective-permute-done.9.refs_0_ = bf16[4,16,1024]{2,1,0:T(8,128)(2,1)S(1)} collective-permute-done((bf16[4,16,1024]{2,1,0:T(8,128)(2,1)S(1)}, bf16[4,16,1024]{2,1,0:T(8,128)(2,1)S(1)}, u32[]{:S(2)}, u32[]{:S(2)}) %collective-permute-start.9) | collective-permute-done | bytes 131104 | tf_op jit(solution)/shard_map/ppermute | solution.py:42
  35.8 3.6 %collective-permute-done.10.refs_1_ = bf16[4,16,1024]{2,1,0:T(8,128)(2,1)S(1)} collective-permute-done((bf16[4,16,1024]{2,1,0:T(8,128)(2,1)S(1)}, bf16[4,16,1024]{2,1,0:T(8,128)(2,1)S(1)}, u32[]{:S(2)}, u32[]{:S(2)}) %collective-permute-start.10) | collective-permute-done | bytes 131104 | tf_op jit(solution)/shard_map/ppermute | solution.py:42
  39.6 0.3 collective-permute-start.12
  39.9 1.8 %collective-permute-start.13 = (bf16[16,1024]{1,0:T(8,128)(2,1)S(1)}, bf16[16,1024]{1,0:T(8,128)(2,1)S(1)}, u32[]{:S(2)}, u32[]{:S(2)}) collective-permute-start(bf16[16,1024]{1,0:T(8,128)(2,1)S(1)} %get-tuple-element.52), channel_id=1, source_target_pairs={{0,16},{2,18},{4,20},{6,22},{8,24},{10,26},{12,28},{14,30},{16,0},... | collective-permute-start | bytes 98312 | tf_op jit(solution)/shard_map/ppermute | solution.py:42
  41.7 2.3 %collective-permute-start.14 = (bf16[16,1024]{1,0:T(8,128)(2,1)S(1)}, bf16[16,1024]{1,0:T(8,128)(2,1)S(1)}, u32[]{:S(2)}, u32[]{:S(2)}) collective-permute-start(bf16[16,1024]{1,0:T(8,128)(2,1)S(1)} %get-tuple-element.53), channel_id=1, source_target_pairs={{0,24},{2,26},{4,28},{6,30},{8,16},{10,18},{12,20},{14,22},{16,8},... | collective-permute-start | bytes 98312 | tf_op jit(solution)/shard_map/ppermute | solution.py:42
  44.0 4.6 %multiply_add_fusion = f32[16,4,128,128]{3,2,1,0:T(8,128)} fusion(f32[16,4,128,128]{3,2,1,0:T(8,128)} %refs_7_.2, f32[16,4,128]{2,1,0:T(4,128)S(1)} %mul.38, f32[16,4,128]{2,1,0:T(4,128)S(1)} %mul.36, f32[16,4]{1,0:T(8,128)S(1)} %get-tuple-element.40.refs_4_, f32[16,4]{1,0:T(8,128)S(1)} %get-tuple-element.39.refs_3_), kind=kLoop, calls=%fused_computation | loop fusion | flops 4194304 | bytes 8454656 | tf_op jit(solution)/shard_map/add | solution.py:389
  48.6 0.6 %add_convert_fusion = bf16[16,1024]{1,0:T(8,128)(2,1)} fusion(bf16[16,1024]{1,0:T(8,128)(2,1)S(1)} %collective-permute-done.14, bf16[16,1024]{1,0:T(8,128)(2,1)S(1)} %collective-permute-done.13, f32[16,1024]{1,0:T(8,128)S(1)} %get-tuple-element.50, bf16[16,1024]{1,0:T(8,128)(2,1)S(1)} %collective-permute-done.12, bf16[16,1024]{1,0:T(8,128)(2,1)S(1)} %out_projection.1.refs_0_), kind=kLoop, calls=%fused_computation.1 | loop fusion | flops 147456 | bytes 229376 | tf_op jit(solution)/shard_map/convert_element_type | solution.py:399
  (32 shorter events, 0.3 us)
Async XLA Ops:
  0.6 2.5 %copy-start = (f32[16,4,128,128]{3,2,1,0:T(8,128)S(1)}, f32[16,4,128,128]{3,2,1,0:T(8,128)}, u32[]{:S(2)}) copy-start(f32[16,4,128,128]{3,2,1,0:T(8,128)} %refs_7_.2) | copy-start | bytes 12582916
  0.6 3.0 %copy-start.1 = (bf16[2048,512]{1,0:T(8,128)(2,1)S(1)}, bf16[2048,512]{1,0:T(8,128)(2,1)}, u32[]{:S(2)}) copy-start(bf16[2048,512]{1,0:T(8,128)(2,1)} %refs_6_.1) | copy-start | bytes 6291460
  1.7 3.8 %copy-start.8 = (bf16[2048,512]{1,0:T(8,128)(2,1)S(1)}, bf16[2048,512]{1,0:T(8,128)(2,1)}, u32[]{:S(2)}) copy-start(bf16[2048,512]{1,0:T(8,128)(2,1)} %refs_7_.3) | copy-start | bytes 6291460
  1.7 3.8 %copy-start.9 = (bf16[2048,512]{1,0:T(8,128)(2,1)S(1)}, bf16[2048,512]{1,0:T(8,128)(2,1)}, u32[]{:S(2)}) copy-start(bf16[2048,512]{1,0:T(8,128)(2,1)} %refs_8_.1) | copy-start | bytes 6291460
  1.7 3.9 %copy-start.10 = (bf16[2048,512]{1,0:T(8,128)(2,1)S(1)}, bf16[2048,512]{1,0:T(8,128)(2,1)}, u32[]{:S(2)}) copy-start(bf16[2048,512]{1,0:T(8,128)(2,1)} %refs_9_.1) | copy-start | bytes 6291460
  1.7 1.4 %collective-permute-start = (bf16[16,1024]{1,0:T(8,128)(2,1)S(1)}, bf16[16,1024]{1,0:T(8,128)(2,1)S(1)}, u32[]{:S(2)}, u32[]{:S(2)}) collective-permute-start(bf16[16,1024]{1,0:T(8,128)(2,1)S(1)} %get-tuple-element.31.refs_0_), channel_id=1, source_target_pairs={{0,1},{1,0},{2,3},{3,2},{4,5},{5,4},{6,7},{7,6},{8,9},{9,8},{10,11... | collective-permute-start | bytes 98312 | tf_op jit(solution)/shard_map/ppermute | solution.py:21
  5.6 2.5 %copy-start.2 = (bf16[1024,1024]{1,0:T(8,128)(2,1)S(1)}, bf16[1024,1024]{1,0:T(8,128)(2,1)}, u32[]{:S(2)}) copy-start(bf16[1024,1024]{1,0:T(8,128)(2,1)} %refs_3_.1) | copy-start | bytes 6291460
  5.6 2.5 %copy-start.6 = (bf16[16,1024]{1,0:T(8,128)(2,1)S(1)}, bf16[16,1024]{1,0:T(8,128)(2,1)}, u32[]{:S(2)}) copy-start(bf16[16,1024]{1,0:T(8,128)(2,1)} %refs_2_.1) | copy-start | bytes 98308
  5.6 21.0 %copy-start.3 = (bf16[1024,352]{0,1:T(8,128)(2,1)S(1)}, bf16[1024,352]{0,1:T(8,128)(2,1)}, u32[]{:S(2)}) copy-start(bf16[1024,352]{0,1:T(8,128)(2,1)} %param.29) | copy-start | bytes 2162692
  5.6 21.0 %copy-start.4 = (bf16[1024,352]{0,1:T(8,128)(2,1)S(1)}, bf16[1024,352]{0,1:T(8,128)(2,1)}, u32[]{:S(2)}) copy-start(bf16[1024,352]{0,1:T(8,128)(2,1)} %param.30) | copy-start | bytes 2162692
  5.6 21.0 %copy-start.7 = (f32[1024]{0:T(1024)S(1)}, f32[1024]{0:T(1024)}, u32[]{:S(2)}) copy-start(f32[1024]{0:T(1024)} %param.28) | copy-start | bytes 12292
  6.8 22.5 %copy-start.5 = (bf16[352,1024]{1,0:T(8,128)(2,1)S(1)}, bf16[352,1024]{1,0:T(8,128)(2,1)}, u32[]{:S(2)}) copy-start(bf16[352,1024]{1,0:T(8,128)(2,1)} %refs_1_.1) | copy-start | bytes 2162692
  6.8 1.3 %collective-permute-start.1 = (bf16[16,512]{1,0:T(8,128)(2,1)S(1)}, bf16[16,512]{1,0:T(8,128)(2,1)S(1)}, u32[]{:S(2)}, u32[]{:S(2)}) collective-permute-start(bf16[16,512]{1,0:T(8,128)(2,1)S(1)} %get-tuple-element.43.refs_0_), channel_id=1, source_target_pairs={{0,1},{1,0},{2,3},{3,2},{4,5},{5,4},{6,7},{7,6},{8,9},{9,8},{10,11... | collective-permute-start | bytes 49160 | tf_op jit(solution)/shard_map/ppermute | solution.py:21
  8.5 6.8 %collective-permute-start.4 = (bf16[16,1024]{1,0:T(8,128)(2,1)S(1)}, bf16[16,1024]{1,0:T(8,128)(2,1)S(1)}, u32[]{:S(2)}, u32[]{:S(2)}) collective-permute-start(bf16[16,1024]{1,0:T(8,128)(2,1)S(1)} %out_projection.1.refs_0_), channel_id=1, source_target_pairs={{0,24},{2,26},{4,28},{6,30},{8,16},{10,18},{12,20},{14,22},{16,8},... | collective-permute-start | bytes 98312 | tf_op jit(solution)/shard_map/ppermute | solution.py:42
  13.4 4.8 %collective-permute-start.3 = (bf16[16,1024]{1,0:T(8,128)(2,1)S(1)}, bf16[16,1024]{1,0:T(8,128)(2,1)S(1)}, u32[]{:S(2)}, u32[]{:S(2)}) collective-permute-start(bf16[16,1024]{1,0:T(8,128)(2,1)S(1)} %out_projection.1.refs_0_), channel_id=1, source_target_pairs={{0,16},{2,18},{4,20},{6,22},{8,24},{10,26},{12,28},{14,30},{16,0},... | collective-permute-start | bytes 98312 | tf_op jit(solution)/shard_map/ppermute | solution.py:42
  13.4 4.8 %collective-permute-start.2 = (bf16[16,1024]{1,0:T(8,128)(2,1)S(1)}, bf16[16,1024]{1,0:T(8,128)(2,1)S(1)}, u32[]{:S(2)}, u32[]{:S(2)}) collective-permute-start(bf16[16,1024]{1,0:T(8,128)(2,1)S(1)} %out_projection.1.refs_0_), channel_id=1, source_target_pairs={{0,8},{2,10},{4,12},{6,14},{8,0},{10,2},{12,4},{14,6},{16,24},{18,... | collective-permute-start | bytes 98312 | tf_op jit(solution)/shard_map/ppermute | solution.py:42
  18.3 6.8 %collective-permute-start.7 = (bf16[4,16,1024]{2,1,0:T(8,128)(2,1)S(1)}, bf16[4,16,1024]{2,1,0:T(8,128)(2,1)S(1)}, u32[]{:S(2)}, u32[]{:S(2)}) collective-permute-start(bf16[4,16,1024]{2,1,0:T(8,128)(2,1)S(1)} %stack.1.refs_0_), channel_id=1, source_target_pairs={{0,6},{2,4},{4,2},{6,0},{8,14},{10,12},{12,10},{14,8},{16,22},{18,... | collective-permute-start | bytes 393224 | tf_op jit(solution)/shard_map/ppermute | solution.py:42
  20.8 5.8 %collective-permute-start.6 = (bf16[4,16,1024]{2,1,0:T(8,128)(2,1)S(1)}, bf16[4,16,1024]{2,1,0:T(8,128)(2,1)S(1)}, u32[]{:S(2)}, u32[]{:S(2)}) collective-permute-start(bf16[4,16,1024]{2,1,0:T(8,128)(2,1)S(1)} %stack.1.refs_0_), channel_id=1, source_target_pairs={{0,4},{2,6},{4,0},{6,2},{8,12},{10,14},{12,8},{14,10},{16,20},{18,... | collective-permute-start | bytes 393224 | tf_op jit(solution)/shard_map/ppermute | solution.py:42
  21.3 5.3 %collective-permute-start.5 = (bf16[4,16,1024]{2,1,0:T(8,128)(2,1)S(1)}, bf16[4,16,1024]{2,1,0:T(8,128)(2,1)S(1)}, u32[]{:S(2)}, u32[]{:S(2)}) collective-permute-start(bf16[4,16,1024]{2,1,0:T(8,128)(2,1)S(1)} %stack.1.refs_0_), channel_id=1, source_target_pairs={{0,2},{2,0},{4,6},{6,4},{8,10},{10,8},{12,14},{14,12},{16,18},{18,... | collective-permute-start | bytes 393224 | tf_op jit(solution)/shard_map/ppermute | solution.py:42
  27.4 1.8 %collective-permute-start.8 = (bf16[256,768]{1,0:T(8,128)(2,1)S(1)}, bf16[256,768]{1,0:T(8,128)(2,1)S(1)}, u32[]{:S(2)}, u32[]{:S(2)}) collective-permute-start(bf16[256,768]{1,0:T(8,128)(2,1)S(1)} %get-tuple-element.45), channel_id=1, source_target_pairs={{0,1},{1,0},{2,3},{3,2},{4,5},{5,4},{6,7},{7,6},{8,9},{9,8},{10,11... | collective-permute-start | bytes 1179656 | tf_op jit(solution)/shard_map/ppermute | solution.py:21
  29.8 6.0 %collective-permute-start.9 = (bf16[4,16,1024]{2,1,0:T(8,128)(2,1)S(1)}, bf16[4,16,1024]{2,1,0:T(8,128)(2,1)S(1)}, u32[]{:S(2)}, u32[]{:S(2)}) collective-permute-start(bf16[4,16,1024]{2,1,0:T(8,128)(2,1)S(1)} %get-tuple-element.47), channel_id=1, source_target_pairs={{0,2},{2,0},{4,6},{6,4},{8,10},{10,8},{12,14},{14,12},{16,18},{18,... | collective-permute-start | bytes 393224 | tf_op jit(solution)/shard_map/ppermute | solution.py:42
  31.4 8.1 %collective-permute-start.10 = (bf16[4,16,1024]{2,1,0:T(8,128)(2,1)S(1)}, bf16[4,16,1024]{2,1,0:T(8,128)(2,1)S(1)}, u32[]{:S(2)}, u32[]{:S(2)}) collective-permute-start(bf16[4,16,1024]{2,1,0:T(8,128)(2,1)S(1)} %get-tuple-element.48), channel_id=1, source_target_pairs={{0,4},{2,6},{4,0},{6,2},{8,12},{10,14},{12,8},{14,10},{16,20},{18,... | collective-permute-start | bytes 393224 | tf_op jit(solution)/shard_map/ppermute | solution.py:42
  32.1 7.3 %collective-permute-start.11 = (bf16[4,16,1024]{2,1,0:T(8,128)(2,1)S(1)}, bf16[4,16,1024]{2,1,0:T(8,128)(2,1)S(1)}, u32[]{:S(2)}, u32[]{:S(2)}) collective-permute-start(bf16[4,16,1024]{2,1,0:T(8,128)(2,1)S(1)} %get-tuple-element.49), channel_id=1, source_target_pairs={{0,6},{2,4},{4,2},{6,0},{8,14},{10,12},{12,10},{14,8},{16,22},{18,... | collective-permute-start | bytes 393224 | tf_op jit(solution)/shard_map/ppermute | solution.py:42
  39.6 9.0 %collective-permute-start.12 = (bf16[16,1024]{1,0:T(8,128)(2,1)S(1)}, bf16[16,1024]{1,0:T(8,128)(2,1)S(1)}, u32[]{:S(2)}, u32[]{:S(2)}) collective-permute-start(bf16[16,1024]{1,0:T(8,128)(2,1)S(1)} %get-tuple-element.51), channel_id=1, source_target_pairs={{0,8},{2,10},{4,12},{6,14},{8,0},{10,2},{12,4},{14,6},{16,24},{18,... | collective-permute-start | bytes 98312 | tf_op jit(solution)/shard_map/ppermute | solution.py:42
  39.9 8.7 %collective-permute-start.13 = (bf16[16,1024]{1,0:T(8,128)(2,1)S(1)}, bf16[16,1024]{1,0:T(8,128)(2,1)S(1)}, u32[]{:S(2)}, u32[]{:S(2)}) collective-permute-start(bf16[16,1024]{1,0:T(8,128)(2,1)S(1)} %get-tuple-element.52), channel_id=1, source_target_pairs={{0,16},{2,18},{4,20},{6,22},{8,24},{10,26},{12,28},{14,30},{16,0},... | collective-permute-start | bytes 98312 | tf_op jit(solution)/shard_map/ppermute | solution.py:42
  41.7 6.9 %collective-permute-start.14 = (bf16[16,1024]{1,0:T(8,128)(2,1)S(1)}, bf16[16,1024]{1,0:T(8,128)(2,1)S(1)}, u32[]{:S(2)}, u32[]{:S(2)}) collective-permute-start(bf16[16,1024]{1,0:T(8,128)(2,1)S(1)} %get-tuple-element.53), channel_id=1, source_target_pairs={{0,24},{2,26},{4,28},{6,30},{8,16},{10,18},{12,20},{14,22},{16,8},... | collective-permute-start | bytes 98312 | tf_op jit(solution)/shard_map/ppermute | solution.py:42

commit v6 on v5

--- a/solution.py
+++ b/solution.py
@@ -271,9 +271,9 @@
     sent[:, first : first + LANES] = tile.astype(BF16)
 
 
-def run_up(pieces, gain, w_gate, w_up):
+def run_up(pieces, gain, gate_t, up_t):
     rows, depth = sum(x.shape[0] * x.shape[1] for x in pieces), pieces[0].shape[2]
-    hidden = w_gate.shape[1]
+    hidden = gate_t.shape[0]
     half = (hidden + 2 + LANES - 1) // LANES * LANES
     return pl.pallas_call(
         functools.partial(up_kernel, len(pieces)),
@@ -283,12 +283,11 @@
         out_specs=[VMEM, VMEM],
         compiler_params=pltpu.CompilerParams(vmem_limit_bytes=24 * 2**20),
         cost_estimate=pl.CostEstimate(flops=4 * rows * depth * hidden, bytes_accessed=4 * 2**20, transcendentals=0),
-    )(*pieces, gain, w_gate.T, w_up.T)
-
-
-def down_kernel(others, channels, low, own, *refs):
-    other_refs, (w_down, *refs) = refs[:others], refs[others:]
-    kept, *sent = refs
+    )(*pieces, gain, gate_t, up_t)
+
+
+def down_kernel(others, channels, own, *refs):
+    other_refs, (w_down, *outs) = refs[:others], refs[others:]
     hidden = w_down.shape[0]
     half = own.shape[1] // 2
     gate, up = own[:, :half], own[:, half:]
@@ -300,22 +299,21 @@
     scale = lax.rsqrt(squares / channels + 1e-06)
     gate = scale * gate[:, :hidden]
     act = (gate * jax.nn.sigmoid(gate) * (scale * up[:, :hidden])).astype(BF16)
-    full = jnp.dot(act, w_down[...], preferred_element_type=F32).reshape(low, *kept.shape)
-    kept[...] = full[0]
-    for step, ref in enumerate(sent, 1):
-        ref[...] = full[step].astype(BF16)
-
-
-def run_down(own, others, w_down, channels, high, low):
-    rows = own.shape[0] // (high * low)
+    full = jnp.dot(act, w_down[...], preferred_element_type=F32).reshape(len(outs), *outs[0].shape)
+    for i, ref in enumerate(outs):
+        ref[...] = full[i].astype(ref.dtype)
+
+
+def run_down(own, others, w_down, channels, kind, pieces, high):
+    rows = own.shape[0] // (pieces * high)
     hidden, width = w_down.shape
     return pl.pallas_call(
-        functools.partial(down_kernel, len(others), channels, low),
+        functools.partial(down_kernel, len(others), channels),
         name="down",
-        out_shape=[pltpu.VMEM((high, rows, width), F32)] + [pltpu.VMEM((high, rows, width), BF16)] * (low - 1),
+        out_shape=[pltpu.VMEM((high, rows, width), kind)] * pieces,
         in_specs=[VMEM] * (2 + len(others)),
-        out_specs=[VMEM] * low,
-        compiler_params=pltpu.CompilerParams(vmem_limit_bytes=24 * 2**20),
+        out_specs=[VMEM] * pieces,
+        compiler_params=pltpu.CompilerParams(vmem_limit_bytes=16 * 2**20),
         cost_estimate=pl.CostEstimate(flops=2 * own.shape[0] * width * hidden, bytes_accessed=2**21, transcendentals=0),
     )(own, *others, w_down)
 
@@ -387,9 +385,15 @@
         by_head = (rows, heads, head_dim)
         outer = keys.reshape(by_head)[..., :, None] * values.reshape(by_head)[..., None, :]
         new_memory = keep[..., None, None] * memory + admit[..., None, None] * outer
-        own, sent = run_up(every_row, ffn_gain[None], w_gate, w_up)
-        others = [shifted(sent, "tp", tp, step) for step in range(1, tp)]
-        kept, *sent = run_down(own, others, w_down, own_channels * tp, high, low)
+        gain, gate_t, up_t = ffn_gain[None], w_gate.T, w_up.T
+
+        def mixer(group, kind):
+            own, sent = run_up(group, gain, gate_t, up_t)
+            others = [shifted(sent, "tp", tp, step) for step in range(1, tp)]
+            return run_down(own, others, w_down, own_channels * tp, kind, len(group), high)
+
+        (kept,) = mixer(every_row[:1], F32)
+        sent = mixer(every_row[1:], BF16) if low > 1 else []
         received = staged(sent, kv, low, True)
         kept, *sent = run_fold(kept, received, low)
         received = staged(sent, kv, low, False)

time: 49.4 us -> 49.1 us (level)
  waiting for transfers between devices: 18.5 us -> 17.3 us
  Pallas kernels: 5.94 us -> 6.69 us
    ppermute x12, waiting for transfers between devices: 15.1 us -> 12.8 us  [exchange(): return lax.ppermute(x, axis, pairs)]
    ppermute x3 -> x4, waiting for transfers between devices: 3.41 us -> 4.51 us  [shifted(): return lax.ppermute(x, axis, [(i, (i + step) % size) for i in range(size)])]
    pallas_call x1 -> x2, Pallas kernels: 0.77 us -> 1.23 us  [run_up(): pl.pallas_call(functools.partial(up_kernel, len(pieces)), name='gate_up',...]
    ppermute x3 -> x4, starting transfers between devices: 1.12 us -> 1.19 us  [shifted(): return lax.ppermute(x, axis, [(i, (i + step) % size) for i in range(size)])]
  transfers between devices with their start and end apart: 15 -> 16, of which waited for: 10 -> 11; matrix products, arithmetic and copies ran while one was open for 9% -> 9% of each run, Pallas kernels for 0% -> 2%
where the time goes in v6:
time: 49.1 us; the launch traced here: 48.9 us
  starting transfers between devices  18.3 us (37%)
  waiting for transfers between devices  17.3 us (35%)
  Pallas kernels  6.69 us (14%)
  other arithmetic  5.22 us (11%)
  between operations  0.8 us (2%)
  local copies, waits for them, and re-layouts  0.6 us (1%)
    ppermute x12, starting transfers between devices, exchange(): return lax.ppermute(x, axis, pairs)  17.1 us
    ppermute x12, waiting for transfers between devices, exchange(): return lax.ppermute(x, axis, pairs)  12.8 us
    add x1, other arithmetic, per_device(): new_memory = keep[..., None, None] * memory + admit[..., None, None] * outer  4.58 us
    ppermute x4, waiting for transfers between devices, shifted(): return lax.ppermute(x, axis, [(i, (i + step) % size) for i in range(size)])  4.51 us
    pallas_call x1, Pallas kernels, run_read(): pl.pallas_call(functools.partial(read_kernel, len(token_pieces)), name='r...  1.93 us
    pallas_call x2, Pallas kernels, run_up(): pl.pallas_call(functools.partial(up_kernel, len(pieces)), name='gate_up',...  1.23 us
    ppermute x4, starting transfers between devices, shifted(): return lax.ppermute(x, axis, [(i, (i + step) % size) for i in range(size)])  1.19 us
    pallas_call x1, Pallas kernels, run_mix(): pl.pallas_call(mix_kernel, name='mix', out_shape=[pltpu.VMEM((rows, inner...  1.11 us
  transfers between devices with their start and end apart: 16, of which 11 were waited for; matrix products, arithmetic and copies ran while one was open for 9% of the time, Pallas kernels for 2%

profile of v6, /device:TPU:0, one launch (start us, length us, event | category | flops | bytes accessed | tf_op | source)
XLA Modules:
  0.0 48.9 jit_solution(13268702527964978644)
XLA Ops:
  0.7 1.0 %load.1 = (bf16[16,1024]{1,0:T(8,128)(2,1)S(1)}, f32[1,2048]{1,0:T(1,128)S(1)}, bf16[8,2048]{1,0:T(8,128)(2,1)S(1)}, bf16[8,2048]{1,0:T(8,128)(2,1)S(1)}, f32[16...) custom-call(bf16[16,1024]{1,0:T(8,128)(2,1)} %refs_2_.1, f32[1,2048]{1,0:T(1,128)} %bitcast.16, bf16[8,2048]{1,0:T(8,128)(2,1)} %bitcast.14, ...), custom_call_target="tpu_custom_call" | custom-call | flops 68719476736 | bytes 262144 | tf_op jit(solution)/shard_map/load/pallas_call | solution.py:83
  1.7 0.6 %collective-permute-start = (bf16[16,1024]{1,0:T(8,128)(2,1)S(1)}, bf16[16,1024]{1,0:T(8,128)(2,1)S(1)}, u32[]{:S(2)}, u32[]{:S(2)}) collective-permute-start(bf16[16,1024]{1,0:T(8,128)(2,1)S(1)} %get-tuple-element.32.refs_0_), channel_id=1, source_target_pairs={{0,1},{1,0},{2,3},{3,2},{4,5},{5,4},{6,7},{7,6},{8,9},{9,8},{10,11... | collective-permute-start | bytes 98312 | tf_op jit(solution)/shard_map/ppermute | solution.py:21
  2.3 0.9 %collective-permute-done.refs_1_ = bf16[16,1024]{1,0:T(8,128)(2,1)S(1)} collective-permute-done((bf16[16,1024]{1,0:T(8,128)(2,1)S(1)}, bf16[16,1024]{1,0:T(8,128)(2,1)S(1)}, u32[]{:S(2)}, u32[]{:S(2)}) %collective-permute-start) | collective-permute-done | bytes 32800 | tf_op jit(solution)/shard_map/ppermute | solution.py:21
  3.2 0.4 copy-done.4
  3.6 1.9 %read.1 = (bf16[16,2048]{1,0:T(8,128)(2,1)S(1)}, f32[16,512]{1,0:T(8,128)S(1)}, f32[4,16,128]{2,1,0:T(8,128)S(1)}, f32[16,4]{1,0:T(8,128)S(1)}, f32[16,4]{1,0:T(...) custom-call(bf16[16,1024]{1,0:T(8,128)(2,1)S(1)} %get-tuple-element.32.refs_0_, ...), custom_call_target="tpu_custom_call" | custom-call | flops 1073741824 | bytes 6291456 | tf_op jit(solution)/shard_map/read/pallas_call | solution.py:141
  5.7 1.1 %mix.1 = (bf16[16,512]{1,0:T(8,128)(2,1)S(1)}, f32[16,4,128]{2,1,0:T(4,128)}, f32[16,512]{1,0:T(8,128)S(1)}, f32[16,512]{1,0:T(8,128)S(1)}) custom-call(bf16[16,2048]{1,0:T(8,128)(2,1)S(1)} %get-tuple-element.37.refs_0_, f32[16,512]{1,0:T(8,128)S(1)} %get-tuple-element.38.refs_1_, f32[4,16,128]{2,1,0:T(8,128)S(1)} %get-tuple-element.39.refs_2_, ...), custom_call_target="tpu_custom_call" | custom-call | flops 3221225472 | bytes 6291456 | tf_op jit(solution)/shard_map/mix/pallas_call | solution.py:194
  6.8 0.5 %collective-permute-start.1 = (bf16[16,512]{1,0:T(8,128)(2,1)S(1)}, bf16[16,512]{1,0:T(8,128)(2,1)S(1)}, u32[]{:S(2)}, u32[]{:S(2)}) collective-permute-start(bf16[16,512]{1,0:T(8,128)(2,1)S(1)} %get-tuple-element.44.refs_0_), channel_id=1, source_target_pairs={{0,1},{1,0},{2,3},{3,2},{4,5},{5,4},{6,7},{7,6},{8,9},{9,8},{10,11... | collective-permute-start | bytes 49160 | tf_op jit(solution)/shard_map/ppermute | solution.py:21
  7.3 0.8 %collective-permute-done.1.refs_1_ = bf16[16,512]{1,0:T(8,128)(2,1)S(1)} collective-permute-done((bf16[16,512]{1,0:T(8,128)(2,1)S(1)}, bf16[16,512]{1,0:T(8,128)(2,1)S(1)}, u32[]{:S(2)}, u32[]{:S(2)}) %collective-permute-start.1) | collective-permute-done | bytes 16416 | tf_op jit(solution)/shard_map/ppermute | solution.py:21
  8.1 0.4 out_projection.1.refs_0_
  8.5 4.9 %collective-permute-start.4 = (bf16[16,1024]{1,0:T(8,128)(2,1)S(1)}, bf16[16,1024]{1,0:T(8,128)(2,1)S(1)}, u32[]{:S(2)}, u32[]{:S(2)}) collective-permute-start(bf16[16,1024]{1,0:T(8,128)(2,1)S(1)} %out_projection.1.refs_0_), channel_id=1, source_target_pairs={{0,24},{2,26},{4,28},{6,30},{8,16},{10,18},{12,20},{14,22},{16,8},... | collective-permute-start | bytes 98312 | tf_op jit(solution)/shard_map/ppermute | solution.py:42
  13.4 0.6 %collective-permute-start.2 = (bf16[16,1024]{1,0:T(8,128)(2,1)S(1)}, bf16[16,1024]{1,0:T(8,128)(2,1)S(1)}, u32[]{:S(2)}, u32[]{:S(2)}) collective-permute-start(bf16[16,1024]{1,0:T(8,128)(2,1)S(1)} %out_projection.1.refs_0_), channel_id=1, source_target_pairs={{0,8},{2,10},{4,12},{6,14},{8,0},{10,2},{12,4},{14,6},{16,24},{18,... | collective-permute-start | bytes 98312 | tf_op jit(solution)/shard_map/ppermute | solution.py:42
  14.0 1.3 %collective-permute-done.4.refs_3_ = bf16[16,1024]{1,0:T(8,128)(2,1)S(1)} collective-permute-done((bf16[16,1024]{1,0:T(8,128)(2,1)S(1)}, bf16[16,1024]{1,0:T(8,128)(2,1)S(1)}, u32[]{:S(2)}, u32[]{:S(2)}) %collective-permute-start.4) | collective-permute-done | bytes 32800 | tf_op jit(solution)/shard_map/ppermute | solution.py:42
  15.3 2.9 %collective-permute-done.3.refs_2_ = bf16[16,1024]{1,0:T(8,128)(2,1)S(1)} collective-permute-done((bf16[16,1024]{1,0:T(8,128)(2,1)S(1)}, bf16[16,1024]{1,0:T(8,128)(2,1)S(1)}, u32[]{:S(2)}, u32[]{:S(2)}) %collective-permute-start.3) | collective-permute-done | bytes 32800 | tf_op jit(solution)/shard_map/ppermute | solution.py:42
  18.3 2.5 %collective-permute-start.8 = (bf16[4,16,1024]{2,1,0:T(8,128)(2,1)S(1)}, bf16[4,16,1024]{2,1,0:T(8,128)(2,1)S(1)}, u32[]{:S(2)}, u32[]{:S(2)}) collective-permute-start(bf16[4,16,1024]{2,1,0:T(8,128)(2,1)S(1)} %stack.1.refs_0_), channel_id=1, source_target_pairs={{0,6},{2,4},{4,2},{6,0},{8,14},{10,12},{12,10},{14,8},{16,22},{18,... | collective-permute-start | bytes 393224 | tf_op jit(solution)/shard_map/ppermute | solution.py:42
  20.8 0.5 %collective-permute-start.7 = (bf16[4,16,1024]{2,1,0:T(8,128)(2,1)S(1)}, bf16[4,16,1024]{2,1,0:T(8,128)(2,1)S(1)}, u32[]{:S(2)}, u32[]{:S(2)}) collective-permute-start(bf16[4,16,1024]{2,1,0:T(8,128)(2,1)S(1)} %stack.1.refs_0_), channel_id=1, source_target_pairs={{0,4},{2,6},{4,0},{6,2},{8,12},{10,14},{12,8},{14,10},{16,20},{18,... | collective-permute-start | bytes 393224 | tf_op jit(solution)/shard_map/ppermute | solution.py:42
  21.3 0.5 %collective-permute-start.6 = (bf16[4,16,1024]{2,1,0:T(8,128)(2,1)S(1)}, bf16[4,16,1024]{2,1,0:T(8,128)(2,1)S(1)}, u32[]{:S(2)}, u32[]{:S(2)}) collective-permute-start(bf16[4,16,1024]{2,1,0:T(8,128)(2,1)S(1)} %stack.1.refs_0_), channel_id=1, source_target_pairs={{0,2},{2,0},{4,6},{6,4},{8,10},{10,8},{12,14},{14,12},{16,18},{18,... | collective-permute-start | bytes 393224 | tf_op jit(solution)/shard_map/ppermute | solution.py:42
  21.8 3.2 %collective-permute-done.8.refs_2_ = bf16[4,16,1024]{2,1,0:T(8,128)(2,1)S(1)} collective-permute-done((bf16[4,16,1024]{2,1,0:T(8,128)(2,1)S(1)}, bf16[4,16,1024]{2,1,0:T(8,128)(2,1)S(1)}, u32[]{:S(2)}, u32[]{:S(2)}) %collective-permute-start.8) | collective-permute-done | bytes 131104 | tf_op jit(solution)/shard_map/ppermute | solution.py:42
  25.0 1.5 %collective-permute-done.7.refs_1_ = bf16[4,16,1024]{2,1,0:T(8,128)(2,1)S(1)} collective-permute-done((bf16[4,16,1024]{2,1,0:T(8,128)(2,1)S(1)}, bf16[4,16,1024]{2,1,0:T(8,128)(2,1)S(1)}, u32[]{:S(2)}, u32[]{:S(2)}) %collective-permute-start.7) | collective-permute-done | bytes 131104 | tf_op jit(solution)/shard_map/ppermute | solution.py:42
  26.6 0.7 %gate_up.3 = (f32[192,768]{1,0:T(8,128)S(1)}, bf16[192,768]{1,0:T(8,128)(2,1)S(1)}) custom-call(bf16[4,16,1024]{2,1,0:T(8,128)(2,1)S(1)} %collective-permute-done.6.refs_0_, bf16[4,16,1024]{2,1,0:T(8,128)(2,1)S(1)} %collective-permute-done.7.refs_1_, bf16[4,16,1024]{2,1,0:T(8,128)(2,1)S(1)} %collective-permute-done.8.refs_2_, f32[1,1024]{1,0:T(1,128)S(1)} %bitcast.12, ...), custom_call_target="tpu_custom_call" | custom-call | flops 276824064 | bytes 4194304 | tf_op jit(solution)/shard_map/gate_up/pallas_call | solution.py:278
  27.4 1.6 %collective-permute-done.9.refs_0_ = bf16[192,768]{1,0:T(8,128)(2,1)S(1)} collective-permute-done((bf16[192,768]{1,0:T(8,128)(2,1)S(1)}, bf16[192,768]{1,0:T(8,128)(2,1)S(1)}, u32[]{:S(2)}, u32[]{:S(2)}) %collective-permute-start.9) | collective-permute-done | bytes 294944 | tf_op jit(solution)/shard_map/ppermute | solution.py:21
  29.0 0.5 %down.3 = (bf16[4,16,1024]{2,1,0:T(8,128)(2,1)S(1)}, bf16[4,16,1024]{2,1,0:T(8,128)(2,1)S(1)}, bf16[4,16,1024]{2,1,0:T(8,128)(2,1)S(1)}) custom-call(f32[192,768]{1,0:T(8,128)S(1)} %get-tuple-element.47.own, bf16[192,768]{1,0:T(8,128)(2,1)S(1)} %collective-permute-done.9.refs_0_, bf16[352,1024]{1,0:T(8,128)(2,1)S(1)} %copy-done.3), custom_call_target="tpu_custom_call" | custom-call | flops 138412032 | bytes 2097152 | tf_op jit(solution)/shard_map/down/pallas_call | solution.py:310
  29.5 1.6 %collective-permute-start.10 = (bf16[4,16,1024]{2,1,0:T(8,128)(2,1)S(1)}, bf16[4,16,1024]{2,1,0:T(8,128)(2,1)S(1)}, u32[]{:S(2)}, u32[]{:S(2)}) collective-permute-start(bf16[4,16,1024]{2,1,0:T(8,128)(2,1)S(1)} %get-tuple-element.49), channel_id=1, source_target_pairs={{0,2},{2,0},{4,6},{6,4},{8,10},{10,8},{12,14},{14,12},{16,18},{18,... | collective-permute-start | bytes 393224 | tf_op jit(solution)/shard_map/ppermute | solution.py:42
  31.1 0.7 %collective-permute-start.11 = (bf16[4,16,1024]{2,1,0:T(8,128)(2,1)S(1)}, bf16[4,16,1024]{2,1,0:T(8,128)(2,1)S(1)}, u32[]{:S(2)}, u32[]{:S(2)}) collective-permute-start(bf16[4,16,1024]{2,1,0:T(8,128)(2,1)S(1)} %get-tuple-element.50), channel_id=1, source_target_pairs={{0,4},{2,6},{4,0},{6,2},{8,12},{10,14},{12,8},{14,10},{16,20},{18,... | collective-permute-start | bytes 393224 | tf_op jit(solution)/shard_map/ppermute | solution.py:42
  31.8 1.3 %collective-permute-start.12 = (bf16[4,16,1024]{2,1,0:T(8,128)(2,1)S(1)}, bf16[4,16,1024]{2,1,0:T(8,128)(2,1)S(1)}, u32[]{:S(2)}, u32[]{:S(2)}) collective-permute-start(bf16[4,16,1024]{2,1,0:T(8,128)(2,1)S(1)} %get-tuple-element.51), channel_id=1, source_target_pairs={{0,6},{2,4},{4,2},{6,0},{8,14},{10,12},{12,10},{14,8},{16,22},{18,... | collective-permute-start | bytes 393224 | tf_op jit(solution)/shard_map/ppermute | solution.py:42
  33.1 0.5 %gate_up.2 = (f32[64,768]{1,0:T(8,128)S(1)}, bf16[64,768]{1,0:T(8,128)(2,1)S(1)}) custom-call(bf16[4,16,1024]{2,1,0:T(8,128)(2,1)S(1)} %stack.1.refs_0_, f32[1,1024]{1,0:T(1,128)S(1)} %bitcast.13, bf16[352,1024]{1,0:T(8,128)(2,1)S(1)} %bitcast.9, bf16[352,1024]{1,0:T(8,128)(2,1)S(1)} %bitcast.11), custom_call_target="tpu_custom_call" | custom-call | flops 92274688 | bytes 4194304 | tf_op jit(solution)/shard_map/gate_up/pallas_call | solution.py:278
  33.8 1.2 %collective-permute-done.5.refs_0_ = bf16[64,768]{1,0:T(8,128)(2,1)S(1)} collective-permute-done((bf16[64,768]{1,0:T(8,128)(2,1)S(1)}, bf16[64,768]{1,0:T(8,128)(2,1)S(1)}, u32[]{:S(2)}, u32[]{:S(2)}) %collective-permute-start.5) | collective-permute-done | bytes 98336 | tf_op jit(solution)/shard_map/ppermute | solution.py:21
  35.0 0.4 down.2.kept
  35.5 3.6 %collective-permute-done.11.refs_1_ = bf16[4,16,1024]{2,1,0:T(8,128)(2,1)S(1)} collective-permute-done((bf16[4,16,1024]{2,1,0:T(8,128)(2,1)S(1)}, bf16[4,16,1024]{2,1,0:T(8,128)(2,1)S(1)}, u32[]{:S(2)}, u32[]{:S(2)}) %collective-permute-start.11) | collective-permute-done | bytes 131104 | tf_op jit(solution)/shard_map/ppermute | solution.py:42
  39.6 1.8 %collective-permute-start.14 = (bf16[16,1024]{1,0:T(8,128)(2,1)S(1)}, bf16[16,1024]{1,0:T(8,128)(2,1)S(1)}, u32[]{:S(2)}, u32[]{:S(2)}) collective-permute-start(bf16[16,1024]{1,0:T(8,128)(2,1)S(1)} %get-tuple-element.54), channel_id=1, source_target_pairs={{0,16},{2,18},{4,20},{6,22},{8,24},{10,26},{12,28},{14,30},{16,0},... | collective-permute-start | bytes 98312 | tf_op jit(solution)/shard_map/ppermute | solution.py:42
  41.4 2.3 %collective-permute-start.15 = (bf16[16,1024]{1,0:T(8,128)(2,1)S(1)}, bf16[16,1024]{1,0:T(8,128)(2,1)S(1)}, u32[]{:S(2)}, u32[]{:S(2)}) collective-permute-start(bf16[16,1024]{1,0:T(8,128)(2,1)S(1)} %get-tuple-element.55), channel_id=1, source_target_pairs={{0,24},{2,26},{4,28},{6,30},{8,16},{10,18},{12,20},{14,22},{16,8},... | collective-permute-start | bytes 98312 | tf_op jit(solution)/shard_map/ppermute | solution.py:42
  43.7 4.6 %multiply_add_fusion = f32[16,4,128,128]{3,2,1,0:T(8,128)} fusion(f32[16,4,128,128]{3,2,1,0:T(8,128)} %refs_7_.2, f32[16,4,128]{2,1,0:T(4,128)S(1)} %mul.38, f32[16,4,128]{2,1,0:T(4,128)S(1)} %mul.36, f32[16,4]{1,0:T(8,128)S(1)} %get-tuple-element.41.refs_4_, f32[16,4]{1,0:T(8,128)S(1)} %get-tuple-element.40.refs_3_), kind=kLoop, calls=%fused_computation | loop fusion | flops 4194304 | bytes 8454656 | tf_op jit(solution)/shard_map/add | solution.py:387
  48.3 0.6 %add_convert_fusion = bf16[16,1024]{1,0:T(8,128)(2,1)} fusion(bf16[16,1024]{1,0:T(8,128)(2,1)S(1)} %collective-permute-done.15, bf16[16,1024]{1,0:T(8,128)(2,1)S(1)} %collective-permute-done.14, f32[16,1024]{1,0:T(8,128)S(1)} %get-tuple-element.52, bf16[16,1024]{1,0:T(8,128)(2,1)S(1)} %collective-permute-done.13, bf16[16,1024]{1,0:T(8,128)(2,1)S(1)} %out_projection.1.refs_0_), kind=kLoop, calls=%fused_computation.1 | loop fusion | flops 147456 | bytes 229376 | tf_op jit(solution)/shard_map/convert_element_type | solution.py:403
  (36 shorter events, 1.0 us)
Async XLA Ops:
  0.6 2.5 %copy-start = (f32[16,4,128,128]{3,2,1,0:T(8,128)S(1)}, f32[16,4,128,128]{3,2,1,0:T(8,128)}, u32[]{:S(2)}) copy-start(f32[16,4,128,128]{3,2,1,0:T(8,128)} %refs_7_.2) | copy-start | bytes 12582916
  0.6 3.0 %copy-start.4 = (bf16[2048,512]{1,0:T(8,128)(2,1)S(1)}, bf16[2048,512]{1,0:T(8,128)(2,1)}, u32[]{:S(2)}) copy-start(bf16[2048,512]{1,0:T(8,128)(2,1)} %refs_6_.1) | copy-start | bytes 6291460
  1.7 3.8 %copy-start.8 = (bf16[2048,512]{1,0:T(8,128)(2,1)S(1)}, bf16[2048,512]{1,0:T(8,128)(2,1)}, u32[]{:S(2)}) copy-start(bf16[2048,512]{1,0:T(8,128)(2,1)} %refs_7_.3) | copy-start | bytes 6291460
  1.7 3.8 %copy-start.9 = (bf16[2048,512]{1,0:T(8,128)(2,1)S(1)}, bf16[2048,512]{1,0:T(8,128)(2,1)}, u32[]{:S(2)}) copy-start(bf16[2048,512]{1,0:T(8,128)(2,1)} %refs_8_.1) | copy-start | bytes 6291460
  1.7 3.9 %copy-start.10 = (bf16[2048,512]{1,0:T(8,128)(2,1)S(1)}, bf16[2048,512]{1,0:T(8,128)(2,1)}, u32[]{:S(2)}) copy-start(bf16[2048,512]{1,0:T(8,128)(2,1)} %refs_9_.1) | copy-start | bytes 6291460
  1.7 1.4 %collective-permute-start = (bf16[16,1024]{1,0:T(8,128)(2,1)S(1)}, bf16[16,1024]{1,0:T(8,128)(2,1)S(1)}, u32[]{:S(2)}, u32[]{:S(2)}) collective-permute-start(bf16[16,1024]{1,0:T(8,128)(2,1)S(1)} %get-tuple-element.32.refs_0_), channel_id=1, source_target_pairs={{0,1},{1,0},{2,3},{3,2},{4,5},{5,4},{6,7},{7,6},{8,9},{9,8},{10,11... | collective-permute-start | bytes 98312 | tf_op jit(solution)/shard_map/ppermute | solution.py:21
  5.6 2.5 %copy-start.5 = (bf16[1024,1024]{1,0:T(8,128)(2,1)S(1)}, bf16[1024,1024]{1,0:T(8,128)(2,1)}, u32[]{:S(2)}) copy-start(bf16[1024,1024]{1,0:T(8,128)(2,1)} %refs_3_.1) | copy-start | bytes 6291460
  5.6 2.5 %copy-start.6 = (bf16[16,1024]{1,0:T(8,128)(2,1)S(1)}, bf16[16,1024]{1,0:T(8,128)(2,1)}, u32[]{:S(2)}) copy-start(bf16[16,1024]{1,0:T(8,128)(2,1)} %refs_2_.1) | copy-start | bytes 98308
  5.6 21.0 %copy-start.1 = (bf16[1024,352]{0,1:T(8,128)(2,1)S(1)}, bf16[1024,352]{0,1:T(8,128)(2,1)}, u32[]{:S(2)}) copy-start(bf16[1024,352]{0,1:T(8,128)(2,1)} %param.29) | copy-start | bytes 2162692
  5.6 21.0 %copy-start.2 = (bf16[1024,352]{0,1:T(8,128)(2,1)S(1)}, bf16[1024,352]{0,1:T(8,128)(2,1)}, u32[]{:S(2)}) copy-start(bf16[1024,352]{0,1:T(8,128)(2,1)} %param.30) | copy-start | bytes 2162692
  5.6 21.0 %copy-start.7 = (f32[1024]{0:T(1024)S(1)}, f32[1024]{0:T(1024)}, u32[]{:S(2)}) copy-start(f32[1024]{0:T(1024)} %param.28) | copy-start | bytes 12292
  6.8 22.2 %copy-start.3 = (bf16[352,1024]{1,0:T(8,128)(2,1)S(1)}, bf16[352,1024]{1,0:T(8,128)(2,1)}, u32[]{:S(2)}) copy-start(bf16[352,1024]{1,0:T(8,128)(2,1)} %refs_1_.3) | copy-start | bytes 2162692
  6.8 1.3 %collective-permute-start.1 = (bf16[16,512]{1,0:T(8,128)(2,1)S(1)}, bf16[16,512]{1,0:T(8,128)(2,1)S(1)}, u32[]{:S(2)}, u32[]{:S(2)}) collective-permute-start(bf16[16,512]{1,0:T(8,128)(2,1)S(1)} %get-tuple-element.44.refs_0_), channel_id=1, source_target_pairs={{0,1},{1,0},{2,3},{3,2},{4,5},{5,4},{6,7},{7,6},{8,9},{9,8},{10,11... | collective-permute-start | bytes 49160 | tf_op jit(solution)/shard_map/ppermute | solution.py:21
  8.5 6.8 %collective-permute-start.4 = (bf16[16,1024]{1,0:T(8,128)(2,1)S(1)}, bf16[16,1024]{1,0:T(8,128)(2,1)S(1)}, u32[]{:S(2)}, u32[]{:S(2)}) collective-permute-start(bf16[16,1024]{1,0:T(8,128)(2,1)S(1)} %out_projection.1.refs_0_), channel_id=1, source_target_pairs={{0,24},{2,26},{4,28},{6,30},{8,16},{10,18},{12,20},{14,22},{16,8},... | collective-permute-start | bytes 98312 | tf_op jit(solution)/shard_map/ppermute | solution.py:42
  13.4 4.8 %collective-permute-start.3 = (bf16[16,1024]{1,0:T(8,128)(2,1)S(1)}, bf16[16,1024]{1,0:T(8,128)(2,1)S(1)}, u32[]{:S(2)}, u32[]{:S(2)}) collective-permute-start(bf16[16,1024]{1,0:T(8,128)(2,1)S(1)} %out_projection.1.refs_0_), channel_id=1, source_target_pairs={{0,16},{2,18},{4,20},{6,22},{8,24},{10,26},{12,28},{14,30},{16,0},... | collective-permute-start | bytes 98312 | tf_op jit(solution)/shard_map/ppermute | solution.py:42
  13.4 4.8 %collective-permute-start.2 = (bf16[16,1024]{1,0:T(8,128)(2,1)S(1)}, bf16[16,1024]{1,0:T(8,128)(2,1)S(1)}, u32[]{:S(2)}, u32[]{:S(2)}) collective-permute-start(bf16[16,1024]{1,0:T(8,128)(2,1)S(1)} %out_projection.1.refs_0_), channel_id=1, source_target_pairs={{0,8},{2,10},{4,12},{6,14},{8,0},{10,2},{12,4},{14,6},{16,24},{18,... | collective-permute-start | bytes 98312 | tf_op jit(solution)/shard_map/ppermute | solution.py:42
  18.3 6.8 %collective-permute-start.8 = (bf16[4,16,1024]{2,1,0:T(8,128)(2,1)S(1)}, bf16[4,16,1024]{2,1,0:T(8,128)(2,1)S(1)}, u32[]{:S(2)}, u32[]{:S(2)}) collective-permute-start(bf16[4,16,1024]{2,1,0:T(8,128)(2,1)S(1)} %stack.1.refs_0_), channel_id=1, source_target_pairs={{0,6},{2,4},{4,2},{6,0},{8,14},{10,12},{12,10},{14,8},{16,22},{18,... | collective-permute-start | bytes 393224 | tf_op jit(solution)/shard_map/ppermute | solution.py:42
  20.8 5.8 %collective-permute-start.7 = (bf16[4,16,1024]{2,1,0:T(8,128)(2,1)S(1)}, bf16[4,16,1024]{2,1,0:T(8,128)(2,1)S(1)}, u32[]{:S(2)}, u32[]{:S(2)}) collective-permute-start(bf16[4,16,1024]{2,1,0:T(8,128)(2,1)S(1)} %stack.1.refs_0_), channel_id=1, source_target_pairs={{0,4},{2,6},{4,0},{6,2},{8,12},{10,14},{12,8},{14,10},{16,20},{18,... | collective-permute-start | bytes 393224 | tf_op jit(solution)/shard_map/ppermute | solution.py:42
  21.3 5.3 %collective-permute-start.6 = (bf16[4,16,1024]{2,1,0:T(8,128)(2,1)S(1)}, bf16[4,16,1024]{2,1,0:T(8,128)(2,1)S(1)}, u32[]{:S(2)}, u32[]{:S(2)}) collective-permute-start(bf16[4,16,1024]{2,1,0:T(8,128)(2,1)S(1)} %stack.1.refs_0_), channel_id=1, source_target_pairs={{0,2},{2,0},{4,6},{6,4},{8,10},{10,8},{12,14},{14,12},{16,18},{18,... | collective-permute-start | bytes 393224 | tf_op jit(solution)/shard_map/ppermute | solution.py:42
  27.3 1.6 %collective-permute-start.9 = (bf16[192,768]{1,0:T(8,128)(2,1)S(1)}, bf16[192,768]{1,0:T(8,128)(2,1)S(1)}, u32[]{:S(2)}, u32[]{:S(2)}) collective-permute-start(bf16[192,768]{1,0:T(8,128)(2,1)S(1)} %get-tuple-element.48), channel_id=1, source_target_pairs={{0,1},{1,0},{2,3},{3,2},{4,5},{5,4},{6,7},{7,6},{8,9},{9,8},{10,11... | collective-permute-start | bytes 884744 | tf_op jit(solution)/shard_map/ppermute | solution.py:21
  29.5 6.0 %collective-permute-start.10 = (bf16[4,16,1024]{2,1,0:T(8,128)(2,1)S(1)}, bf16[4,16,1024]{2,1,0:T(8,128)(2,1)S(1)}, u32[]{:S(2)}, u32[]{:S(2)}) collective-permute-start(bf16[4,16,1024]{2,1,0:T(8,128)(2,1)S(1)} %get-tuple-element.49), channel_id=1, source_target_pairs={{0,2},{2,0},{4,6},{6,4},{8,10},{10,8},{12,14},{14,12},{16,18},{18,... | collective-permute-start | bytes 393224 | tf_op jit(solution)/shard_map/ppermute | solution.py:42
  31.1 8.1 %collective-permute-start.11 = (bf16[4,16,1024]{2,1,0:T(8,128)(2,1)S(1)}, bf16[4,16,1024]{2,1,0:T(8,128)(2,1)S(1)}, u32[]{:S(2)}, u32[]{:S(2)}) collective-permute-start(bf16[4,16,1024]{2,1,0:T(8,128)(2,1)S(1)} %get-tuple-element.50), channel_id=1, source_target_pairs={{0,4},{2,6},{4,0},{6,2},{8,12},{10,14},{12,8},{14,10},{16,20},{18,... | collective-permute-start | bytes 393224 | tf_op jit(solution)/shard_map/ppermute | solution.py:42
  31.8 7.3 %collective-permute-start.12 = (bf16[4,16,1024]{2,1,0:T(8,128)(2,1)S(1)}, bf16[4,16,1024]{2,1,0:T(8,128)(2,1)S(1)}, u32[]{:S(2)}, u32[]{:S(2)}) collective-permute-start(bf16[4,16,1024]{2,1,0:T(8,128)(2,1)S(1)} %get-tuple-element.51), channel_id=1, source_target_pairs={{0,6},{2,4},{4,2},{6,0},{8,14},{10,12},{12,10},{14,8},{16,22},{18,... | collective-permute-start | bytes 393224 | tf_op jit(solution)/shard_map/ppermute | solution.py:42
  33.6 1.4 %collective-permute-start.5 = (bf16[64,768]{1,0:T(8,128)(2,1)S(1)}, bf16[64,768]{1,0:T(8,128)(2,1)S(1)}, u32[]{:S(2)}, u32[]{:S(2)}) collective-permute-start(bf16[64,768]{1,0:T(8,128)(2,1)S(1)} %get-tuple-element.46), channel_id=1, source_target_pairs={{0,1},{1,0},{2,3},{3,2},{4,5},{5,4},{6,7},{7,6},{8,9},{9,8},{10,11... | collective-permute-start | bytes 294920 | tf_op jit(solution)/shard_map/ppermute | solution.py:21
  39.3 9.0 %collective-permute-start.13 = (bf16[16,1024]{1,0:T(8,128)(2,1)S(1)}, bf16[16,1024]{1,0:T(8,128)(2,1)S(1)}, u32[]{:S(2)}, u32[]{:S(2)}) collective-permute-start(bf16[16,1024]{1,0:T(8,128)(2,1)S(1)} %get-tuple-element.53), channel_id=1, source_target_pairs={{0,8},{2,10},{4,12},{6,14},{8,0},{10,2},{12,4},{14,6},{16,24},{18,... | collective-permute-start | bytes 98312 | tf_op jit(solution)/shard_map/ppermute | solution.py:42
  39.6 8.7 %collective-permute-start.14 = (bf16[16,1024]{1,0:T(8,128)(2,1)S(1)}, bf16[16,1024]{1,0:T(8,128)(2,1)S(1)}, u32[]{:S(2)}, u32[]{:S(2)}) collective-permute-start(bf16[16,1024]{1,0:T(8,128)(2,1)S(1)} %get-tuple-element.54), channel_id=1, source_target_pairs={{0,16},{2,18},{4,20},{6,22},{8,24},{10,26},{12,28},{14,30},{16,0},... | collective-permute-start | bytes 98312 | tf_op jit(solution)/shard_map/ppermute | solution.py:42
  41.4 6.9 %collective-permute-start.15 = (bf16[16,1024]{1,0:T(8,128)(2,1)S(1)}, bf16[16,1024]{1,0:T(8,128)(2,1)S(1)}, u32[]{:S(2)}, u32[]{:S(2)}) collective-permute-start(bf16[16,1024]{1,0:T(8,128)(2,1)S(1)} %get-tuple-element.55), channel_id=1, source_target_pairs={{0,24},{2,26},{4,28},{6,30},{8,16},{10,18},{12,20},{14,22},{16,8},... | collective-permute-start | bytes 98312 | tf_op jit(solution)/shard_map/ppermute | solution.py:42

commit v7 on v6

--- a/solution.py
+++ b/solution.py
@@ -257,18 +257,21 @@
     x = jnp.concatenate([ref[...].reshape(-1, ref.shape[2]) for ref in piece_refs], axis=0).astype(F32)
     squares = jnp.sum(x * x, axis=1, keepdims=True)
     ffn_in = (x * gain[...]).astype(BF16)
-    own[...] = jnp.zeros_like(own)
-    for weight, first in [(w_gate, 0), (w_up, half)]:
-        own[:, first : first + hidden] = lax.dot_general(ffn_in, weight[...], NT, preferred_element_type=F32)
     lane = lax.broadcasted_iota(jnp.int32, (x.shape[0], LANES), 1)
     high = squares.astype(BF16).astype(F32)
-    first = hidden // LANES * LANES
-    tile = own[:, first : first + LANES]
-    spot = hidden - first
-    own[:, first : first + LANES] = jnp.where(lane == spot, squares, tile)
-    sent[...] = own[...].astype(BF16)
+    whole = hidden // LANES * LANES
+    spot = hidden - whole
+    blank = jnp.zeros((x.shape[0], half - hidden), F32)
+    for weight, first in [(w_gate, 0), (w_up, half)]:
+        part = lax.dot_general(ffn_in, weight[...], NT, preferred_element_type=F32)
+        part = jnp.concatenate([part, blank], axis=1)
+        own[:, first : first + half] = part
+        sent[:, first : first + half] = part.astype(BF16)
+        if not first:
+            tile = part[:, whole : whole + LANES]
+    own[:, whole : whole + LANES] = jnp.where(lane == spot, squares, tile)
     tile = jnp.where(lane == spot, high, jnp.where(lane == spot + 1, squares - high, tile))
-    sent[:, first : first + LANES] = tile.astype(BF16)
+    sent[:, whole : whole + LANES] = tile.astype(BF16)
 
 
 def run_up(pieces, gain, gate_t, up_t):

time: 49.1 us -> 49.1 us (level)
  no operation moved by 1% of the time
where the time goes in v7:
time: 49.1 us; the launch traced here: 48.9 us
  starting transfers between devices  18.3 us (37%)
  waiting for transfers between devices  17.3 us (35%)
  Pallas kernels  6.65 us (14%)
  other arithmetic  5.22 us (11%)
  between operations  0.81 us (2%)
  local copies, waits for them, and re-layouts  0.6 us (1%)
    ppermute x12, starting transfers between devices, exchange(): return lax.ppermute(x, axis, pairs)  17.1 us
    ppermute x12, waiting for transfers between devices, exchange(): return lax.ppermute(x, axis, pairs)  12.8 us
    add x1, other arithmetic, per_device(): new_memory = keep[..., None, None] * memory + admit[..., None, None] * outer  4.58 us
    ppermute x4, waiting for transfers between devices, shifted(): return lax.ppermute(x, axis, [(i, (i + step) % size) for i in range(size)])  4.51 us
    pallas_call x1, Pallas kernels, run_read(): pl.pallas_call(functools.partial(read_kernel, len(token_pieces)), name='r...  1.93 us
    ppermute x4, starting transfers between devices, shifted(): return lax.ppermute(x, axis, [(i, (i + step) % size) for i in range(size)])  1.19 us
    pallas_call x2, Pallas kernels, run_up(): pl.pallas_call(functools.partial(up_kernel, len(pieces)), name='gate_up',...  1.19 us
    pallas_call x1, Pallas kernels, run_mix(): pl.pallas_call(mix_kernel, name='mix', out_shape=[pltpu.VMEM((rows, inner...  1.11 us
  transfers between devices with their start and end apart: 16, of which 11 were waited for; matrix products, arithmetic and copies ran while one was open for 9% of the time, Pallas kernels for 2%

profile of v7, /device:TPU:0, one launch (start us, length us, event | category | flops | bytes accessed | tf_op | source)
XLA Modules:
  0.0 48.9 jit_solution(1370819641936522794)
XLA Ops:
  0.7 1.0 %load.1 = (bf16[16,1024]{1,0:T(8,128)(2,1)S(1)}, f32[1,2048]{1,0:T(1,128)S(1)}, bf16[8,2048]{1,0:T(8,128)(2,1)S(1)}, bf16[8,2048]{1,0:T(8,128)(2,1)S(1)}, f32[16...) custom-call(bf16[16,1024]{1,0:T(8,128)(2,1)} %refs_2_.1, f32[1,2048]{1,0:T(1,128)} %bitcast.16, bf16[8,2048]{1,0:T(8,128)(2,1)} %bitcast.14, ...), custom_call_target="tpu_custom_call" | custom-call | flops 68719476736 | bytes 262144 | tf_op jit(solution)/shard_map/load/pallas_call | solution.py:83
  1.7 0.6 %collective-permute-start = (bf16[16,1024]{1,0:T(8,128)(2,1)S(1)}, bf16[16,1024]{1,0:T(8,128)(2,1)S(1)}, u32[]{:S(2)}, u32[]{:S(2)}) collective-permute-start(bf16[16,1024]{1,0:T(8,128)(2,1)S(1)} %get-tuple-element.32.refs_0_), channel_id=1, source_target_pairs={{0,1},{1,0},{2,3},{3,2},{4,5},{5,4},{6,7},{7,6},{8,9},{9,8},{10,11... | collective-permute-start | bytes 98312 | tf_op jit(solution)/shard_map/ppermute | solution.py:21
  2.3 0.9 %collective-permute-done.refs_1_ = bf16[16,1024]{1,0:T(8,128)(2,1)S(1)} collective-permute-done((bf16[16,1024]{1,0:T(8,128)(2,1)S(1)}, bf16[16,1024]{1,0:T(8,128)(2,1)S(1)}, u32[]{:S(2)}, u32[]{:S(2)}) %collective-permute-start) | collective-permute-done | bytes 32800 | tf_op jit(solution)/shard_map/ppermute | solution.py:21
  3.2 0.4 copy-done.4
  3.6 1.9 %read.1 = (bf16[16,2048]{1,0:T(8,128)(2,1)S(1)}, f32[16,512]{1,0:T(8,128)S(1)}, f32[4,16,128]{2,1,0:T(8,128)S(1)}, f32[16,4]{1,0:T(8,128)S(1)}, f32[16,4]{1,0:T(...) custom-call(bf16[16,1024]{1,0:T(8,128)(2,1)S(1)} %get-tuple-element.32.refs_0_, ...), custom_call_target="tpu_custom_call" | custom-call | flops 1073741824 | bytes 6291456 | tf_op jit(solution)/shard_map/read/pallas_call | solution.py:141
  5.7 1.1 %mix.1 = (bf16[16,512]{1,0:T(8,128)(2,1)S(1)}, f32[16,4,128]{2,1,0:T(4,128)}, f32[16,512]{1,0:T(8,128)S(1)}, f32[16,512]{1,0:T(8,128)S(1)}) custom-call(bf16[16,2048]{1,0:T(8,128)(2,1)S(1)} %get-tuple-element.37.refs_0_, f32[16,512]{1,0:T(8,128)S(1)} %get-tuple-element.38.refs_1_, f32[4,16,128]{2,1,0:T(8,128)S(1)} %get-tuple-element.39.refs_2_, ...), custom_call_target="tpu_custom_call" | custom-call | flops 3221225472 | bytes 6291456 | tf_op jit(solution)/shard_map/mix/pallas_call | solution.py:194
  6.8 0.5 %collective-permute-start.1 = (bf16[16,512]{1,0:T(8,128)(2,1)S(1)}, bf16[16,512]{1,0:T(8,128)(2,1)S(1)}, u32[]{:S(2)}, u32[]{:S(2)}) collective-permute-start(bf16[16,512]{1,0:T(8,128)(2,1)S(1)} %get-tuple-element.44.refs_0_), channel_id=1, source_target_pairs={{0,1},{1,0},{2,3},{3,2},{4,5},{5,4},{6,7},{7,6},{8,9},{9,8},{10,11... | collective-permute-start | bytes 49160 | tf_op jit(solution)/shard_map/ppermute | solution.py:21
  7.3 0.8 %collective-permute-done.1.refs_1_ = bf16[16,512]{1,0:T(8,128)(2,1)S(1)} collective-permute-done((bf16[16,512]{1,0:T(8,128)(2,1)S(1)}, bf16[16,512]{1,0:T(8,128)(2,1)S(1)}, u32[]{:S(2)}, u32[]{:S(2)}) %collective-permute-start.1) | collective-permute-done | bytes 16416 | tf_op jit(solution)/shard_map/ppermute | solution.py:21
  8.1 0.4 out_projection.1.refs_0_
  8.5 4.9 %collective-permute-start.4 = (bf16[16,1024]{1,0:T(8,128)(2,1)S(1)}, bf16[16,1024]{1,0:T(8,128)(2,1)S(1)}, u32[]{:S(2)}, u32[]{:S(2)}) collective-permute-start(bf16[16,1024]{1,0:T(8,128)(2,1)S(1)} %out_projection.1.refs_0_), channel_id=1, source_target_pairs={{0,24},{2,26},{4,28},{6,30},{8,16},{10,18},{12,20},{14,22},{16,8},... | collective-permute-start | bytes 98312 | tf_op jit(solution)/shard_map/ppermute | solution.py:42
  13.4 0.6 %collective-permute-start.2 = (bf16[16,1024]{1,0:T(8,128)(2,1)S(1)}, bf16[16,1024]{1,0:T(8,128)(2,1)S(1)}, u32[]{:S(2)}, u32[]{:S(2)}) collective-permute-start(bf16[16,1024]{1,0:T(8,128)(2,1)S(1)} %out_projection.1.refs_0_), channel_id=1, source_target_pairs={{0,8},{2,10},{4,12},{6,14},{8,0},{10,2},{12,4},{14,6},{16,24},{18,... | collective-permute-start | bytes 98312 | tf_op jit(solution)/shard_map/ppermute | solution.py:42
  14.0 1.3 %collective-permute-done.4.refs_3_ = bf16[16,1024]{1,0:T(8,128)(2,1)S(1)} collective-permute-done((bf16[16,1024]{1,0:T(8,128)(2,1)S(1)}, bf16[16,1024]{1,0:T(8,128)(2,1)S(1)}, u32[]{:S(2)}, u32[]{:S(2)}) %collective-permute-start.4) | collective-permute-done | bytes 32800 | tf_op jit(solution)/shard_map/ppermute | solution.py:42
  15.3 2.9 %collective-permute-done.3.refs_2_ = bf16[16,1024]{1,0:T(8,128)(2,1)S(1)} collective-permute-done((bf16[16,1024]{1,0:T(8,128)(2,1)S(1)}, bf16[16,1024]{1,0:T(8,128)(2,1)S(1)}, u32[]{:S(2)}, u32[]{:S(2)}) %collective-permute-start.3) | collective-permute-done | bytes 32800 | tf_op jit(solution)/shard_map/ppermute | solution.py:42
  18.3 2.5 %collective-permute-start.8 = (bf16[4,16,1024]{2,1,0:T(8,128)(2,1)S(1)}, bf16[4,16,1024]{2,1,0:T(8,128)(2,1)S(1)}, u32[]{:S(2)}, u32[]{:S(2)}) collective-permute-start(bf16[4,16,1024]{2,1,0:T(8,128)(2,1)S(1)} %stack.1.refs_0_), channel_id=1, source_target_pairs={{0,6},{2,4},{4,2},{6,0},{8,14},{10,12},{12,10},{14,8},{16,22},{18,... | collective-permute-start | bytes 393224 | tf_op jit(solution)/shard_map/ppermute | solution.py:42
  20.8 0.5 %collective-permute-start.7 = (bf16[4,16,1024]{2,1,0:T(8,128)(2,1)S(1)}, bf16[4,16,1024]{2,1,0:T(8,128)(2,1)S(1)}, u32[]{:S(2)}, u32[]{:S(2)}) collective-permute-start(bf16[4,16,1024]{2,1,0:T(8,128)(2,1)S(1)} %stack.1.refs_0_), channel_id=1, source_target_pairs={{0,4},{2,6},{4,0},{6,2},{8,12},{10,14},{12,8},{14,10},{16,20},{18,... | collective-permute-start | bytes 393224 | tf_op jit(solution)/shard_map/ppermute | solution.py:42
  21.3 0.5 %collective-permute-start.6 = (bf16[4,16,1024]{2,1,0:T(8,128)(2,1)S(1)}, bf16[4,16,1024]{2,1,0:T(8,128)(2,1)S(1)}, u32[]{:S(2)}, u32[]{:S(2)}) collective-permute-start(bf16[4,16,1024]{2,1,0:T(8,128)(2,1)S(1)} %stack.1.refs_0_), channel_id=1, source_target_pairs={{0,2},{2,0},{4,6},{6,4},{8,10},{10,8},{12,14},{14,12},{16,18},{18,... | collective-permute-start | bytes 393224 | tf_op jit(solution)/shard_map/ppermute | solution.py:42
  21.8 3.2 %collective-permute-done.8.refs_2_ = bf16[4,16,1024]{2,1,0:T(8,128)(2,1)S(1)} collective-permute-done((bf16[4,16,1024]{2,1,0:T(8,128)(2,1)S(1)}, bf16[4,16,1024]{2,1,0:T(8,128)(2,1)S(1)}, u32[]{:S(2)}, u32[]{:S(2)}) %collective-permute-start.8) | collective-permute-done | bytes 131104 | tf_op jit(solution)/shard_map/ppermute | solution.py:42
  25.0 1.5 %collective-permute-done.7.refs_1_ = bf16[4,16,1024]{2,1,0:T(8,128)(2,1)S(1)} collective-permute-done((bf16[4,16,1024]{2,1,0:T(8,128)(2,1)S(1)}, bf16[4,16,1024]{2,1,0:T(8,128)(2,1)S(1)}, u32[]{:S(2)}, u32[]{:S(2)}) %collective-permute-start.7) | collective-permute-done | bytes 131104 | tf_op jit(solution)/shard_map/ppermute | solution.py:42
  26.6 0.7 %gate_up.3 = (f32[192,768]{1,0:T(8,128)S(1)}, bf16[192,768]{1,0:T(8,128)(2,1)S(1)}) custom-call(bf16[4,16,1024]{2,1,0:T(8,128)(2,1)S(1)} %collective-permute-done.6.refs_0_, bf16[4,16,1024]{2,1,0:T(8,128)(2,1)S(1)} %collective-permute-done.7.refs_1_, bf16[4,16,1024]{2,1,0:T(8,128)(2,1)S(1)} %collective-permute-done.8.refs_2_, f32[1,1024]{1,0:T(1,128)S(1)} %bitcast.12, ...), custom_call_target="tpu_custom_call" | custom-call | flops 276824064 | bytes 4194304 | tf_op jit(solution)/shard_map/gate_up/pallas_call | solution.py:281
  27.4 1.6 %collective-permute-done.9.refs_0_ = bf16[192,768]{1,0:T(8,128)(2,1)S(1)} collective-permute-done((bf16[192,768]{1,0:T(8,128)(2,1)S(1)}, bf16[192,768]{1,0:T(8,128)(2,1)S(1)}, u32[]{:S(2)}, u32[]{:S(2)}) %collective-permute-start.9) | collective-permute-done | bytes 294944 | tf_op jit(solution)/shard_map/ppermute | solution.py:21
  29.0 0.5 %down.3 = (bf16[4,16,1024]{2,1,0:T(8,128)(2,1)S(1)}, bf16[4,16,1024]{2,1,0:T(8,128)(2,1)S(1)}, bf16[4,16,1024]{2,1,0:T(8,128)(2,1)S(1)}) custom-call(f32[192,768]{1,0:T(8,128)S(1)} %get-tuple-element.47.own, bf16[192,768]{1,0:T(8,128)(2,1)S(1)} %collective-permute-done.9.refs_0_, bf16[352,1024]{1,0:T(8,128)(2,1)S(1)} %copy-done.3), custom_call_target="tpu_custom_call" | custom-call | flops 138412032 | bytes 2097152 | tf_op jit(solution)/shard_map/down/pallas_call | solution.py:313
  29.5 1.6 %collective-permute-start.10 = (bf16[4,16,1024]{2,1,0:T(8,128)(2,1)S(1)}, bf16[4,16,1024]{2,1,0:T(8,128)(2,1)S(1)}, u32[]{:S(2)}, u32[]{:S(2)}) collective-permute-start(bf16[4,16,1024]{2,1,0:T(8,128)(2,1)S(1)} %get-tuple-element.49), channel_id=1, source_target_pairs={{0,2},{2,0},{4,6},{6,4},{8,10},{10,8},{12,14},{14,12},{16,18},{18,... | collective-permute-start | bytes 393224 | tf_op jit(solution)/shard_map/ppermute | solution.py:42
  31.1 0.7 %collective-permute-start.11 = (bf16[4,16,1024]{2,1,0:T(8,128)(2,1)S(1)}, bf16[4,16,1024]{2,1,0:T(8,128)(2,1)S(1)}, u32[]{:S(2)}, u32[]{:S(2)}) collective-permute-start(bf16[4,16,1024]{2,1,0:T(8,128)(2,1)S(1)} %get-tuple-element.50), channel_id=1, source_target_pairs={{0,4},{2,6},{4,0},{6,2},{8,12},{10,14},{12,8},{14,10},{16,20},{18,... | collective-permute-start | bytes 393224 | tf_op jit(solution)/shard_map/ppermute | solution.py:42
  31.8 1.3 %collective-permute-start.12 = (bf16[4,16,1024]{2,1,0:T(8,128)(2,1)S(1)}, bf16[4,16,1024]{2,1,0:T(8,128)(2,1)S(1)}, u32[]{:S(2)}, u32[]{:S(2)}) collective-permute-start(bf16[4,16,1024]{2,1,0:T(8,128)(2,1)S(1)} %get-tuple-element.51), channel_id=1, source_target_pairs={{0,6},{2,4},{4,2},{6,0},{8,14},{10,12},{12,10},{14,8},{16,22},{18,... | collective-permute-start | bytes 393224 | tf_op jit(solution)/shard_map/ppermute | solution.py:42
  33.1 0.5 %gate_up.2 = (f32[64,768]{1,0:T(8,128)S(1)}, bf16[64,768]{1,0:T(8,128)(2,1)S(1)}) custom-call(bf16[4,16,1024]{2,1,0:T(8,128)(2,1)S(1)} %stack.1.refs_0_, f32[1,1024]{1,0:T(1,128)S(1)} %bitcast.13, bf16[352,1024]{1,0:T(8,128)(2,1)S(1)} %bitcast.9, bf16[352,1024]{1,0:T(8,128)(2,1)S(1)} %bitcast.11), custom_call_target="tpu_custom_call" | custom-call | flops 92274688 | bytes 4194304 | tf_op jit(solution)/shard_map/gate_up/pallas_call | solution.py:281
  33.7 1.2 %collective-permute-done.5.refs_0_ = bf16[64,768]{1,0:T(8,128)(2,1)S(1)} collective-permute-done((bf16[64,768]{1,0:T(8,128)(2,1)S(1)}, bf16[64,768]{1,0:T(8,128)(2,1)S(1)}, u32[]{:S(2)}, u32[]{:S(2)}) %collective-permute-start.5) | collective-permute-done | bytes 98336 | tf_op jit(solution)/shard_map/ppermute | solution.py:21
  35.0 0.4 down.2.kept
  35.5 3.6 %collective-permute-done.11.refs_1_ = bf16[4,16,1024]{2,1,0:T(8,128)(2,1)S(1)} collective-permute-done((bf16[4,16,1024]{2,1,0:T(8,128)(2,1)S(1)}, bf16[4,16,1024]{2,1,0:T(8,128)(2,1)S(1)}, u32[]{:S(2)}, u32[]{:S(2)}) %collective-permute-start.11) | collective-permute-done | bytes 131104 | tf_op jit(solution)/shard_map/ppermute | solution.py:42
  39.5 1.8 %collective-permute-start.14 = (bf16[16,1024]{1,0:T(8,128)(2,1)S(1)}, bf16[16,1024]{1,0:T(8,128)(2,1)S(1)}, u32[]{:S(2)}, u32[]{:S(2)}) collective-permute-start(bf16[16,1024]{1,0:T(8,128)(2,1)S(1)} %get-tuple-element.54), channel_id=1, source_target_pairs={{0,16},{2,18},{4,20},{6,22},{8,24},{10,26},{12,28},{14,30},{16,0},... | collective-permute-start | bytes 98312 | tf_op jit(solution)/shard_map/ppermute | solution.py:42
  41.4 2.3 %collective-permute-start.15 = (bf16[16,1024]{1,0:T(8,128)(2,1)S(1)}, bf16[16,1024]{1,0:T(8,128)(2,1)S(1)}, u32[]{:S(2)}, u32[]{:S(2)}) collective-permute-start(bf16[16,1024]{1,0:T(8,128)(2,1)S(1)} %get-tuple-element.55), channel_id=1, source_target_pairs={{0,24},{2,26},{4,28},{6,30},{8,16},{10,18},{12,20},{14,22},{16,8},... | collective-permute-start | bytes 98312 | tf_op jit(solution)/shard_map/ppermute | solution.py:42
  43.7 4.6 %multiply_add_fusion = f32[16,4,128,128]{3,2,1,0:T(8,128)} fusion(f32[16,4,128,128]{3,2,1,0:T(8,128)} %refs_7_.2, f32[16,4,128]{2,1,0:T(4,128)S(1)} %mul.38, f32[16,4,128]{2,1,0:T(4,128)S(1)} %mul.36, f32[16,4]{1,0:T(8,128)S(1)} %get-tuple-element.41.refs_4_, f32[16,4]{1,0:T(8,128)S(1)} %get-tuple-element.40.refs_3_), kind=kLoop, calls=%fused_computation | loop fusion | flops 4194304 | bytes 8454656 | tf_op jit(solution)/shard_map/add | solution.py:390
  48.3 0.6 %add_convert_fusion = bf16[16,1024]{1,0:T(8,128)(2,1)} fusion(bf16[16,1024]{1,0:T(8,128)(2,1)S(1)} %collective-permute-done.15, bf16[16,1024]{1,0:T(8,128)(2,1)S(1)} %collective-permute-done.14, f32[16,1024]{1,0:T(8,128)S(1)} %get-tuple-element.52, bf16[16,1024]{1,0:T(8,128)(2,1)S(1)} %collective-permute-done.13, bf16[16,1024]{1,0:T(8,128)(2,1)S(1)} %out_projection.1.refs_0_), kind=kLoop, calls=%fused_computation.1 | loop fusion | flops 147456 | bytes 229376 | tf_op jit(solution)/shard_map/convert_element_type | solution.py:406
  (36 shorter events, 1.0 us)
Async XLA Ops:
  0.6 2.5 %copy-start = (f32[16,4,128,128]{3,2,1,0:T(8,128)S(1)}, f32[16,4,128,128]{3,2,1,0:T(8,128)}, u32[]{:S(2)}) copy-start(f32[16,4,128,128]{3,2,1,0:T(8,128)} %refs_7_.2) | copy-start | bytes 12582916
  0.6 3.0 %copy-start.4 = (bf16[2048,512]{1,0:T(8,128)(2,1)S(1)}, bf16[2048,512]{1,0:T(8,128)(2,1)}, u32[]{:S(2)}) copy-start(bf16[2048,512]{1,0:T(8,128)(2,1)} %refs_6_.1) | copy-start | bytes 6291460
  1.7 3.8 %copy-start.8 = (bf16[2048,512]{1,0:T(8,128)(2,1)S(1)}, bf16[2048,512]{1,0:T(8,128)(2,1)}, u32[]{:S(2)}) copy-start(bf16[2048,512]{1,0:T(8,128)(2,1)} %refs_7_.3) | copy-start | bytes 6291460
  1.7 3.8 %copy-start.9 = (bf16[2048,512]{1,0:T(8,128)(2,1)S(1)}, bf16[2048,512]{1,0:T(8,128)(2,1)}, u32[]{:S(2)}) copy-start(bf16[2048,512]{1,0:T(8,128)(2,1)} %refs_8_.1) | copy-start | bytes 6291460
  1.7 3.9 %copy-start.10 = (bf16[2048,512]{1,0:T(8,128)(2,1)S(1)}, bf16[2048,512]{1,0:T(8,128)(2,1)}, u32[]{:S(2)}) copy-start(bf16[2048,512]{1,0:T(8,128)(2,1)} %refs_9_.1) | copy-start | bytes 6291460
  1.7 1.4 %collective-permute-start = (bf16[16,1024]{1,0:T(8,128)(2,1)S(1)}, bf16[16,1024]{1,0:T(8,128)(2,1)S(1)}, u32[]{:S(2)}, u32[]{:S(2)}) collective-permute-start(bf16[16,1024]{1,0:T(8,128)(2,1)S(1)} %get-tuple-element.32.refs_0_), channel_id=1, source_target_pairs={{0,1},{1,0},{2,3},{3,2},{4,5},{5,4},{6,7},{7,6},{8,9},{9,8},{10,11... | collective-permute-start | bytes 98312 | tf_op jit(solution)/shard_map/ppermute | solution.py:21
  5.6 2.5 %copy-start.5 = (bf16[1024,1024]{1,0:T(8,128)(2,1)S(1)}, bf16[1024,1024]{1,0:T(8,128)(2,1)}, u32[]{:S(2)}) copy-start(bf16[1024,1024]{1,0:T(8,128)(2,1)} %refs_3_.1) | copy-start | bytes 6291460
  5.6 2.5 %copy-start.6 = (bf16[16,1024]{1,0:T(8,128)(2,1)S(1)}, bf16[16,1024]{1,0:T(8,128)(2,1)}, u32[]{:S(2)}) copy-start(bf16[16,1024]{1,0:T(8,128)(2,1)} %refs_2_.1) | copy-start | bytes 98308
  5.6 21.0 %copy-start.1 = (bf16[1024,352]{0,1:T(8,128)(2,1)S(1)}, bf16[1024,352]{0,1:T(8,128)(2,1)}, u32[]{:S(2)}) copy-start(bf16[1024,352]{0,1:T(8,128)(2,1)} %param.29) | copy-start | bytes 2162692
  5.6 21.0 %copy-start.2 = (bf16[1024,352]{0,1:T(8,128)(2,1)S(1)}, bf16[1024,352]{0,1:T(8,128)(2,1)}, u32[]{:S(2)}) copy-start(bf16[1024,352]{0,1:T(8,128)(2,1)} %param.30) | copy-start | bytes 2162692
  5.6 21.0 %copy-start.7 = (f32[1024]{0:T(1024)S(1)}, f32[1024]{0:T(1024)}, u32[]{:S(2)}) copy-start(f32[1024]{0:T(1024)} %param.28) | copy-start | bytes 12292
  6.8 22.2 %copy-start.3 = (bf16[352,1024]{1,0:T(8,128)(2,1)S(1)}, bf16[352,1024]{1,0:T(8,128)(2,1)}, u32[]{:S(2)}) copy-start(bf16[352,1024]{1,0:T(8,128)(2,1)} %refs_1_.3) | copy-start | bytes 2162692
  6.8 1.3 %collective-permute-start.1 = (bf16[16,512]{1,0:T(8,128)(2,1)S(1)}, bf16[16,512]{1,0:T(8,128)(2,1)S(1)}, u32[]{:S(2)}, u32[]{:S(2)}) collective-permute-start(bf16[16,512]{1,0:T(8,128)(2,1)S(1)} %get-tuple-element.44.refs_0_), channel_id=1, source_target_pairs={{0,1},{1,0},{2,3},{3,2},{4,5},{5,4},{6,7},{7,6},{8,9},{9,8},{10,11... | collective-permute-start | bytes 49160 | tf_op jit(solution)/shard_map/ppermute | solution.py:21
  8.5 6.8 %collective-permute-start.4 = (bf16[16,1024]{1,0:T(8,128)(2,1)S(1)}, bf16[16,1024]{1,0:T(8,128)(2,1)S(1)}, u32[]{:S(2)}, u32[]{:S(2)}) collective-permute-start(bf16[16,1024]{1,0:T(8,128)(2,1)S(1)} %out_projection.1.refs_0_), channel_id=1, source_target_pairs={{0,24},{2,26},{4,28},{6,30},{8,16},{10,18},{12,20},{14,22},{16,8},... | collective-permute-start | bytes 98312 | tf_op jit(solution)/shard_map/ppermute | solution.py:42
  13.4 4.8 %collective-permute-start.3 = (bf16[16,1024]{1,0:T(8,128)(2,1)S(1)}, bf16[16,1024]{1,0:T(8,128)(2,1)S(1)}, u32[]{:S(2)}, u32[]{:S(2)}) collective-permute-start(bf16[16,1024]{1,0:T(8,128)(2,1)S(1)} %out_projection.1.refs_0_), channel_id=1, source_target_pairs={{0,16},{2,18},{4,20},{6,22},{8,24},{10,26},{12,28},{14,30},{16,0},... | collective-permute-start | bytes 98312 | tf_op jit(solution)/shard_map/ppermute | solution.py:42
  13.4 4.8 %collective-permute-start.2 = (bf16[16,1024]{1,0:T(8,128)(2,1)S(1)}, bf16[16,1024]{1,0:T(8,128)(2,1)S(1)}, u32[]{:S(2)}, u32[]{:S(2)}) collective-permute-start(bf16[16,1024]{1,0:T(8,128)(2,1)S(1)} %out_projection.1.refs_0_), channel_id=1, source_target_pairs={{0,8},{2,10},{4,12},{6,14},{8,0},{10,2},{12,4},{14,6},{16,24},{18,... | collective-permute-start | bytes 98312 | tf_op jit(solution)/shard_map/ppermute | solution.py:42
  18.3 6.8 %collective-permute-start.8 = (bf16[4,16,1024]{2,1,0:T(8,128)(2,1)S(1)}, bf16[4,16,1024]{2,1,0:T(8,128)(2,1)S(1)}, u32[]{:S(2)}, u32[]{:S(2)}) collective-permute-start(bf16[4,16,1024]{2,1,0:T(8,128)(2,1)S(1)} %stack.1.refs_0_), channel_id=1, source_target_pairs={{0,6},{2,4},{4,2},{6,0},{8,14},{10,12},{12,10},{14,8},{16,22},{18,... | collective-permute-start | bytes 393224 | tf_op jit(solution)/shard_map/ppermute | solution.py:42
  20.8 5.8 %collective-permute-start.7 = (bf16[4,16,1024]{2,1,0:T(8,128)(2,1)S(1)}, bf16[4,16,1024]{2,1,0:T(8,128)(2,1)S(1)}, u32[]{:S(2)}, u32[]{:S(2)}) collective-permute-start(bf16[4,16,1024]{2,1,0:T(8,128)(2,1)S(1)} %stack.1.refs_0_), channel_id=1, source_target_pairs={{0,4},{2,6},{4,0},{6,2},{8,12},{10,14},{12,8},{14,10},{16,20},{18,... | collective-permute-start | bytes 393224 | tf_op jit(solution)/shard_map/ppermute | solution.py:42
  21.3 5.3 %collective-permute-start.6 = (bf16[4,16,1024]{2,1,0:T(8,128)(2,1)S(1)}, bf16[4,16,1024]{2,1,0:T(8,128)(2,1)S(1)}, u32[]{:S(2)}, u32[]{:S(2)}) collective-permute-start(bf16[4,16,1024]{2,1,0:T(8,128)(2,1)S(1)} %stack.1.refs_0_), channel_id=1, source_target_pairs={{0,2},{2,0},{4,6},{6,4},{8,10},{10,8},{12,14},{14,12},{16,18},{18,... | collective-permute-start | bytes 393224 | tf_op jit(solution)/shard_map/ppermute | solution.py:42
  27.3 1.6 %collective-permute-start.9 = (bf16[192,768]{1,0:T(8,128)(2,1)S(1)}, bf16[192,768]{1,0:T(8,128)(2,1)S(1)}, u32[]{:S(2)}, u32[]{:S(2)}) collective-permute-start(bf16[192,768]{1,0:T(8,128)(2,1)S(1)} %get-tuple-element.48), channel_id=1, source_target_pairs={{0,1},{1,0},{2,3},{3,2},{4,5},{5,4},{6,7},{7,6},{8,9},{9,8},{10,11... | collective-permute-start | bytes 884744 | tf_op jit(solution)/shard_map/ppermute | solution.py:21
  29.5 6.0 %collective-permute-start.10 = (bf16[4,16,1024]{2,1,0:T(8,128)(2,1)S(1)}, bf16[4,16,1024]{2,1,0:T(8,128)(2,1)S(1)}, u32[]{:S(2)}, u32[]{:S(2)}) collective-permute-start(bf16[4,16,1024]{2,1,0:T(8,128)(2,1)S(1)} %get-tuple-element.49), channel_id=1, source_target_pairs={{0,2},{2,0},{4,6},{6,4},{8,10},{10,8},{12,14},{14,12},{16,18},{18,... | collective-permute-start | bytes 393224 | tf_op jit(solution)/shard_map/ppermute | solution.py:42
  31.1 8.1 %collective-permute-start.11 = (bf16[4,16,1024]{2,1,0:T(8,128)(2,1)S(1)}, bf16[4,16,1024]{2,1,0:T(8,128)(2,1)S(1)}, u32[]{:S(2)}, u32[]{:S(2)}) collective-permute-start(bf16[4,16,1024]{2,1,0:T(8,128)(2,1)S(1)} %get-tuple-element.50), channel_id=1, source_target_pairs={{0,4},{2,6},{4,0},{6,2},{8,12},{10,14},{12,8},{14,10},{16,20},{18,... | collective-permute-start | bytes 393224 | tf_op jit(solution)/shard_map/ppermute | solution.py:42
  31.8 7.3 %collective-permute-start.12 = (bf16[4,16,1024]{2,1,0:T(8,128)(2,1)S(1)}, bf16[4,16,1024]{2,1,0:T(8,128)(2,1)S(1)}, u32[]{:S(2)}, u32[]{:S(2)}) collective-permute-start(bf16[4,16,1024]{2,1,0:T(8,128)(2,1)S(1)} %get-tuple-element.51), channel_id=1, source_target_pairs={{0,6},{2,4},{4,2},{6,0},{8,14},{10,12},{12,10},{14,8},{16,22},{18,... | collective-permute-start | bytes 393224 | tf_op jit(solution)/shard_map/ppermute | solution.py:42
  33.6 1.4 %collective-permute-start.5 = (bf16[64,768]{1,0:T(8,128)(2,1)S(1)}, bf16[64,768]{1,0:T(8,128)(2,1)S(1)}, u32[]{:S(2)}, u32[]{:S(2)}) collective-permute-start(bf16[64,768]{1,0:T(8,128)(2,1)S(1)} %get-tuple-element.46), channel_id=1, source_target_pairs={{0,1},{1,0},{2,3},{3,2},{4,5},{5,4},{6,7},{7,6},{8,9},{9,8},{10,11... | collective-permute-start | bytes 294920 | tf_op jit(solution)/shard_map/ppermute | solution.py:21
  39.2 9.0 %collective-permute-start.13 = (bf16[16,1024]{1,0:T(8,128)(2,1)S(1)}, bf16[16,1024]{1,0:T(8,128)(2,1)S(1)}, u32[]{:S(2)}, u32[]{:S(2)}) collective-permute-start(bf16[16,1024]{1,0:T(8,128)(2,1)S(1)} %get-tuple-element.53), channel_id=1, source_target_pairs={{0,8},{2,10},{4,12},{6,14},{8,0},{10,2},{12,4},{14,6},{16,24},{18,... | collective-permute-start | bytes 98312 | tf_op jit(solution)/shard_map/ppermute | solution.py:42
  39.5 8.7 %collective-permute-start.14 = (bf16[16,1024]{1,0:T(8,128)(2,1)S(1)}, bf16[16,1024]{1,0:T(8,128)(2,1)S(1)}, u32[]{:S(2)}, u32[]{:S(2)}) collective-permute-start(bf16[16,1024]{1,0:T(8,128)(2,1)S(1)} %get-tuple-element.54), channel_id=1, source_target_pairs={{0,16},{2,18},{4,20},{6,22},{8,24},{10,26},{12,28},{14,30},{16,0},... | collective-permute-start | bytes 98312 | tf_op jit(solution)/shard_map/ppermute | solution.py:42
  41.4 6.9 %collective-permute-start.15 = (bf16[16,1024]{1,0:T(8,128)(2,1)S(1)}, bf16[16,1024]{1,0:T(8,128)(2,1)S(1)}, u32[]{:S(2)}, u32[]{:S(2)}) collective-permute-start(bf16[16,1024]{1,0:T(8,128)(2,1)S(1)} %get-tuple-element.55), channel_id=1, source_target_pairs={{0,24},{2,26},{4,28},{6,30},{8,16},{10,18},{12,20},{14,22},{16,8},... | collective-permute-start | bytes 98312 | tf_op jit(solution)/shard_map/ppermute | solution.py:42
